TPU v7x, 256 devices: a whole 4x4x8 slice. The times are simulated.
256 devices in a mesh: sp: 64 (over z, x, core), tp: 4 (over y).
Axes of the slice: x: 4, y: 4, z: 8, core: 2. Of those that a mesh axis runs over, the one named last changes fastest.
Arguments:
- stream: bfloat16 [32768, 2048], P(('sp', 'tp')), may hold values from -6 to 6
- pool_in: bfloat16 [32768, 1024], P('sp', 'tp'), may hold values from -6 to 6
- doc_ids: int32 [32768], P('sp'), may hold values from 0 to 7, never falling along the last dimension, each value on 1 to 8192 neighbouring positions
- pool_map: bfloat16 [4, 256, 512], P('tp'), may hold values from -0.375 to 0.375
- pool_scale: float32 [2048], P('tp'), may hold values from 0.1 to 1.9
- out_weight: bfloat16 [2048, 2048], P('tp'), may hold values from -0.125 to 0.125
- norm_gain: float32 [2048], replicated, may hold values from 0.1 to 1.9
- routes: int32 [32768, 2], P('sp'), may hold values from 0 to 63, all different within a row; in each aligned block of 128 rows (0 to 127, 128 to 255, ...) at most 6 rows name the same one
- route_weight: float32 [32768, 2], P(('sp', 'tp')), may hold values from 0.2 to 1
- expert_gate: bfloat16 [64, 2048, 1024], P('sp', None, 'tp'), may hold values from -0.125 to 0.125
- expert_up: bfloat16 [64, 2048, 1024], P('sp', None, 'tp'), may hold values from -0.125 to 0.125
- expert_down: bfloat16 [64, 1024, 2048], P('sp', 'tp'), may hold values from -0.1875 to 0.1875
Outputs:
- result: bfloat16 [32768, 2048], P(('sp', 'tp'))
Inputs may be any that keep to these rules, and one draw needn't show every extreme that they name: `routes`: each token names 2 different experts; in each aligned block of 128 rows no expert is named by more than 6 rows, a bound that some block reaches. `doc_ids`: never falling; each document holds at most 8192 positions.
All inputs are finite; a program needn't handle non-finite values.
Results may differ from a plain program's by a relative error of at most 0.014.
Values may be sent and summed in bfloat16 or wider, within the bound.
No kernel may reach another device: no remote copies, remote signals or barrier semaphores. Data moves between devices by JAX's collectives and lax.ppermute only.
A program may use at most 64 MiB of HBM per device.

v0:
```python
import jax
import jax.numpy as jnp
from jax import lax
from jax.sharding import PartitionSpec as P

SPAN = 16


EPS = 1e-06


def passed_along(value, axis, by):
    length = lax.axis_size(axis)
    pairs = [(i, i + by) for i in range(length) if 0 <= i + by < length]
    return lax.ppermute(value, axis, pairs)


def cut_along(value, dim, length):
    before, after = (value.shape[:dim], value.shape[dim + 1 :])
    return jnp.moveaxis(value.reshape(*before, length, -1, *after), dim, 0)


def sum_at_owner(value, axis, dim):
    length = lax.axis_size(axis)
    tiles = lax.all_to_all(cut_along(value, dim, length), axis, 0, 0, tiled=True)
    return jnp.sum(tiles.astype(jnp.float32), axis=0)


def slot_table(route_block, expert_count, capacity, top_count):
    flattened = route_block.reshape(-1)
    one_hot = (flattened[:, None] == jnp.arange(expert_count, dtype=jnp.int32)[None, :]).astype(
        jnp.int32
    )
    ranking = jnp.sum((jnp.cumsum(one_hot, axis=0) - one_hot) * one_hot, axis=1)
    target_slot = flattened * capacity + ranking
    matches = target_slot[None, :] == jnp.arange(expert_count * capacity, dtype=jnp.int32)[:, None]
    sources = jnp.sum(
        jnp.where(matches, jnp.arange(flattened.shape[0], dtype=jnp.int32)[None, :], 0), axis=1
    )
    filled = jnp.any(matches, axis=1)
    return (target_slot, sources // top_count, filled)


def per_device(
    stream,
    pool_in,
    doc_ids,
    pool_map,
    pool_scale,
    out_weight,
    norm_gain,
    routes,
    route_weight,
    expert_gate,
    expert_up,
    expert_down,
):
    row_count = pool_in.shape[0]
    model_width = stream.shape[1]
    top_count = routes.shape[1]
    tp_count = lax.axis_size("tp")
    expert_count = lax.axis_size("sp")
    quarter = row_count // tp_count
    capacity = max(2, 3 * top_count * quarter // (2 * expert_count))
    reach_rows = SPAN - 1
    tail_rows = (
        pool_in[row_count - reach_rows :],
        doc_ids[row_count - reach_rows :].astype(jnp.bfloat16),
    )
    prior_rows, prior_docs = passed_along((tail_rows[0], tail_rows[1]), "sp", 1)
    extended = jnp.concatenate([prior_rows, pool_in], axis=0).astype(jnp.float32)
    extended_docs = jnp.concatenate([prior_docs.astype(jnp.float32), doc_ids.astype(jnp.float32)])
    own_docs = doc_ids.astype(jnp.float32)
    window = jnp.left_shift(jnp.int32(2), lax.axis_index("tp"))
    positions = lax.axis_index("sp") * row_count + jnp.arange(row_count, dtype=jnp.int32)
    running = jnp.zeros(pool_in.shape, jnp.float32)
    counts = jnp.zeros((row_count,), jnp.float32)
    for offset in range(reach_rows + 1):
        begin_row = reach_rows - offset
        piece_rows = extended[begin_row : begin_row + row_count]
        piece_docs = extended_docs[begin_row : begin_row + row_count]
        in_window = (offset < window) & (positions - offset >= 0) & (piece_docs == own_docs)
        running = running + jnp.where(in_window[:, None], piece_rows, 0.0)
        counts = counts + in_window.astype(jnp.float32)
    pooled = (running / counts[:, None] - pool_in.astype(jnp.float32)).astype(jnp.bfloat16)
    branch = (jnp.dot(pooled, pool_map[0], preferred_element_type=jnp.float32) * pool_scale).astype(
        jnp.bfloat16
    )
    projected = sum_at_owner(
        jnp.dot(branch, out_weight, preferred_element_type=jnp.float32).astype(jnp.bfloat16),
        "tp",
        0,
    )
    mixed_rows = (stream.astype(jnp.float32) + projected).astype(jnp.bfloat16)
    mixed_up = mixed_rows.astype(jnp.float32)
    normed = (
        mixed_up * lax.rsqrt(jnp.mean(mixed_up * mixed_up, axis=1, keepdims=True) + EPS) * norm_gain
    ).astype(jnp.bfloat16)
    own_routes = lax.dynamic_slice_in_dim(routes, lax.axis_index("tp") * quarter, quarter, 0)
    own_slots, own_sources, own_filled = slot_table(own_routes, expert_count, capacity, top_count)
    token_index = own_sources.reshape(expert_count, 1, capacity)
    filled_slots = own_filled.reshape(expert_count, 1, capacity)
    dispatch = jnp.where(filled_slots[..., None], normed[token_index], jnp.zeros((), jnp.bfloat16))
    arrived = lax.all_to_all(dispatch, "sp", split_axis=0, concat_axis=0, tiled=True)
    arrived = lax.all_gather(arrived, "tp", axis=1, tiled=True)
    stacked = arrived.reshape(-1, model_width)
    gate_pre = jnp.dot(stacked, expert_gate[0], preferred_element_type=jnp.float32)
    up_pre = jnp.dot(stacked, expert_up[0], preferred_element_type=jnp.float32)
    hidden = (jax.nn.silu(gate_pre) * up_pre).astype(jnp.bfloat16)
    partial_out = jnp.dot(hidden, expert_down[0], preferred_element_type=jnp.float32).reshape(
        arrived.shape
    )
    summed = sum_at_owner(partial_out.astype(jnp.bfloat16), "tp", 1).astype(jnp.bfloat16)
    returned = lax.all_to_all(summed, "sp", split_axis=0, concat_axis=0, tiled=True)
    outputs = returned.reshape(expert_count * capacity, model_width)
    picked = outputs[own_slots].astype(jnp.float32).reshape(quarter, top_count, model_width)
    combined = jnp.sum(route_weight[:, :, None] * picked, axis=1)
    return (mixed_up + combined).astype(jnp.bfloat16)


def solution(mesh):
    in_specs = (
        P(("sp", "tp"), None),
        P("sp", "tp"),
        P("sp"),
        P("tp", None, None),
        P("tp"),
        P("tp", None),
        P(),
        P("sp", None),
        P(("sp", "tp"), None),
        P("sp", None, "tp"),
        P("sp", None, "tp"),
        P("sp", "tp", None),
    )
    out_specs = P(("sp", "tp"), None)
    return jax.shard_map(
        per_device, mesh=mesh, in_specs=in_specs, out_specs=out_specs, check_vma=False
    )
```

profile of v0, /device:TPU:2, one launch (start us, length us, event | category | flops | bytes accessed | tf_op | source)
XLA Modules:
  0.0 378.5 jit_solution(2949899418363238842)
XLA Ops:
  6.5 0.0 copy-start
  6.5 0.9 fusion.128
  7.4 0.1 slice.108
  7.5 1.9 collective-permute-start.1
  9.4 0.7 slice.106
  10.1 3.5 collective-permute-start
  13.6 0.0 collective-permute-done.1
  13.6 0.1 pad_maximum_fusion
  13.7 0.8 convert_add_fusion.1
  14.5 0.5 collective-permute-done
  15.0 1.0 maximum_convert_fusion
  16.1 0.0 copy-done
  16.1 5.4 %convolution_convert_fusion = bf16[512,2048]{1,0:T(8,128)(2,1)} fusion(bf16[512,2048]{1,0:T(8,128)(2,1)S(1)} %copy-done, f32[512]{0:T(512)} %param.16, bf16[512,256]{1,0:T(8,128)(2,1)} %param.13, f32[527,256]{1,0:T(8,128)S(1)} %maximum_convert_fusion, bf16[1,256,512]{2,1,0:T(8,128)(2,1)} %param.15, f32[512]{0:T(512)S(1)} %get-tuple-element.9, ...), kind=kOutput, calls=%fused_computation.5 | convolution fusion | flops 1214119936 | bytes 13119488 | tf_op jit(solution)/shard_map/dot_general | solution.py:90
  21.5 4.5 %all-to-all-start = ((bf16[4,128,2048]{2,1,0:T(8,128)(2,1)}), bf16[4,128,2048]{2,1,0:T(8,128)(2,1)S(1)}, u32[]{:S(2)}, u32[]{:S(2)}) async-start(bf16[4,128,2048]{2,1,0:T(8,128)(2,1)} %bitcast.58), calls=%async_computation | async-start | bytes 4194304 | tf_op jit(solution)/shard_map/all_to_all | solution.py:25
  25.9 0.0 all-gather.2.cloned.1.call-start
  25.9 0.7 broadcast_multiply_fusion
  26.7 0.1 copy.35
  26.8 0.1 eq.103
  26.9 0.1 reshape.209
  27.1 0.6 reduce-window.6
  27.7 0.2 slice_reduce_fusion
  27.9 0.1 fusion.73
  28.0 0.2 select_reduce_fusion
  28.2 0.1 reduce_sum.67
  28.4 0.1 reshape.217
  28.5 0.2 fusion.30
  28.7 0.2 broadcast_in_dim.172
  28.8 0.0 copy-start.5
  28.9 23.3 %all-to-all-done = bf16[4,128,2048]{2,1,0:T(8,128)(2,1)S(1)} async-done(((bf16[4,128,2048]{2,1,0:T(8,128)(2,1)}), bf16[4,128,2048]{2,1,0:T(8,128)(2,1)S(1)}, u32[]{:S(2)}, u32[]{:S(2)}) %all-to-all-start) | async-done | bytes 2097184 | tf_op jit(solution)/shard_map/all_to_all | solution.py:25
  52.1 0.4 convert_reduce_fusion
  52.5 0.0 copy-done.4
  52.5 0.3 fusion.2
  52.8 0.0 copy-done.5
  52.8 0.2 fusion.4
  53.0 2.5 gather_fusion
  55.4 1.6 reshape.216
  57.1 1.8 select_bitcast_fusion
  58.9 62.8 %all_to_all.20 = bf16[64,1,6,2048]{3,2,1,0:T(8,128)(2,1)S(1)} all-to-all(bf16[64,1,6,2048]{3,2,1,0:T(8,128)(2,1)S(1)} %select_bitcast_fusion), channel_id=1, replica_groups=mesh['sp'=64,'tp'=4] {'sp'}, dimensions={0} | all-to-all | bytes 3145728 | tf_op jit(solution)/shard_map/all_to_all | solution.py:104
  121.7 2.0 copy.39
  123.7 0.0 all-gather.2.cloned.1.call-update
  123.7 62.7 %all-gather.2.cloned.1.call-done = bf16[64,4,6,2048]{3,0,2,1:T(8,128)(2,1)} async-done(((bf16[64,1,6,2048]{3,0,2,1:T(8,128)(2,1)}), bf16[64,4,6,2048]{3,0,2,1:T(8,128)(2,1)}) %all-gather.2.cloned.1.call-update) | async-done | bytes 6291472 | tf_op jit(solution)/shard_map/all_gather | solution.py:105
  186.4 9.6 %copy.40 = bf16[64,4,6,2048]{3,2,1,0:T(8,128)(2,1)} copy(bf16[64,4,6,2048]{3,0,2,1:T(8,128)(2,1)} %all-gather.2.cloned.1.call-done) | data formatting | bytes 12582912 | tf_op jit(solution)/shard_map/all_gather | solution.py:105
  196.0 11.1 %reshape.211 = bf16[1536,2048]{1,0:T(8,128)(2,1)} reshape(bf16[64,4,6,2048]{3,2,1,0:T(8,128)(2,1)} %copy.40) | data formatting | bytes 12582912 | tf_op jit(solution)/shard_map/reshape | solution.py:106
  207.2 4.8 %fusion.8 = f32[1536,256]{1,0:T(8,128)S(1)} fusion(bf16[1536,2048]{1,0:T(8,128)(2,1)} %reshape.211, bf16[1,2048,256]{2,1,0:T(8,128)(2,1)S(1)} %copy-done.7), kind=kOutput, calls=%fused_computation.21 | convolution fusion | flops 1610612736 | bytes 8912896 | tf_op jit(solution)/shard_map/dot_general | solution.py:107
  212.0 0.0 copy-done.8
  212.0 2.1 fusion
  214.1 0.0 copy-start.3
  214.1 0.3 dot_general.21
  214.4 0.9 copy-done.3
  215.3 2.0 convert_bitcast_fusion
  217.4 74.6 %all_to_all.21 = bf16[4,64,1,6,2048]{4,1,3,2,0:T(8,128)(2,1)S(1)} all-to-all(bf16[4,64,1,6,2048]{4,1,3,2,0:T(8,128)(2,1)S(1)} %convert_bitcast_fusion), channel_id=1, replica_groups=mesh['sp'=64,'tp'=4] {'tp'}, dimensions={0} | all-to-all | bytes 12582912 | tf_op jit(solution)/shard_map/all_to_all | solution.py:25
  291.9 1.2 bitcast_reduce_fusion
  293.2 2.2 copy.44
  295.4 10.9 %all-to-all-start.3 = ((bf16[64,1,6,2048]{3,2,1,0:T(8,128)(2,1)}), bf16[64,1,6,2048]{3,2,1,0:T(8,128)(2,1)}, u32[]{:S(2)}, u32[]{:S(2)}) async-start(bf16[64,1,6,2048]{3,2,1,0:T(8,128)(2,1)} %copy.44), calls=%async_computation.3 | async-start | bytes 4194304 | tf_op jit(solution)/shard_map/all_to_all | solution.py:114
  306.2 0.1 copy.45
  306.3 0.1 mul.92
  306.5 0.1 copy.34
  306.6 50.8 %all-to-all-done.3 = bf16[64,1,6,2048]{3,2,1,0:T(8,128)(2,1)} async-done(((bf16[64,1,6,2048]{3,2,1,0:T(8,128)(2,1)}), bf16[64,1,6,2048]{3,2,1,0:T(8,128)(2,1)}, u32[]{:S(2)}, u32[]{:S(2)}) %all-to-all-start.3) | async-done | bytes 1572896 | tf_op jit(solution)/shard_map/all_to_all | solution.py:114
  357.4 2.6 reshape.213
  360.0 2.3 gather_fusion.1
  362.3 3.5 reshape.214
  365.9 4.8 %multiply_reduce_fusion = f32[128,2048]{1,0:T(8,128)S(1)} fusion(f32[128,2,2048]{2,1,0:T(2,128)} %reshape.214, f32[128,2]{1,0:T(8,128)S(1)} %copy.34), kind=kLoop, calls=%fused_computation.8 | loop fusion | flops 786432 | bytes 3146752 | tf_op jit(solution)/shard_map/reduce_sum | solution.py:117
  370.7 0.9 fusion.5
  371.6 0.0 copy-done.1
  (19 shorter events, 0.1 us)
Async XLA Ops:
  6.5 9.5 %copy-start = (bf16[512,2048]{1,0:T(8,128)(2,1)S(1)}, bf16[512,2048]{1,0:T(8,128)(2,1)}, u32[]{:S(2)}) copy-start(bf16[512,2048]{1,0:T(8,128)(2,1)} %param.17) | copy-start | bytes 6291460
  7.5 6.2 %collective-permute-start.1 = (bf16[15]{0:T(256)(128)(2,1)S(1)}, bf16[15]{0:T(256)(128)(2,1)S(1)}, u32[]{:S(2)}, u32[]{:S(2)}) collective-permute-start(bf16[15]{0:T(256)(128)(2,1)S(1)} %slice.108), channel_id=1, source_target_pairs={{0,4},{4,8},{8,12},{12,16},{16,20},{20,24},{24,28},{28,32},{32,36}... | collective-permute-start | bytes 98 | tf_op jit(solution)/shard_map/ppermute | solution.py:15
  10.1 5.0 %collective-permute-start = (bf16[15,256]{1,0:T(8,128)(2,1)S(1)}, bf16[15,256]{1,0:T(8,128)(2,1)S(1)}, u32[]{:S(2)}, u32[]{:S(2)}) collective-permute-start(bf16[15,256]{1,0:T(8,128)(2,1)S(1)} %slice.106), channel_id=1, source_target_pairs={{0,4},{4,8},{8,12},{12,16},{16,20},{20,24},{24,28},{28,32},{32,36}... | collective-permute-start | bytes 23048 | tf_op jit(solution)/shard_map/ppermute | solution.py:15
  21.5 30.6 %all-to-all-start = ((bf16[4,128,2048]{2,1,0:T(8,128)(2,1)}), bf16[4,128,2048]{2,1,0:T(8,128)(2,1)S(1)}, u32[]{:S(2)}, u32[]{:S(2)}) async-start(bf16[4,128,2048]{2,1,0:T(8,128)(2,1)} %bitcast.58), calls=%async_computation | async-start | bytes 4194304 | tf_op jit(solution)/shard_map/all_to_all | solution.py:25
  25.9 26.6 %copy-start.4 = (bf16[128,2048]{1,0:T(8,128)(2,1)S(1)}, bf16[128,2048]{1,0:T(8,128)(2,1)}, u32[]{:S(2)}) copy-start(bf16[128,2048]{1,0:T(8,128)(2,1)} %param.12) | copy-start | bytes 1572868
  25.9 160.5 %all-gather.2.cloned.1.call-start = ((), (), s32[]{:S(2)}) async-start(), calls=%async_computation.4 | async-start | bytes 7864320 | tf_op jit(solution)/shard_map/all_gather | solution.py:105
  28.8 23.9 %copy-start.5 = (f32[2048]{0:T(1024)S(1)}, f32[2048]{0:T(1024)}, u32[]{:S(2)}) copy-start(f32[2048]{0:T(1024)} %param.18) | copy-start | bytes 24580
  196.0 11.1 %copy-start.7 = (bf16[1,2048,256]{2,1,0:T(8,128)(2,1)S(1)}, bf16[1,2048,256]{2,1,0:T(8,128)(2,1)}, u32[]{:S(2)}) copy-start(bf16[1,2048,256]{2,1,0:T(8,128)(2,1)} %param.21) | copy-start | bytes 3145732
  207.2 4.8 %copy-start.2 = (bf16[1536,2048]{1,0:T(8,128)(2,1)S(1)}, bf16[1536,2048]{1,0:T(8,128)(2,1)}, u32[]{:S(2)}) copy-start(bf16[1536,2048]{1,0:T(8,128)(2,1)} %reshape.211) | copy-start | bytes 18874372
  207.2 4.9 %copy-start.8 = (bf16[1,2048,256]{2,1,0:T(8,128)(2,1)S(1)}, bf16[1,2048,256]{2,1,0:T(8,128)(2,1)}, u32[]{:S(2)}) copy-start(bf16[1,2048,256]{2,1,0:T(8,128)(2,1)} %param.22) | copy-start | bytes 3145732
  214.1 1.2 copy-start.3
  295.4 11.1 %copy-start.6 = (f32[128,2]{0,1:T(2,128)S(1)}, f32[128,2]{0,1:T(2,128)}, u32[]{:S(2)}) copy-start(f32[128,2]{0,1:T(2,128)} %param.20) | copy-start | bytes 3076
  295.4 62.0 %all-to-all-start.3 = ((bf16[64,1,6,2048]{3,2,1,0:T(8,128)(2,1)}), bf16[64,1,6,2048]{3,2,1,0:T(8,128)(2,1)}, u32[]{:S(2)}, u32[]{:S(2)}) async-start(bf16[64,1,6,2048]{3,2,1,0:T(8,128)(2,1)} %copy.44), calls=%async_computation.3 | async-start | bytes 4194304 | tf_op jit(solution)/shard_map/all_to_all | solution.py:114
  362.3 9.3 %copy-start.1 = (bf16[512,2048]{1,0:T(8,128)(2,1)S(1)}, bf16[512,2048]{1,0:T(8,128)(2,1)}, u32[]{:S(2)}) copy-start(bf16[512,2048]{1,0:T(8,128)(2,1)} %param.17) | copy-start | bytes 6291460
Sparse Core Ops, SparseCore 0:
  123.8 62.5 all-gather.1
where the time goes:
time: 379 us; the launch traced here: 378 us
  waiting for transfers between devices  137 us (36%)
  blocking collectives  137 us (36%)
  local copies, waits for them, and re-layouts  40.9 us (11%)
  starting transfers between devices  20.7 us (5%)
  matrix products  14.3 us (4%)
  other arithmetic  14.2 us (4%)
  between operations  13.7 us (4%)
    all_to_all x1, blocking collectives, sum_at_owner(): lax.all_to_all(cut_along(value, dim, length), axis, 0, 0, tiled=True)  74.6 us
    all_to_all x1, blocking collectives, per_device(): lax.all_to_all(dispatch, 'sp', split_axis=0, concat_axis=0, tiled=True)  62.8 us
    all_gather x1, waiting for transfers between devices, per_device(): arrived = lax.all_gather(arrived, 'tp', axis=1, tiled=True)  62.7 us
    all_to_all x1, waiting for transfers between devices, per_device(): lax.all_to_all(summed, 'sp', split_axis=0, concat_axis=0, tiled=True)  50.8 us
    all_to_all x1, waiting for transfers between devices, sum_at_owner(): lax.all_to_all(cut_along(value, dim, length), axis, 0, 0, tiled=True)  23.3 us
    reshape x1, local copies, waits for them, and re-layouts, per_device(): stacked = arrived.reshape(-1, model_width)  11.1 us
    all_to_all x1, starting transfers between devices, per_device(): lax.all_to_all(summed, 'sp', split_axis=0, concat_axis=0, tiled=True)  10.9 us
    all_gather x1, local copies, waits for them, and re-layouts, per_device(): arrived = lax.all_gather(arrived, 'tp', axis=1, tiled=True)  9.61 us
  transfers between devices with their start and end apart: 5, of which 4 were waited for; matrix products, arithmetic and copies ran while one was open for 1% of the time, Pallas kernels for 0%

commit v1 on v0

--- a/solution.py
+++ b/solution.py
@@ -98,23 +98,26 @@
     ).astype(jnp.bfloat16)
     own_routes = lax.dynamic_slice_in_dim(routes, lax.axis_index("tp") * quarter, quarter, 0)
     own_slots, own_sources, own_filled = slot_table(own_routes, expert_count, capacity, top_count)
-    token_index = own_sources.reshape(expert_count, 1, capacity)
-    filled_slots = own_filled.reshape(expert_count, 1, capacity)
-    dispatch = jnp.where(filled_slots[..., None], normed[token_index], jnp.zeros((), jnp.bfloat16))
+    token_index = own_sources.reshape(expert_count, capacity)
+    lanes = 128
+    rows3 = normed.reshape(quarter, model_width // lanes, lanes)
+    dispatch = rows3[token_index]
     arrived = lax.all_to_all(dispatch, "sp", split_axis=0, concat_axis=0, tiled=True)
-    arrived = lax.all_gather(arrived, "tp", axis=1, tiled=True)
     stacked = arrived.reshape(-1, model_width)
-    gate_pre = jnp.dot(stacked, expert_gate[0], preferred_element_type=jnp.float32)
-    up_pre = jnp.dot(stacked, expert_up[0], preferred_element_type=jnp.float32)
-    hidden = (jax.nn.silu(gate_pre) * up_pre).astype(jnp.bfloat16)
-    partial_out = jnp.dot(hidden, expert_down[0], preferred_element_type=jnp.float32).reshape(
-        arrived.shape
-    )
-    summed = sum_at_owner(partial_out.astype(jnp.bfloat16), "tp", 1).astype(jnp.bfloat16)
-    returned = lax.all_to_all(summed, "sp", split_axis=0, concat_axis=0, tiled=True)
-    outputs = returned.reshape(expert_count * capacity, model_width)
-    picked = outputs[own_slots].astype(jnp.float32).reshape(quarter, top_count, model_width)
-    combined = jnp.sum(route_weight[:, :, None] * picked, axis=1)
+    gates = lax.all_gather(expert_gate[0], "tp", axis=0, tiled=False)
+    ups = lax.all_gather(expert_up[0], "tp", axis=0, tiled=False)
+    downs = lax.all_gather(expert_down[0], "tp", axis=0, tiled=False)
+    summed = jnp.zeros(stacked.shape, jnp.float32)
+    for part in range(tp_count):
+        gate_pre = jnp.dot(stacked, gates[part], preferred_element_type=jnp.float32)
+        up_pre = jnp.dot(stacked, ups[part], preferred_element_type=jnp.float32)
+        hidden = (jax.nn.silu(gate_pre) * up_pre).astype(jnp.bfloat16)
+        summed = summed + jnp.dot(hidden, downs[part], preferred_element_type=jnp.float32)
+    expert_out = summed.astype(jnp.bfloat16).reshape(arrived.shape)
+    returned = lax.all_to_all(expert_out, "sp", split_axis=0, concat_axis=0, tiled=True)
+    outputs = returned.reshape(expert_count * capacity, model_width // lanes, lanes)
+    picked = outputs[own_slots].astype(jnp.float32).reshape(quarter, top_count, model_width // lanes, lanes)
+    combined = jnp.sum(route_weight[:, :, None, None] * picked, axis=1).reshape(quarter, model_width)
     return (mixed_up + combined).astype(jnp.bfloat16)
 
 

time: 379 us -> 282 us (0.74)
  blocking collectives: 137 us -> 52.9 us
  local copies, waits for them, and re-layouts: 40.9 us -> 10.7 us
  matrix products: 14.3 us -> 36 us
  other arithmetic: 14.2 us -> 8.51 us
    all_to_all x1 -> x0, blocking collectives: 74.6 us -> none  [sum_at_owner(): lax.all_to_all(cut_along(value, dim, length), axis, 0, 0, tiled=True)]
    dot_general x3 -> x8, matrix products: 8.89 us -> 31.5 us  [the longest x4 24.5 us: per_device(): jnp.dot(hidden, downs[part], preferred_element_type=jnp.float32)]
    all_to_all x1, waiting for transfers between devices: 23.3 us -> 45.6 us  [sum_at_owner(): lax.all_to_all(cut_along(value, dim, length), axis, 0, 0, tiled=True)]
    reshape x2 -> x0, local copies, waits for them, and re-layouts: 13.7 us -> none  [the longest x1 11.1 us: per_device(): stacked = arrived.reshape(-1, model_width)]
    all_gather x1 -> x3, waiting for transfers between devices: 62.7 us -> 51 us  [the longest x1 51 us: per_device(): downs = lax.all_gather(expert_down[0], 'tp', axis=0, tiled=False)]
    all_to_all x1, waiting for transfers between devices: 50.8 us -> 39.5 us  [per_device(): lax.all_to_all(expert_out, 'sp', split_axis=0, concat_axis=0, tiled=True)]
    all_to_all x1, blocking collectives: 62.8 us -> 52.9 us  [per_device(): lax.all_to_all(dispatch, 'sp', split_axis=0, concat_axis=0, tiled=True)]
    all_gather x1 -> x0, local copies, waits for them, and re-layouts: 9.61 us -> none  [per_device(): arrived = lax.all_gather(arrived, 'tp', axis=1, tiled=True)]
  transfers between devices with their start and end apart: 5 -> 7, of which waited for: 4 -> 4; matrix products, arithmetic and copies ran while one was open for 1% -> 7% of each run, Pallas kernels for 0% -> 0%
where the time goes in v1:
time: 282 us
  waiting for transfers between devices  139 us (49%)
  blocking collectives  52.9 us (19%)
  matrix products  36 us (13%)
  starting transfers between devices  20.8 us (7%)
  between operations  13.4 us (5%)
  local copies, waits for them, and re-layouts  10.7 us (4%)
  other arithmetic  8.51 us (3%)
    all_to_all x1, blocking collectives, per_device(): lax.all_to_all(dispatch, 'sp', split_axis=0, concat_axis=0, tiled=True)  52.9 us
    all_gather x1, waiting for transfers between devices, per_device(): downs = lax.all_gather(expert_down[0], 'tp', axis=0, tiled=False)  51 us
    all_to_all x1, waiting for transfers between devices, sum_at_owner(): lax.all_to_all(cut_along(value, dim, length), axis, 0, 0, tiled=True)  45.6 us
    all_to_all x1, waiting for transfers between devices, per_device(): lax.all_to_all(expert_out, 'sp', split_axis=0, concat_axis=0, tiled=True)  39.5 us
    dot_general x4, matrix products, per_device(): jnp.dot(hidden, downs[part], preferred_element_type=jnp.float32)  24.5 us
    all_to_all x1, starting transfers between devices, per_device(): lax.all_to_all(expert_out, 'sp', split_axis=0, concat_axis=0, tiled=True)  10.8 us
    dot_general x4, matrix products, per_device(): gate_pre = jnp.dot(stacked, gates[part], preferred_element_type=jnp.float32)  7.01 us
  transfers between devices with their start and end apart: 7, of which 4 were waited for; matrix products, arithmetic and copies ran while one was open for 7% of the time, Pallas kernels for 0%

profile of v1, /device:TPU:2, one launch (start us, length us, event | category | flops | bytes accessed | tf_op | source)
XLA Modules:
  0.0 281.7 jit_solution(1760337872202226005)
XLA Ops:
  6.5 0.0 copy-start
  6.5 0.0 copy-start.2
  6.5 0.0 all-gather.4.cloned.1.call-start
  6.6 0.7 all-gather.4.cloned.1.call-update
  7.3 0.0 all-gather.6.cloned.1.call-start
  7.3 0.7 all-gather.6.cloned.1.call-update
  8.0 0.0 copy-done.4
  8.1 0.1 slice.144
  8.1 1.9 collective-permute-start.1
  10.0 0.0 copy-done.2
  10.1 3.5 %collective-permute-start = (bf16[15,256]{1,0:T(8,128)(2,1)S(1)}, bf16[15,256]{1,0:T(8,128)(2,1)S(1)}, u32[]{:S(2)}, u32[]{:S(2)}) collective-permute-start(bf16[15,256]{1,0:T(8,128)(2,1)S(1)} %slice.142), channel_id=1, source_target_pairs={{0,4},{4,8},{8,12},{12,16},{16,20},{20,24},{24,28},{28,32},{32,36}... | collective-permute-start | bytes 23048 | tf_op jit(solution)/shard_map/ppermute | solution.py:15
  13.6 0.0 collective-permute-done.1
  13.6 0.1 pad_maximum_fusion
  13.7 0.1 convert_add_fusion.1
  13.8 1.2 collective-permute-done
  15.0 0.1 maximum_convert_fusion
  15.1 0.0 copy-done
  15.1 0.0 copy-done.8
  15.1 0.0 copy-done.7
  15.1 4.4 %convolution_convert_fusion = bf16[512,2048]{1,0:T(8,128)(2,1)} fusion(bf16[512,2048]{1,0:T(8,128)(2,1)S(1)} %copy-done, f32[512]{0:T(512)S(1)} %copy-done.8, bf16[512,256]{1,0:T(8,128)(2,1)S(1)} %copy-done.2, f32[527,256]{1,0:T(8,128)S(1)} %maximum_convert_fusion, bf16[1,256,512]{2,1,0:T(8,128)(2,1)S(1)} %copy-done.7, f32[512]{0:T(512)S(1)} %get-tuple-element.9, ...), kind=kOutput, calls=%fused_computation.4 | convolution fusion | flops 1214119936 | bytes 13119488 | tf_op jit(solution)/shard_map/dot_general | solution.py:90
  19.5 4.5 %all-to-all-start = ((bf16[4,128,2048]{2,1,0:T(8,128)(2,1)}), bf16[4,128,2048]{2,1,0:T(8,128)(2,1)}, u32[]{:S(2)}, u32[]{:S(2)}) async-start(bf16[4,128,2048]{2,1,0:T(8,128)(2,1)} %bitcast.140), calls=%async_computation | async-start | bytes 4194304 | tf_op jit(solution)/shard_map/all_to_all | solution.py:25
  24.0 0.0 all-gather.8.cloned.1.call-start
  24.1 0.7 all-gather.8.cloned.1.call-update
  24.8 0.7 broadcast_multiply_fusion
  25.5 0.1 copy.25
  25.6 0.1 eq.103
  25.7 0.1 reshape.189
  25.9 0.6 reduce-window.6
  26.5 0.2 slice_reduce_fusion
  26.7 0.1 fusion.156
  26.8 0.2 select_reduce_fusion
  27.0 0.1 reduce_sum.53
  27.2 0.1 reshape.198
  27.3 0.0 copy-start.3
  27.3 45.6 %all-to-all-done = bf16[4,128,2048]{2,1,0:T(8,128)(2,1)} async-done(((bf16[4,128,2048]{2,1,0:T(8,128)(2,1)}), bf16[4,128,2048]{2,1,0:T(8,128)(2,1)}, u32[]{:S(2)}, u32[]{:S(2)}) %all-to-all-start) | async-done | bytes 2097184 | tf_op jit(solution)/shard_map/all_to_all | solution.py:25
  73.0 2.1 convert_reduce_fusion
  75.1 1.3 fusion.52
  76.4 0.0 copy-done.3
  76.4 0.2 fusion.58
  76.6 0.1 copy.30
  76.8 2.6 gather_fusion
  79.4 52.9 %all_to_all.15 = bf16[64,6,16,128]{3,2,1,0:T(8,128)(2,1)} all-to-all(bf16[64,6,16,128]{3,2,1,0:T(8,128)(2,1)} %bitcast.138), channel_id=1, replica_groups=mesh['sp'=64,'tp'=4] {'sp'}, dimensions={0} | all-to-all | bytes 3145728 | tf_op jit(solution)/shard_map/all_to_all | solution.py:105
  132.2 2.4 fusion.3
  134.6 0.0 copy-done.1
  134.6 0.0 copy-start.6
  134.7 2.0 fusion.7
  136.6 0.5 copy-done.6
  137.2 1.3 fusion.11
  138.5 1.3 fusion.15
  139.8 51.0 %all-gather.8.cloned.1.call-done = bf16[4,256,2048]{2,1,0:T(8,128)(2,1)} async-done(((bf16[1,256,2048]{2,1,0:T(8,128)(2,1)}), bf16[4,256,2048]{2,1,0:T(8,128)(2,1)}) %all-gather.8.cloned.1.call-update) | async-done | bytes 4194320 | tf_op jit(solution)/shard_map/all_gather | solution.py:109
  190.8 5.7 %fusion.44 = f32[384,2048]{1,0:T(8,128)} fusion(bf16[4,256,2048]{2,1,0:T(8,128)(2,1)} %all-gather.8.cloned.1.call-done, bf16[4,2048,256]{2,1,0:T(8,128)(2,1)} %all-gather.6.cloned.1.call-done, f32[384,256]{1,0:T(8,128)} %fusion.15, bf16[48,8,16,128]{3,2,1,0:T(8,128)(2,1)} %bitcast.130), kind=kOutput, calls=%fused_computation.37 | convolution fusion | flops 805896192 | bytes 7208960 | tf_op jit(solution)/shard_map/dot_general | solution.py:115
  196.5 5.7 %fusion.47 = f32[384,2048]{1,0:T(8,128)} fusion(bf16[4,256,2048]{2,1,0:T(8,128)(2,1)} %all-gather.8.cloned.1.call-done, bf16[4,2048,256]{2,1,0:T(8,128)(2,1)} %all-gather.6.cloned.1.call-done, f32[384,256]{1,0:T(8,128)} %fusion.11, bf16[48,8,16,128]{3,2,1,0:T(8,128)(2,1)} %bitcast.131), kind=kOutput, calls=%fused_computation.38 | convolution fusion | flops 805896192 | bytes 7208960 | tf_op jit(solution)/shard_map/dot_general | solution.py:115
  202.1 5.4 %fusion.50 = f32[384,2048]{1,0:T(8,128)} fusion(bf16[4,256,2048]{2,1,0:T(8,128)(2,1)} %all-gather.8.cloned.1.call-done, bf16[4,2048,256]{2,1,0:T(8,128)(2,1)} %all-gather.6.cloned.1.call-done, f32[384,256]{1,0:T(8,128)S(1)} %fusion.7, bf16[48,8,16,128]{3,2,1,0:T(8,128)(2,1)} %bitcast.132), kind=kOutput, calls=%fused_computation.39 | convolution fusion | flops 805896192 | bytes 7208960 | tf_op jit(solution)/shard_map/dot_general | solution.py:115
  207.6 7.8 %fusion.17 = bf16[48,8,16,128]{3,1,2,0:T(8,128)(2,1)} fusion(f32[384,2048]{1,0:T(8,128)} %fusion.50, f32[384,2048]{1,0:T(8,128)} %fusion.44, f32[384,2048]{1,0:T(8,128)} %fusion.47, bf16[4,256,2048]{2,1,0:T(8,128)(2,1)} %all-gather.8.cloned.1.call-done, bf16[4,2048,256]{2,1,0:T(8,128)(2,1)} %all-gather.6.cloned.1.call-done, f32[384,256]{1,0:T(8,128)S(1)} %fusion.3, ...), kind=kOutput, calls=%fused_computation.26 | convolution fusion | flops 809041920 | bytes 15073280 | tf_op jit(solution)/shard_map/dot_general | solution.py:115
  215.3 3.0 %copy.32 = bf16[48,8,16,128]{3,2,1,0:T(8,128)(2,1)} copy(bf16[48,8,16,128]{3,1,2,0:T(8,128)(2,1)} %fusion.17) | data formatting | bytes 3145728
  218.3 10.8 %all-to-all-start.2 = ((bf16[64,6,16,128]{3,2,1,0:T(8,128)(2,1)}), bf16[64,6,16,128]{3,2,1,0:T(8,128)(2,1)}, u32[]{:S(2)}, u32[]{:S(2)}) async-start(bf16[64,6,16,128]{3,2,1,0:T(8,128)(2,1)} %bitcast.137), calls=%async_computation.2 | async-start | bytes 3145728 | tf_op jit(solution)/shard_map/all_to_all | solution.py:117
  229.2 0.1 copy.28
  229.3 0.1 mul.116
  229.4 0.0 copy-done.5
  229.4 0.1 copy.24
  229.6 39.5 %all-to-all-done.2 = bf16[64,6,16,128]{3,2,1,0:T(8,128)(2,1)} async-done(((bf16[64,6,16,128]{3,2,1,0:T(8,128)(2,1)}), bf16[64,6,16,128]{3,2,1,0:T(8,128)(2,1)}, u32[]{:S(2)}, u32[]{:S(2)}) %all-to-all-start.2) | async-done | bytes 1572896 | tf_op jit(solution)/shard_map/all_to_all | solution.py:117
  269.1 3.1 %gather_fusion.1 = bf16[256,16,128]{2,1,0:T(8,128)(2,1)} fusion(bf16[384,16,128]{2,1,0:T(8,128)(2,1)} %bitcast.16, s32[1024]{0:T(1024)S(1)} %pad_clamp_fusion), kind=kCustom, calls=%fused_computation.1 | custom fusion | bytes 2098176 | tf_op jit(solution)/shard_map/gather | solution.py:119
  272.3 1.8 fusion
  274.0 1.2 fusion.55
  (19 shorter events, 0.1 us)
Async XLA Ops:
  6.5 8.6 %copy-start = (bf16[512,2048]{1,0:T(8,128)(2,1)S(1)}, bf16[512,2048]{1,0:T(8,128)(2,1)}, u32[]{:S(2)}) copy-start(bf16[512,2048]{1,0:T(8,128)(2,1)} %param.17) | copy-start | bytes 6291460
  6.5 1.5 copy-start.4
  6.5 3.5 %copy-start.2 = (bf16[512,256]{1,0:T(8,128)(2,1)S(1)}, bf16[512,256]{1,0:T(8,128)(2,1)}, u32[]{:S(2)}) copy-start(bf16[512,256]{1,0:T(8,128)(2,1)} %param.13) | copy-start | bytes 786436
  6.5 8.6 %copy-start.8 = (f32[512]{0:T(512)S(1)}, f32[512]{0:T(512)}, u32[]{:S(2)}) copy-start(f32[512]{0:T(512)} %param.16) | copy-start | bytes 6148
  6.5 8.6 %copy-start.7 = (bf16[1,256,512]{2,1,0:T(8,128)(2,1)S(1)}, bf16[1,256,512]{2,1,0:T(8,128)(2,1)}, u32[]{:S(2)}) copy-start(bf16[1,256,512]{2,1,0:T(8,128)(2,1)} %param.15) | copy-start | bytes 786436
  6.5 125.7 %all-gather.4.cloned.1.call-start = ((), (), s32[]{:S(2)}) async-start(), calls=%async_computation.3 | async-start | bytes 5242880 | tf_op jit(solution)/shard_map/all_gather | solution.py:107
  7.3 132.5 %all-gather.6.cloned.1.call-start = ((), (), s32[]{:S(2)}) async-start(), calls=%async_computation.4 | async-start | bytes 5242880 | tf_op jit(solution)/shard_map/all_gather | solution.py:108
  8.1 5.5 %collective-permute-start.1 = (bf16[15]{0:T(256)(128)(2,1)S(1)}, bf16[15]{0:T(256)(128)(2,1)S(1)}, u32[]{:S(2)}, u32[]{:S(2)}) collective-permute-start(bf16[15]{0:T(256)(128)(2,1)S(1)} %slice.144), channel_id=1, source_target_pairs={{0,4},{4,8},{8,12},{12,16},{16,20},{20,24},{24,28},{28,32},{32,36}... | collective-permute-start | bytes 98 | tf_op jit(solution)/shard_map/ppermute | solution.py:15
  10.1 5.0 %collective-permute-start = (bf16[15,256]{1,0:T(8,128)(2,1)S(1)}, bf16[15,256]{1,0:T(8,128)(2,1)S(1)}, u32[]{:S(2)}, u32[]{:S(2)}) collective-permute-start(bf16[15,256]{1,0:T(8,128)(2,1)S(1)} %slice.142), channel_id=1, source_target_pairs={{0,4},{4,8},{8,12},{12,16},{16,20},{20,24},{24,28},{28,32},{32,36}... | collective-permute-start | bytes 23048 | tf_op jit(solution)/shard_map/ppermute | solution.py:15
  19.5 53.4 %all-to-all-start = ((bf16[4,128,2048]{2,1,0:T(8,128)(2,1)}), bf16[4,128,2048]{2,1,0:T(8,128)(2,1)}, u32[]{:S(2)}, u32[]{:S(2)}) async-start(bf16[4,128,2048]{2,1,0:T(8,128)(2,1)} %bitcast.140), calls=%async_computation | async-start | bytes 4194304 | tf_op jit(solution)/shard_map/all_to_all | solution.py:25
  24.0 166.8 %all-gather.8.cloned.1.call-start = ((), (), s32[]{:S(2)}) async-start(), calls=%async_computation.5 | async-start | bytes 5242880 | tf_op jit(solution)/shard_map/all_gather | solution.py:109
  27.3 49.1 %copy-start.3 = (f32[2048]{0:T(1024)S(1)}, f32[2048]{0:T(1024)}, u32[]{:S(2)}) copy-start(f32[2048]{0:T(1024)} %param.18) | copy-start | bytes 24580
  132.2 2.4 copy-start.1
  134.6 2.5 copy-start.6
  218.3 11.1 %copy-start.5 = (f32[128,2]{0,1:T(2,128)S(1)}, f32[128,2]{0,1:T(2,128)}, u32[]{:S(2)}) copy-start(f32[128,2]{0,1:T(2,128)} %param.20) | copy-start | bytes 3076
  218.3 50.8 %all-to-all-start.2 = ((bf16[64,6,16,128]{3,2,1,0:T(8,128)(2,1)}), bf16[64,6,16,128]{3,2,1,0:T(8,128)(2,1)}, u32[]{:S(2)}, u32[]{:S(2)}) async-start(bf16[64,6,16,128]{3,2,1,0:T(8,128)(2,1)} %bitcast.137), calls=%async_computation.2 | async-start | bytes 3145728 | tf_op jit(solution)/shard_map/all_to_all | solution.py:117
Sparse Core Ops, SparseCore 0:
  9.2 75.0 all-gather.3
  86.1 51.7 all-gather.5
  139.7 51.1 all-gather.7

commit v2 on v0

v2 whole, which is shorter than its diff:
```python
import functools

import jax
import jax.numpy as jnp
from jax import lax
from jax.experimental import pallas as pl
from jax.experimental.pallas import tpu as pltpu
from jax.sharding import Mesh, PartitionSpec as P

SPAN = 16
EPS = 1e-06
LANES = 128


VMEM = pl.BlockSpec(memory_space=pltpu.VMEM)
SMEM = pl.BlockSpec(memory_space=pltpu.SMEM)
HBM = pl.BlockSpec(memory_space=pltpu.HBM)


def dispatch_kernel(rows, width, slots, tok_ref, parts_ref, stream_ref, gain_ref, out_ref, mixed_ref, wide, tiles):
    chunks = width // LANES
    total = stream_ref[...].astype(jnp.float32)
    own = parts_ref[0].astype(jnp.float32)
    for part in range(1, parts_ref.shape[0]):
        own = own + parts_ref[part].astype(jnp.float32)
    mixed = (total + own).astype(jnp.bfloat16)
    mixed_ref[...] = mixed
    up = mixed.astype(jnp.float32)
    scale = lax.rsqrt(jnp.sum(up * up, axis=1, keepdims=True) * (1.0 / width) + EPS)
    for chunk in range(chunks):
        cols = slice(chunk * LANES, (chunk + 1) * LANES)
        piece = up[:, cols] * scale * gain_ref[:, cols]
        wide[pl.ds(chunk, rows, stride=chunks), :] = piece
    tiles[...] = wide[...].astype(jnp.bfloat16).reshape(rows, chunks, LANES)

    @pl.loop(0, slots, unroll=8)
    def _(slot):
        out_ref[slot] = tiles[tok_ref[slot]]


def hidden_kernel(rows, width, ff, half, x_ref, *refs):
    w_refs = refs[:10]
    out_ref, wide, flat = refs[10:]
    chunks = width // LANES
    is_home = half()
    wide[...] = x_ref[...].astype(jnp.float32)
    for chunk in range(chunks):
        flat[:, chunk * LANES : (chunk + 1) * LANES] = wide[pl.ds(chunk, rows, stride=chunks), :].astype(jnp.bfloat16)

    def fill(place, gate_ref, up_ref):
        gate_pre = jnp.dot(flat[...], gate_ref[...], preferred_element_type=jnp.float32)
        up_pre = jnp.dot(flat[...], up_ref[...], preferred_element_type=jnp.float32)
        hidden = gate_pre / (1.0 + jnp.exp(-gate_pre)) * up_pre
        out_ref[:, place * ff : (place + 1) * ff] = hidden.astype(jnp.bfloat16)

    @pl.when(is_home == 1)
    def _():
        fill(0, w_refs[0], w_refs[1])

    @pl.when(is_home == 0)
    def _():
        fill(0, w_refs[2], w_refs[3])

    for place in range(1, 4):
        fill(place, w_refs[2 + 2 * place], w_refs[3 + 2 * place])


def down_kernel(rows, width, ff, half, hidden_ref, *refs):
    own_ref, late_ref = refs[:2]
    w_refs = refs[2:5]
    out_ref, wide, first = refs[5:]
    chunks = width // LANES
    is_home = half()

    @pl.when(is_home == 1)
    def _():
        first[...] = own_ref[...]

    @pl.when(is_home == 0)
    def _():
        first[...] = late_ref[...]

    step = 2 * LANES
    for begin in range(0, width, step):
        cols = slice(begin, begin + step)
        total = jnp.dot(hidden_ref[:, :ff], first[:, cols], preferred_element_type=jnp.float32)
        for place in range(1, 4):
            total = total + jnp.dot(
                hidden_ref[:, place * ff : (place + 1) * ff],
                w_refs[place - 1][:, cols],
                preferred_element_type=jnp.float32,
            )
        for piece in range(2):
            wide[pl.ds(begin // LANES + piece, rows, stride=chunks), :] = total[:, piece * LANES : (piece + 1) * LANES]
    out_ref[...] = wide[...].astype(jnp.bfloat16)


def combine_kernel(rows, width, top, pos_ref, weight_ref, got_ref, mixed_ref, out_ref, wide):
    chunks = width // LANES

    @pl.loop(0, rows, unroll=4)
    def _(row):
        total = weight_ref[row * top] * got_ref[pos_ref[row * top]].astype(jnp.float32)
        for k in range(1, top):
            total = total + weight_ref[row * top + k] * got_ref[pos_ref[row * top + k]].astype(jnp.float32)
        wide[pl.ds(row * chunks, chunks), :] = total

    for chunk in range(chunks):
        cols = slice(chunk * LANES, (chunk + 1) * LANES)
        piece = wide[pl.ds(chunk, rows, stride=chunks), :]
        out_ref[:, cols] = (mixed_ref[:, cols].astype(jnp.float32) + piece).astype(jnp.bfloat16)


def slot_tables(route_block, expert_count, capacity, top_count):
    flattened = route_block.reshape(-1)
    one_hot = (flattened[:, None] == jnp.arange(expert_count, dtype=jnp.int32)[None, :]).astype(jnp.int32)
    ranking = jnp.sum((jnp.cumsum(one_hot, axis=0) - one_hot) * one_hot, axis=1)
    side = capacity // 2
    place = ((flattened // 2 * 2 + ranking // side) * 2 + flattened % 2) * side + ranking % side
    matches = place[None, :] == jnp.arange(expert_count * capacity, dtype=jnp.int32)[:, None]
    sources = jnp.sum(jnp.where(matches, jnp.arange(flattened.shape[0], dtype=jnp.int32)[None, :], 0), axis=1)
    return place, sources // top_count


def weight_moves(sp_count, tp_count):
    def at(pair, core, y):
        return (2 * pair + core) * tp_count + y % tp_count

    pairs = [(pair, y) for pair in range(sp_count // 2) for y in range(tp_count)]
    home = lambda p, y: at(p, y % 2, y)
    away = lambda p, y: at(p, 1 - y % 2, y)
    over = [(home(p, y), away(p, y)) for p, y in pairs]
    back = [(away(p, y), home(p, y)) for p, y in pairs]
    plus = [(away(p, y), home(p, y + 1)) for p, y in pairs]
    minus = [(away(p, y), home(p, y - 1)) for p, y in pairs]
    far = [(home(p, y), away(p, y + 2)) for p, y in pairs]
    return plus + far, over + back, minus + over, over


ALL = ("sp", "yh", "yl")
TP = ("yh", "yl")


def forward(
    stream,
    pool_in,
    doc_ids,
    pool_map,
    pool_scale,
    out_weight,
    norm_gain,
    routes,
    route_weight,
    expert_gate,
    expert_up,
    expert_down,
):
    row_count = pool_in.shape[0]
    model_width = stream.shape[1]
    top_count = routes.shape[1]
    tp_count = lax.axis_size(TP)
    expert_count = lax.axis_size("sp")
    quarter = row_count // tp_count
    capacity = max(2, 3 * top_count * quarter // (2 * expert_count))
    slots = expert_count * capacity
    chunks = model_width // LANES
    reach_rows = SPAN - 1
    tp_index = lax.axis_index(TP)

    tail = jnp.concatenate(
        [
            pool_in[row_count - reach_rows :],
            jnp.pad(doc_ids[row_count - reach_rows :].astype(jnp.bfloat16), (0, pool_in.shape[1] - reach_rows))[None],
        ],
        axis=0,
    )
    prior = lax.ppermute(tail, "sp", [(i, i + 1) for i in range(expert_count - 1)])
    prior_rows, prior_docs = prior[:reach_rows], prior[reach_rows, :reach_rows]
    extended = jnp.concatenate([prior_rows, pool_in], axis=0).astype(jnp.float32)
    extended_docs = jnp.concatenate([prior_docs.astype(jnp.float32), doc_ids.astype(jnp.float32)])
    own_docs = doc_ids.astype(jnp.float32)
    window = jnp.left_shift(jnp.int32(2), tp_index)
    positions = lax.axis_index("sp") * row_count + jnp.arange(row_count, dtype=jnp.int32)
    running = jnp.zeros(pool_in.shape, jnp.float32)
    counts = jnp.zeros((row_count,), jnp.float32)
    for offset in range(reach_rows + 1):
        begin_row = reach_rows - offset
        piece_rows = extended[begin_row : begin_row + row_count]
        piece_docs = extended_docs[begin_row : begin_row + row_count]
        in_window = (offset < window) & (positions - offset >= 0) & (piece_docs == own_docs)
        running = running + jnp.where(in_window[:, None], piece_rows, 0.0)
        counts = counts + in_window.astype(jnp.float32)
    pooled = (running / counts[:, None] - pool_in.astype(jnp.float32)).astype(jnp.bfloat16)
    branch = (jnp.dot(pooled, pool_map[0], preferred_element_type=jnp.float32) * pool_scale).astype(jnp.bfloat16)
    partial = jnp.dot(branch, out_weight, preferred_element_type=jnp.float32).astype(jnp.bfloat16)
    partial = partial.reshape(tp_count, quarter, model_width)

    own = (expert_gate[0], expert_up[0], expert_down[0])
    ahead, swap, behind, over = weight_moves(expert_count, tp_count)
    parts = lax.all_to_all(partial, TP, 0, 0, tiled=True)
    held = []
    for array in own:
        first = lax.ppermute(array, ALL, ahead)
        second = lax.ppermute(array, ALL, behind)
        third = lax.ppermute(first, ALL, swap)
        fourth = lax.ppermute(second, ALL, over)
        held.append((array, fourth, second, first, third))

    own_routes = lax.dynamic_slice_in_dim(routes, tp_index * quarter, quarter, 0)
    places, tokens = slot_tables(own_routes, expert_count, capacity, top_count)

    dispatch, mixed_rows = pl.pallas_call(
        functools.partial(dispatch_kernel, quarter, model_width, slots),
        out_shape=(
            jax.ShapeDtypeStruct((slots, chunks, LANES), jnp.bfloat16),
            jax.ShapeDtypeStruct((quarter, model_width), jnp.bfloat16),
        ),
        in_specs=[SMEM, VMEM, VMEM, VMEM],
        out_specs=(VMEM, VMEM),
        scratch_shapes=[
            pltpu.VMEM((quarter * chunks, LANES), jnp.float32),
            pltpu.VMEM((quarter, chunks, LANES), jnp.bfloat16),
        ],
        name="dispatch",
    )(tokens, parts, stream, norm_gain[None])

    groups = expert_count * 2
    send = dispatch.reshape(groups, capacity // 2, chunks, LANES)
    arrived = lax.all_to_all(send, ("sp", "yl"), 0, 0, tiled=True)

    ff = expert_gate.shape[2]
    is_home = lambda: (lax.axis_index("sp") % 2 == lax.axis_index("yl")).astype(jnp.int32)
    hidden = pl.pallas_call(
        functools.partial(hidden_kernel, slots, model_width, ff, is_home),
        out_shape=jax.ShapeDtypeStruct((slots, ff * tp_count), jnp.bfloat16),
        in_specs=[VMEM] * 11,
        out_specs=VMEM,
        scratch_shapes=[
            pltpu.VMEM((slots * chunks, LANES), jnp.float32),
            pltpu.VMEM((slots, model_width), jnp.bfloat16),
        ],
        name="hidden",
    )(arrived.reshape(slots * chunks, LANES), *[h[i] for i in range(5) for h in held[:2]])
    expert_rows = pl.pallas_call(
        functools.partial(down_kernel, slots, model_width, ff, is_home),
        out_shape=jax.ShapeDtypeStruct((slots * chunks, LANES), jnp.bfloat16),
        in_specs=[VMEM] * 6,
        out_specs=VMEM,
        scratch_shapes=[
            pltpu.VMEM((slots * chunks, LANES), jnp.float32),
            pltpu.VMEM((ff, model_width), jnp.bfloat16),
        ],
        name="down",
    )(hidden, *held[2])

    returned = lax.all_to_all(
        expert_rows.reshape(groups, capacity // 2, chunks, LANES), ("sp", "yl"), 0, 0, tiled=True
    )
    return pl.pallas_call(
        functools.partial(combine_kernel, quarter, model_width, top_count),
        out_shape=jax.ShapeDtypeStruct((quarter, model_width), jnp.bfloat16),
        in_specs=[SMEM, SMEM, VMEM, VMEM],
        out_specs=VMEM,
        scratch_shapes=[pltpu.VMEM((quarter * chunks, LANES), jnp.float32)],
        name="combine",
    )(places, route_weight.reshape(-1), returned.reshape(slots, chunks, LANES), mixed_rows)


def solution(mesh):
    split = Mesh(mesh.devices.reshape(mesh.shape["sp"], mesh.shape["tp"] // 2, 2), ALL)
    in_specs = (
        P(ALL, None),
        P("sp", TP),
        P("sp"),
        P(TP, None, None),
        P(TP),
        P(TP, None),
        P(),
        P("sp", None),
        P(ALL, None),
        P("sp", None, TP),
        P("sp", None, TP),
        P("sp", TP, None),
    )
    return jax.shard_map(forward, mesh=split, in_specs=in_specs, out_specs=P(ALL, None), check_vma=False)
```

time: 379 us -> 228 us (0.60)
  blocking collectives: 137 us -> 0 us
  local copies, waits for them, and re-layouts: 40.9 us -> 4.88 us
  starting transfers between devices: 20.7 us -> 52 us
  Pallas kernels: 0 us -> 25 us
  between operations: 13.7 us -> 0.22 us
  other arithmetic: 14.2 us -> 4.26 us
  matrix products: 14.3 us -> 5.32 us
    all_to_all x2 -> x0, blocking collectives: 137 us -> none  [the longest x1 74.6 us: sum_at_owner(): lax.all_to_all(cut_along(value, dim, length), axis, 0, 0, tiled=True)]
    ppermute x2 -> x13, waiting for transfers between devices: 0.54 us -> 74.9 us  [the longest x3 71.9 us: forward(): first = lax.ppermute(array, ALL, ahead)]
    all_gather x1 -> x0, waiting for transfers between devices: 62.7 us -> none  [per_device(): arrived = lax.all_gather(arrived, 'tp', axis=1, tiled=True)]
    pallas_call x0 -> x4, Pallas kernels: none -> 25 us  [the longest x1 10.7 us: forward(): pl.pallas_call(functools.partial(hidden_kernel, slots, model_width, ff, i...]
    ppermute x2 -> x13, starting transfers between devices: 5.4 us -> 21.1 us  [the longest x3 9.42 us: forward(): fourth = lax.ppermute(second, ALL, over)]
    all_to_all x2 -> x3, starting transfers between devices: 15.3 us -> 30.9 us  [the longest x1 15.1 us: forward(): arrived = lax.all_to_all(send, ('sp', 'yl'), 0, 0, tiled=True)]
    all_to_all x2 -> x3, waiting for transfers between devices: 74 us -> 60.2 us  [the longest x1 39 us: forward(): lax.all_to_all(expert_rows.reshape(groups, capacity // 2, chunks, LANES),...]
    reshape x3 -> x2, local copies, waits for them, and re-layouts: 13.9 us -> 0.87 us  [the longest x1 0.73 us: forward(): route_weight.reshape(-1)]
  transfers between devices with their start and end apart: 5 -> 16, of which waited for: 4 -> 6; matrix products, arithmetic and copies ran while one was open for 1% -> 2% of each run, Pallas kernels for 0% -> 7%
where the time goes in v2:
time: 228 us; the launch traced here: 227 us
  waiting for transfers between devices  135 us (59%)
  starting transfers between devices  52 us (23%)
  Pallas kernels  25 us (11%)
  matrix products  5.32 us (2%)
  local copies, waits for them, and re-layouts  4.88 us (2%)
  other arithmetic  4.26 us (2%)
    ppermute x3, waiting for transfers between devices, forward(): first = lax.ppermute(array, ALL, ahead)  71.9 us
    all_to_all x1, waiting for transfers between devices, forward(): lax.all_to_all(expert_rows.reshape(groups, capacity // 2, chunks, LANES),...  39 us
    all_to_all x1, waiting for transfers between devices, forward(): parts = lax.all_to_all(partial, TP, 0, 0, tiled=True)  21.2 us
    all_to_all x1, starting transfers between devices, forward(): arrived = lax.all_to_all(send, ('sp', 'yl'), 0, 0, tiled=True)  15.1 us
    all_to_all x1, starting transfers between devices, forward(): lax.all_to_all(expert_rows.reshape(groups, capacity // 2, chunks, LANES),...  11.2 us
    pallas_call x1, Pallas kernels, forward(): pl.pallas_call(functools.partial(hidden_kernel, slots, model_width, ff, i...  10.7 us
    ppermute x3, starting transfers between devices, forward(): fourth = lax.ppermute(second, ALL, over)  9.42 us
    pallas_call x1, Pallas kernels, forward(): pl.pallas_call(functools.partial(down_kernel, slots, model_width, ff, is_...  6.45 us
  transfers between devices with their start and end apart: 16, of which 6 were waited for; matrix products, arithmetic and copies ran while one was open for 2% of the time, Pallas kernels for 7%

profile of v2, /device:TPU:2, one launch (start us, length us, event | category | flops | bytes accessed | tf_op | source)
XLA Modules:
  0.0 226.8 jit_solution(2775791612886333637)
XLA Ops:
  0.0 0.0 copy-start
  0.0 0.9 fusion.120
  0.9 0.1 slice.115
  0.9 0.7 slice.114
  1.7 1.9 collective-permute-start
  3.6 3.0 %collective-permute-done = bf16[16,256]{1,0:T(8,128)(2,1)S(1)} collective-permute-done((bf16[16,256]{1,0:T(8,128)(2,1)S(1)}, bf16[16,256]{1,0:T(8,128)(2,1)S(1)}, u32[]{:S(2)}, u32[]{:S(2)}) %collective-permute-start) | collective-permute-done | bytes 8224 | tf_op jit(solution)/shard_map/ppermute | solution.py:177
  6.6 1.0 maximum_convert_fusion
  7.6 0.1 pad_maximum_fusion.1
  7.7 0.8 convert_add_fusion
  8.5 0.0 copy-done
  8.5 5.3 %convolution_convert_fusion = bf16[512,2048]{1,0:T(8,128)(2,1)} fusion(bf16[512,2048]{1,0:T(8,128)(2,1)S(1)} %copy-done, f32[512]{0:T(512)} %param.16, bf16[512,256]{1,0:T(8,128)(2,1)} %param.13, f32[527,256]{1,0:T(8,128)S(1)} %maximum_convert_fusion, bf16[1,256,512]{2,1,0:T(8,128)(2,1)} %param.15, f32[512]{0:T(512)S(1)} %get-tuple-element.9, ...), kind=kOutput, calls=%fused_computation | convolution fusion | flops 1214119936 | bytes 13119488 | tf_op jit(solution)/shard_map/dot_general | solution.py:195
  13.8 4.6 %all-to-all-start = ((bf16[4,128,2048]{2,1,0:T(8,128)(2,1)}), bf16[4,128,2048]{2,1,0:T(8,128)(2,1)}, u32[]{:S(2)}, u32[]{:S(2)}) async-start(bf16[4,128,2048]{2,1,0:T(8,128)(2,1)} %bitcast.40), calls=%async_computation | async-start | bytes 4194304 | tf_op jit(solution)/shard_map/all_to_all | solution.py:200
  18.4 0.0 copy-done.1
  18.5 0.1 collective-permute-start.1
  18.6 2.0 collective-permute-start.3
  20.6 0.7 constant_dynamic-slice_fusion
  21.3 0.1 copy.17
  21.4 0.1 eq.90
  21.5 0.1 reshape.126
  21.7 0.6 reduce-window.6
  22.3 0.2 slice_reduce_fusion
  22.5 0.1 fusion.62
  22.7 0.0 copy-start.7
  22.7 0.1 select_reduce_fusion
  22.8 0.6 add_select_fusion.tok_ref
  23.4 21.2 %all-to-all-done.parts_ref = bf16[4,128,2048]{2,1,0:T(8,128)(2,1)} async-done(((bf16[4,128,2048]{2,1,0:T(8,128)(2,1)}), bf16[4,128,2048]{2,1,0:T(8,128)(2,1)}, u32[]{:S(2)}, u32[]{:S(2)}) %all-to-all-start) | async-done | bytes 2097184 | tf_op jit(solution)/shard_map/all_to_all | solution.py:200
  44.6 4.5 %dispatch.1 = (bf16[384,16,128]{2,1,0:T(8,128)(2,1)}, bf16[128,2048]{1,0:T(8,128)(2,1)}) custom-call(s32[384]{0:T(512)} %add_select_fusion.tok_ref, bf16[4,128,2048]{2,1,0:T(8,128)(2,1)} %all-to-all-done.parts_ref, bf16[128,2048]{1,0:T(8,128)(2,1)} %stream_ref.1, f32[1,2048]{1,0:T(1,128)} %bitcast.51), custom_call_target="tpu_custom_call" | custom-call | tf_op jit(solution)/shard_map/dispatch/pallas_call | solution.py:212
  49.1 0.0 copy-done.7
  49.1 15.1 %all-to-all-start.1 = ((bf16[128,3,16,128]{3,2,1,0:T(8,128)(2,1)}), bf16[128,3,16,128]{3,2,1,0:T(8,128)(2,1)}, u32[]{:S(2)}, u32[]{:S(2)}) async-start(bf16[128,3,16,128]{3,2,1,0:T(8,128)(2,1)} %bitcast.41), calls=%async_computation.1 | async-start | bytes 3145728 | tf_op jit(solution)/shard_map/all_to_all | solution.py:229
  64.3 1.0 collective-permute-start.5
  65.3 1.2 collective-permute-start.6
  66.5 0.0 collective-permute-start.9
  66.5 0.0 collective-permute-done.1.refs_4_
  66.5 3.5 %collective-permute-start.11 = (bf16[256,2048]{1,0:T(8,128)(2,1)}, bf16[256,2048]{1,0:T(8,128)(2,1)}, u32[]{:S(2)}, u32[]{:S(2)}) collective-permute-start(bf16[256,2048]{1,0:T(8,128)(2,1)} %bitcast.49), channel_id=1, source_target_pairs={{4,5},{1,2},{6,7},{3,0},{12,13},{9,10},{14,15},{11,8},{20,21},{17,... | collective-permute-start | bytes 3145736 | tf_op jit(solution)/shard_map/ppermute | solution.py:203
  70.0 0.0 collective-permute-done.3.refs_5_
  70.0 1.3 collective-permute-start.2
  71.4 32.6 %collective-permute-done.5.refs_6_ = bf16[2048,256]{1,0:T(8,128)(2,1)S(1)} collective-permute-done((bf16[2048,256]{1,0:T(8,128)(2,1)S(1)}, bf16[2048,256]{1,0:T(8,128)(2,1)S(1)}, u32[]{:S(2)}, u32[]{:S(2)}) %collective-permute-start.5) | collective-permute-done | bytes 1048608 | tf_op jit(solution)/shard_map/ppermute | solution.py:203
  103.9 3.7 %collective-permute-start.4 = (bf16[2048,256]{1,0:T(8,128)(2,1)}, bf16[2048,256]{1,0:T(8,128)(2,1)S(1)}, u32[]{:S(2)}, u32[]{:S(2)}) collective-permute-start(bf16[2048,256]{1,0:T(8,128)(2,1)} %collective-permute-done.3.refs_5_), channel_id=1, source_target_pairs={{0,4},{5,1},{2,6},{7,3},{8,12},{13,9},{10,14},{15,11},{16,20},{21,... | collective-permute-start | bytes 3145736 | tf_op jit(solution)/shard_map/ppermute | solution.py:206
  107.6 18.9 %collective-permute-done.6.refs_7_ = bf16[2048,256]{1,0:T(8,128)(2,1)S(1)} collective-permute-done((bf16[2048,256]{1,0:T(8,128)(2,1)}, bf16[2048,256]{1,0:T(8,128)(2,1)S(1)}, u32[]{:S(2)}, u32[]{:S(2)}) %collective-permute-start.6) | collective-permute-done | bytes 1048608 | tf_op jit(solution)/shard_map/ppermute | solution.py:203
  126.5 0.0 copy-done.2
  126.5 1.6 collective-permute-start.7
  128.2 0.0 collective-permute-done.9.refs_2_
  128.2 0.3 collective-permute-start.8
  128.4 20.4 %collective-permute-done.11.refs_3_ = bf16[256,2048]{1,0:T(8,128)(2,1)} collective-permute-done((bf16[256,2048]{1,0:T(8,128)(2,1)}, bf16[256,2048]{1,0:T(8,128)(2,1)}, u32[]{:S(2)}, u32[]{:S(2)}) %collective-permute-start.11) | collective-permute-done | bytes 1048608 | tf_op jit(solution)/shard_map/ppermute | solution.py:203
  148.9 4.4 %collective-permute-start.10 = (bf16[256,2048]{1,0:T(8,128)(2,1)}, bf16[256,2048]{1,0:T(8,128)(2,1)}, u32[]{:S(2)}, u32[]{:S(2)}) collective-permute-start(bf16[256,2048]{1,0:T(8,128)(2,1)} %collective-permute-done.9.refs_2_), channel_id=1, source_target_pairs={{0,4},{5,1},{2,6},{7,3},{8,12},{13,9},{10,14},{15,11},{16,20},{21,... | collective-permute-start | bytes 3145736 | tf_op jit(solution)/shard_map/ppermute | solution.py:206
  153.3 0.0 collective-permute-done.2.refs_2_
  153.3 0.0 collective-permute-start.12
  153.3 0.0 collective-permute-done.4.refs_3_
  153.3 0.0 collective-permute-done.7.refs_8_
  153.3 0.9 copy-done.4
  154.2 1.0 copy-done.6
  155.3 0.0 collective-permute-done.8.refs_9_
  155.3 0.0 all-to-all-done.1
  155.3 0.0 copy-done.5
  155.3 10.7 %hidden.1.hidden_ref = bf16[384,1024]{1,0:T(8,128)(2,1)} custom-call(bf16[6144,128]{1,0:T(8,128)(2,1)} %bitcast.6.x_ref, bf16[2048,256]{1,0:T(8,128)(2,1)} %bitcast.42, bf16[2048,256]{1,0:T(8,128)(2,1)} %bitcast.47, bf16[2048,256]{1,0:T(8,128)(2,1)} %copy-done.4, bf16[2048,256]{1,0:T(8,128)(2,1)} %copy-done.5, ...), custom_call_target="tpu_custom_call" | custom-call | tf_op jit(solution)/shard_map/hidden/pallas_call | solution.py:233
  165.9 0.0 collective-permute-done.10.refs_1_
  165.9 0.0 collective-permute-done.12.refs_4_
  166.0 6.4 %down.1 = bf16[6144,128]{1,0:T(8,128)(2,1)} custom-call(bf16[384,1024]{1,0:T(8,128)(2,1)} %hidden.1.hidden_ref, bf16[256,2048]{1,0:T(8,128)(2,1)} %bitcast.50, bf16[256,2048]{1,0:T(8,128)(2,1)} %collective-permute-done.10.refs_1_, bf16[256,2048]{1,0:T(8,128)(2,1)} %collective-permute-done.9.refs_2_, bf16[256,2048]{1,0:T(8,128)(2,1)} %collective-permute-done.11.refs_3_, ...), custom_call_target="tpu_custom_call" | custom-call | tf_op jit(solution)/shard_map/down/pallas_call | solution.py:244
  172.4 11.2 %all-to-all-start.2 = ((bf16[128,3,16,128]{3,2,1,0:T(8,128)(2,1)}), bf16[128,3,16,128]{3,2,1,0:T(8,128)(2,1)}, u32[]{:S(2)}, u32[]{:S(2)}) async-start(bf16[128,3,16,128]{3,2,1,0:T(8,128)(2,1)} %bitcast.39), calls=%async_computation.2 | async-start | bytes 3145728 | tf_op jit(solution)/shard_map/all_to_all | solution.py:256
  183.6 0.0 copy-done.8
  183.6 0.1 copy.20
  183.7 0.7 reshape.128.weight_ref
  184.5 39.0 %all-to-all-done.2 = bf16[128,3,16,128]{3,2,1,0:T(8,128)(2,1)} async-done(((bf16[128,3,16,128]{3,2,1,0:T(8,128)(2,1)}), bf16[128,3,16,128]{3,2,1,0:T(8,128)(2,1)}, u32[]{:S(2)}, u32[]{:S(2)}) %all-to-all-start.2) | async-done | bytes 1572896 | tf_op jit(solution)/shard_map/all_to_all | solution.py:256
  223.5 3.3 %combine.1 = bf16[128,2048]{1,0:T(8,128)(2,1)} custom-call(s32[256]{0:T(256)} %copy-done.7, f32[256]{0:T(256)} %reshape.128.weight_ref, bf16[384,16,128]{2,1,0:T(8,128)(2,1)} %bitcast.11.got_ref, bf16[128,2048]{1,0:T(8,128)(2,1)} %get-tuple-element.8.mixed_ref), custom_call_target="tpu_custom_call" | custom-call | tf_op jit(solution)/shard_map/combine/pallas_call | solution.py:259
  (16 shorter events, 0.1 us)
Async XLA Ops:
  0.0 8.5 %copy-start = (bf16[512,2048]{1,0:T(8,128)(2,1)S(1)}, bf16[512,2048]{1,0:T(8,128)(2,1)}, u32[]{:S(2)}) copy-start(bf16[512,2048]{1,0:T(8,128)(2,1)} %param.17) | copy-start | bytes 6291460
  1.7 5.0 %collective-permute-start = (bf16[16,256]{1,0:T(8,128)(2,1)S(1)}, bf16[16,256]{1,0:T(8,128)(2,1)S(1)}, u32[]{:S(2)}, u32[]{:S(2)}) collective-permute-start(bf16[16,256]{1,0:T(8,128)(2,1)S(1)} %pad_maximum_fusion), channel_id=1, source_target_pairs={{0,4},{4,8},{8,12},{12,16},{16,20},{20,24},{24,28},{28,32},{32,36}... | collective-permute-start | bytes 24584 | tf_op jit(solution)/shard_map/ppermute | solution.py:177
  13.8 4.6 %copy-start.1 = (bf16[1,2048,256]{2,1,0:T(8,128)(2,1)S(1)}, bf16[1,2048,256]{2,1,0:T(8,128)(2,1)}, u32[]{:S(2)}) copy-start(bf16[1,2048,256]{2,1,0:T(8,128)(2,1)} %param.21) | copy-start | bytes 3145732
  13.8 30.8 %all-to-all-start = ((bf16[4,128,2048]{2,1,0:T(8,128)(2,1)}), bf16[4,128,2048]{2,1,0:T(8,128)(2,1)}, u32[]{:S(2)}, u32[]{:S(2)}) async-start(bf16[4,128,2048]{2,1,0:T(8,128)(2,1)} %bitcast.40), calls=%async_computation | async-start | bytes 4194304 | tf_op jit(solution)/shard_map/all_to_all | solution.py:200
  18.5 48.1 %collective-permute-start.1 = (bf16[2048,256]{1,0:T(8,128)(2,1)S(1)}, bf16[2048,256]{1,0:T(8,128)(2,1)}, u32[]{:S(2)}, u32[]{:S(2)}) collective-permute-start(bf16[2048,256]{1,0:T(8,128)(2,1)S(1)} %bitcast.43), channel_id=1, source_target_pairs={{4,7},{1,0},{6,5},{3,2},{12,15},{9,8},{14,13},{11,10},{20,23},{17,... | collective-permute-start | bytes 3145736 | tf_op jit(solution)/shard_map/ppermute | solution.py:204
  18.6 51.4 %collective-permute-start.3 = (bf16[2048,256]{1,0:T(8,128)(2,1)}, bf16[2048,256]{1,0:T(8,128)(2,1)}, u32[]{:S(2)}, u32[]{:S(2)}) collective-permute-start(bf16[2048,256]{1,0:T(8,128)(2,1)} %bitcast.45), channel_id=1, source_target_pairs={{4,7},{1,0},{6,5},{3,2},{12,15},{9,8},{14,13},{11,10},{20,23},{17,... | collective-permute-start | bytes 3145736 | tf_op jit(solution)/shard_map/ppermute | solution.py:204
  22.7 26.5 %copy-start.7 = (s32[256]{0:T(256)}, s32[256]{0:T(256)S(1)}, u32[]{:S(2)}) copy-start(s32[256]{0:T(256)S(1)} %fusion.100.pos_ref) | copy-start | bytes 3076
  49.1 106.1 %all-to-all-start.1 = ((bf16[128,3,16,128]{3,2,1,0:T(8,128)(2,1)}), bf16[128,3,16,128]{3,2,1,0:T(8,128)(2,1)}, u32[]{:S(2)}, u32[]{:S(2)}) async-start(bf16[128,3,16,128]{3,2,1,0:T(8,128)(2,1)} %bitcast.41), calls=%async_computation.1 | async-start | bytes 3145728 | tf_op jit(solution)/shard_map/all_to_all | solution.py:229
  64.3 39.6 %collective-permute-start.5 = (bf16[2048,256]{1,0:T(8,128)(2,1)S(1)}, bf16[2048,256]{1,0:T(8,128)(2,1)S(1)}, u32[]{:S(2)}, u32[]{:S(2)}) collective-permute-start(bf16[2048,256]{1,0:T(8,128)(2,1)S(1)} %bitcast.44), channel_id=1, source_target_pairs={{4,5},{1,2},{6,7},{3,0},{12,13},{9,10},{14,15},{11,8},{20,21},{17,... | collective-permute-start | bytes 3145736 | tf_op jit(solution)/shard_map/ppermute | solution.py:203
  65.3 61.2 %collective-permute-start.6 = (bf16[2048,256]{1,0:T(8,128)(2,1)}, bf16[2048,256]{1,0:T(8,128)(2,1)S(1)}, u32[]{:S(2)}, u32[]{:S(2)}) collective-permute-start(bf16[2048,256]{1,0:T(8,128)(2,1)} %bitcast.46), channel_id=1, source_target_pairs={{4,5},{1,2},{6,7},{3,0},{12,13},{9,10},{14,15},{11,8},{20,21},{17,... | collective-permute-start | bytes 3145736 | tf_op jit(solution)/shard_map/ppermute | solution.py:203
  66.5 61.7 %collective-permute-start.9 = (bf16[256,2048]{1,0:T(8,128)(2,1)}, bf16[256,2048]{1,0:T(8,128)(2,1)}, u32[]{:S(2)}, u32[]{:S(2)}) collective-permute-start(bf16[256,2048]{1,0:T(8,128)(2,1)} %bitcast.48), channel_id=1, source_target_pairs={{4,7},{1,0},{6,5},{3,2},{12,15},{9,8},{14,13},{11,10},{20,23},{17,... | collective-permute-start | bytes 3145736 | tf_op jit(solution)/shard_map/ppermute | solution.py:204
  66.5 82.4 %collective-permute-start.11 = (bf16[256,2048]{1,0:T(8,128)(2,1)}, bf16[256,2048]{1,0:T(8,128)(2,1)}, u32[]{:S(2)}, u32[]{:S(2)}) collective-permute-start(bf16[256,2048]{1,0:T(8,128)(2,1)} %bitcast.49), channel_id=1, source_target_pairs={{4,5},{1,2},{6,7},{3,0},{12,13},{9,10},{14,15},{11,8},{20,21},{17,... | collective-permute-start | bytes 3145736 | tf_op jit(solution)/shard_map/ppermute | solution.py:203
  70.0 83.3 %collective-permute-start.2 = (bf16[2048,256]{1,0:T(8,128)(2,1)}, bf16[2048,256]{1,0:T(8,128)(2,1)S(1)}, u32[]{:S(2)}, u32[]{:S(2)}) collective-permute-start(bf16[2048,256]{1,0:T(8,128)(2,1)} %collective-permute-done.1.refs_4_), channel_id=1, source_target_pairs={{0,4},{5,1},{2,6},{7,3},{8,12},{13,9},{10,14},{15,11},{16,20},{21,... | collective-permute-start | bytes 3145736 | tf_op jit(solution)/shard_map/ppermute | solution.py:206
  103.9 22.6 %copy-start.2 = (bf16[2048,256]{1,0:T(8,128)(2,1)}, bf16[2048,256]{1,0:T(8,128)(2,1)S(1)}, u32[]{:S(2)}) copy-start(bf16[2048,256]{1,0:T(8,128)(2,1)S(1)} %collective-permute-done.5.refs_6_) | copy-start | bytes 3145732
  103.9 49.3 %collective-permute-start.4 = (bf16[2048,256]{1,0:T(8,128)(2,1)}, bf16[2048,256]{1,0:T(8,128)(2,1)S(1)}, u32[]{:S(2)}, u32[]{:S(2)}) collective-permute-start(bf16[2048,256]{1,0:T(8,128)(2,1)} %collective-permute-done.3.refs_5_), channel_id=1, source_target_pairs={{0,4},{5,1},{2,6},{7,3},{8,12},{13,9},{10,14},{15,11},{16,20},{21,... | collective-permute-start | bytes 3145736 | tf_op jit(solution)/shard_map/ppermute | solution.py:206
  126.5 26.8 %copy-start.3 = (bf16[2048,256]{1,0:T(8,128)(2,1)}, bf16[2048,256]{1,0:T(8,128)(2,1)S(1)}, u32[]{:S(2)}) copy-start(bf16[2048,256]{1,0:T(8,128)(2,1)S(1)} %collective-permute-done.6.refs_7_) | copy-start | bytes 3145732
  126.5 26.8 %collective-permute-start.7 = (bf16[2048,256]{1,0:T(8,128)(2,1)S(1)}, bf16[2048,256]{1,0:T(8,128)(2,1)S(1)}, u32[]{:S(2)}, u32[]{:S(2)}) collective-permute-start(bf16[2048,256]{1,0:T(8,128)(2,1)S(1)} %collective-permute-done.5.refs_6_), channel_id=1, source_target_pairs={{0,4},{5,1},{2,6},{7,3},{8,12},{13,9},{10,14},{15,11},{16,20},{21,... | collective-permute-start | bytes 3145736 | tf_op jit(solution)/shard_map/ppermute | solution.py:205
  128.2 27.1 %collective-permute-start.8 = (bf16[2048,256]{1,0:T(8,128)(2,1)S(1)}, bf16[2048,256]{1,0:T(8,128)(2,1)}, u32[]{:S(2)}, u32[]{:S(2)}) collective-permute-start(bf16[2048,256]{1,0:T(8,128)(2,1)S(1)} %collective-permute-done.6.refs_7_), channel_id=1, source_target_pairs={{0,4},{5,1},{2,6},{7,3},{8,12},{13,9},{10,14},{15,11},{16,20},{21,... | collective-permute-start | bytes 3145736 | tf_op jit(solution)/shard_map/ppermute | solution.py:205
  148.9 17.1 %collective-permute-start.10 = (bf16[256,2048]{1,0:T(8,128)(2,1)}, bf16[256,2048]{1,0:T(8,128)(2,1)}, u32[]{:S(2)}, u32[]{:S(2)}) collective-permute-start(bf16[256,2048]{1,0:T(8,128)(2,1)} %collective-permute-done.9.refs_2_), channel_id=1, source_target_pairs={{0,4},{5,1},{2,6},{7,3},{8,12},{13,9},{10,14},{15,11},{16,20},{21,... | collective-permute-start | bytes 3145736 | tf_op jit(solution)/shard_map/ppermute | solution.py:206
  153.3 1.0 copy-start.4
  153.3 12.7 %collective-permute-start.12 = (bf16[256,2048]{1,0:T(8,128)(2,1)}, bf16[256,2048]{1,0:T(8,128)(2,1)}, u32[]{:S(2)}, u32[]{:S(2)}) collective-permute-start(bf16[256,2048]{1,0:T(8,128)(2,1)} %collective-permute-done.11.refs_3_), channel_id=1, source_target_pairs={{0,4},{5,1},{2,6},{7,3},{8,12},{13,9},{10,14},{15,11},{16,20},{21,... | collective-permute-start | bytes 3145736 | tf_op jit(solution)/shard_map/ppermute | solution.py:205
  153.3 2.0 copy-start.5
  154.2 1.0 copy-start.6
  172.4 11.2 %copy-start.8 = (f32[128,2]{0,1:T(2,128)S(1)}, f32[128,2]{0,1:T(2,128)}, u32[]{:S(2)}) copy-start(f32[128,2]{0,1:T(2,128)} %param.20) | copy-start | bytes 3076
  172.4 51.1 %all-to-all-start.2 = ((bf16[128,3,16,128]{3,2,1,0:T(8,128)(2,1)}), bf16[128,3,16,128]{3,2,1,0:T(8,128)(2,1)}, u32[]{:S(2)}, u32[]{:S(2)}) async-start(bf16[128,3,16,128]{3,2,1,0:T(8,128)(2,1)} %bitcast.39), calls=%async_computation.2 | async-start | bytes 3145728 | tf_op jit(solution)/shard_map/all_to_all | solution.py:256

commit v3 on v2

v3 whole, which is shorter than its diff:
```python
import functools

import jax
import jax.numpy as jnp
from jax import lax
from jax.experimental import pallas as pl
from jax.experimental.pallas import tpu as pltpu
from jax.sharding import Mesh, PartitionSpec as P

SPAN = 16
EPS = 1e-06
LANES = 128


VMEM = pl.BlockSpec(memory_space=pltpu.VMEM)
SMEM = pl.BlockSpec(memory_space=pltpu.SMEM)
HBM = pl.BlockSpec(memory_space=pltpu.HBM)


def tile_rows(rows, chunk):
    return pl.ds(chunk // 8 * rows * 8 + chunk % 8, rows, stride=8)


def spread(wide, rows, chunks, value):
    tall = value.astype(jnp.float32).reshape(rows, chunks, LANES)
    for part in range(chunks // 8):
        wide[part * rows * 8 : (part + 1) * rows * 8] = tall[:, part * 8 : part * 8 + 8].reshape(rows * 8, LANES)


def gathered(wide, rows, chunks):
    parts = [wide[part * rows * 8 : (part + 1) * rows * 8].reshape(rows, 8, LANES) for part in range(chunks // 8)]
    return jnp.concatenate(parts, axis=1).astype(jnp.bfloat16)


def mix_kernel(rows, reach, pool_ref, docs_ref, prior_ref, map_ref, scale_ref, weight_ref, *refs):
    own_ref, far_plus, far_minus, next_low, next_high, prev_low, prev_high = refs[:7]
    data, docs, tally, turned = refs[7:]
    width = pool_ref.shape[1]
    tp = lax.axis_index(TP)
    window = jnp.left_shift(jnp.int32(2), tp)
    first = (lax.axis_index(SP) == 0).astype(jnp.float32)
    data[:reach] = jnp.zeros((reach, width), jnp.float32)
    data[reach : 2 * reach] = prior_ref[:, :width].astype(jnp.float32)
    data[2 * reach :] = pool_ref[...].astype(jnp.float32)
    docs[:reach] = jnp.full((reach, LANES), -1.0, jnp.float32)
    docs[reach : 2 * reach] = prior_ref[:, width:].astype(jnp.float32) * (1.0 - first) - first
    docs[2 * reach :] = docs_ref[...].astype(jnp.float32)
    tally[...] = jnp.ones(tally.shape, jnp.float32)
    extent = rows + reach
    span = 1
    while span < reach:
        @pl.when(span < window)
        def _():
            same = docs[reach:] == docs[reach - span : reach - span + extent]
            wide_same = jnp.concatenate([same] * (width // LANES), axis=1)
            grown = data[reach:] + jnp.where(wide_same, data[reach - span : reach - span + extent], 0.0)
            counted = tally[reach:] + jnp.where(same, tally[reach - span : reach - span + extent], 0.0)
            data[reach:] = grown
            tally[reach:] = counted

        span *= 2
    count = jnp.concatenate([tally[2 * reach :]] * (width // LANES), axis=1)
    pooled = (data[2 * reach :] / count - pool_ref[...].astype(jnp.float32)).astype(jnp.bfloat16)
    branch = (jnp.dot(pooled, map_ref[0], preferred_element_type=jnp.float32) * scale_ref[...]).astype(jnp.bfloat16)
    quarter = rows // 4
    turned[...] = branch
    order = [turned[pl.ds(lax.rem(tp + step, 4) * quarter, quarter), :] for step in range(4)]
    lined = jnp.concatenate(order, axis=0)
    half = weight_ref.shape[1] // 2
    low = jnp.dot(lined, weight_ref[:, :half], preferred_element_type=jnp.float32).astype(jnp.bfloat16)
    own_ref[:, :half] = low[:quarter]
    next_low[...] = low[quarter : 2 * quarter]
    far_minus[...] = low[2 * quarter : 3 * quarter]
    prev_low[...] = low[3 * quarter :]
    high = jnp.dot(lined, weight_ref[:, half:], preferred_element_type=jnp.float32).astype(jnp.bfloat16)
    own_ref[:, half:] = high[:quarter]
    next_high[...] = high[quarter : 2 * quarter]
    far_plus[...] = high[2 * quarter : 3 * quarter]
    prev_high[...] = high[3 * quarter :]


def dispatch_kernel(rows, width, slots, tok_ref, own_ref, nl_ref, nh_ref, pl_ref, ph_ref, stream_ref, gain_ref, out_ref, mixed_ref, wide, tiles):
    chunks = width // LANES
    low = nl_ref[...].astype(jnp.float32) + pl_ref[...].astype(jnp.float32)
    high = nh_ref[...].astype(jnp.float32) + ph_ref[...].astype(jnp.float32)
    total = own_ref[...].astype(jnp.float32) + jnp.concatenate([low, high], axis=1)
    mixed = (stream_ref[...].astype(jnp.float32) + total).astype(jnp.bfloat16)
    mixed_ref[...] = mixed
    up = mixed.astype(jnp.float32)
    scale = lax.rsqrt(jnp.sum(up * up, axis=1, keepdims=True) * (1.0 / width) + EPS)
    for chunk in range(chunks):
        cols = slice(chunk * LANES, (chunk + 1) * LANES)
        piece = up[:, cols] * scale * gain_ref[:, cols]
        wide[tile_rows(rows, chunk), :] = piece
    tiles[...] = gathered(wide, rows, chunks)

    @pl.loop(0, slots, unroll=8)
    def _(slot):
        out_ref[slot] = tiles[tok_ref[slot]]


def hidden_kernel(rows, width, ff, half, x_ref, *refs):
    own, late, near, both, other, last = [refs[2 * i : 2 * i + 2] for i in range(6)]
    out_ref, got, wide, flat, gates, ups, sems, got_sem = refs[12:]
    chunks = width // LANES
    is_home = half()
    home_side = (own, near, both, other)
    away_side = (late, near, both, last)
    targets = (gates, ups)

    got_copy = pltpu.make_async_copy(x_ref, got, got_sem)
    got_copy.start()

    def copy_in(side, place, j):
        return pltpu.make_async_copy(side[place][j], targets[j].at[place], sems.at[j, place])

    for place in range(4):
        for j in range(2):
            if home_side[place] is away_side[place]:
                copy_in(home_side, place, j).start()
            else:
                @pl.when(is_home == 1)
                def _():
                    copy_in(home_side, place, j).start()

                @pl.when(is_home == 0)
                def _():
                    copy_in(away_side, place, j).start()

    got_copy.wait()
    spread(wide, rows, chunks, got[...])
    for chunk in range(chunks):
        flat[:, chunk * LANES : (chunk + 1) * LANES] = wide[tile_rows(rows, chunk), :].astype(jnp.bfloat16)

    for place in range(4):
        copy_in(home_side, place, 0).wait()
        copy_in(home_side, place, 1).wait()
        gate_pre = jnp.dot(flat[...], gates[place], preferred_element_type=jnp.float32)
        up_pre = jnp.dot(flat[...], ups[place], preferred_element_type=jnp.float32)
        hidden = gate_pre / (1.0 + jnp.exp(-gate_pre)) * up_pre
        out_ref[:, place * ff : (place + 1) * ff] = hidden.astype(jnp.bfloat16)


def down_kernel(rows, width, ff, half, hidden_ref, *refs):
    own, late, near, both, other, last = refs[:6]
    out_ref, wide, downs, sems = refs[7:]
    chunks = width // LANES
    is_home = half()
    home_side = (own, near, both, other)
    away_side = (late, near, both, last)
    step = 4 * LANES

    def copy_in(side, place, begin):
        cols = pl.ds(begin, step)
        return pltpu.make_async_copy(
            side[place].at[:, cols], downs.at[pl.ds(place * ff, ff), cols], sems.at[place, begin // step]
        )

    for begin in range(0, width, step):
        for place in range(4):
            if home_side[place] is away_side[place]:
                copy_in(home_side, place, begin).start()
            else:
                @pl.when(is_home == 1)
                def _():
                    copy_in(home_side, place, begin).start()

                if place < 3:
                    @pl.when(is_home == 0)
                    def _():
                        copy_in(away_side, place, begin).start()

    @pl.when(is_home == 0)
    def _():
        downs[3 * ff :, :] = last[...]

    for begin in range(0, width, step):
        for place in range(3):
            copy_in(home_side, place, begin).wait()

        @pl.when(is_home == 1)
        def _():
            copy_in(home_side, 3, begin).wait()

        total = jnp.dot(hidden_ref[...], downs[:, begin : begin + step], preferred_element_type=jnp.float32)
        for piece in range(step // LANES):
            wide[tile_rows(rows, begin // LANES + piece), :] = total[:, piece * LANES : (piece + 1) * LANES]
    out_ref[...] = gathered(wide, rows, chunks)


def combine_kernel(rows, width, top, pos_ref, weight_ref, got_ref, mixed_ref, out_ref, wide):
    chunks = width // LANES

    @pl.loop(0, rows, unroll=4)
    def _(row):
        total = weight_ref[row * top] * got_ref[pos_ref[row * top]].astype(jnp.float32)
        for k in range(1, top):
            total = total + weight_ref[row * top + k] * got_ref[pos_ref[row * top + k]].astype(jnp.float32)
        for part in range(chunks // 8):
            wide[pl.ds(pl.multiple_of(part * rows * 8 + row * 8, 8), 8), :] = total[part * 8 : part * 8 + 8]

    for chunk in range(chunks):
        cols = slice(chunk * LANES, (chunk + 1) * LANES)
        piece = wide[tile_rows(rows, chunk), :]
        out_ref[:, cols] = (mixed_ref[:, cols].astype(jnp.float32) + piece).astype(jnp.bfloat16)


def slot_tables(route_block, expert_count, capacity, top_count, flip):
    flattened = route_block.reshape(-1)
    one_hot = (flattened[:, None] == jnp.arange(expert_count, dtype=jnp.int32)[None, :]).astype(jnp.int32)
    ranking = jnp.sum((jnp.cumsum(one_hot, axis=0) - one_hot) * one_hot, axis=1)
    place = (flattened // 2 * 2 + (flattened + flip) % 2) * capacity + ranking
    matches = place[None, :] == jnp.arange(expert_count * capacity, dtype=jnp.int32)[:, None]
    sources = jnp.sum(jnp.where(matches, jnp.arange(flattened.shape[0], dtype=jnp.int32)[None, :], 0), axis=1)
    return place, sources // top_count


def weight_moves(sp_count, tp_count):
    def at(pair, core, y):
        return (2 * pair + core) * tp_count + y

    served = lambda y: (y % 2 + y // 2) % 2
    home = lambda p, y: at(p, served(y), y)
    away = lambda p, y: at(p, 1 - served(y), y)
    inner = lambda y: tp_count - 1 - y
    outer = lambda y: y + 1 - 2 * (y % 2)
    pairs = [(pair, y) for pair in range(sp_count // 2) for y in range(tp_count)]
    over = [(home(p, y), away(p, y)) for p, y in pairs]
    back = [(away(p, y), home(p, y)) for p, y in pairs]
    near = [(home(p, y), home(p, inner(y))) for p, y in pairs] + [(away(p, y), away(p, outer(y))) for p, y in pairs]
    relay = [(away(p, y), home(p, inner(y))) for p, y in pairs] + over
    return near, relay, over, back


ALL = ("pair", "core", "yh", "yl")
SP = ("pair", "core")
TP = ("yh", "yl")


def forward(
    stream,
    pool_in,
    doc_ids,
    pool_map,
    pool_scale,
    out_weight,
    norm_gain,
    routes,
    route_weight,
    expert_gate,
    expert_up,
    expert_down,
):
    row_count = pool_in.shape[0]
    model_width = stream.shape[1]
    top_count = routes.shape[1]
    tp_count = lax.axis_size(TP)
    expert_count = lax.axis_size(SP)
    quarter = row_count // tp_count
    capacity = max(2, 3 * top_count * quarter // (2 * expert_count))
    slots = expert_count * capacity
    chunks = model_width // LANES
    tp_index = lax.axis_index(TP)
    docs = jnp.broadcast_to(doc_ids.astype(jnp.bfloat16)[:, None], (row_count, LANES))
    tail = jnp.concatenate([pool_in[row_count - SPAN :], docs[row_count - SPAN :]], axis=1)
    prior = lax.ppermute(tail, SP, [(i, i + 1) for i in range(expert_count - 1)])
    piece = jax.ShapeDtypeStruct((quarter, model_width // 2), jnp.bfloat16)
    held_rows, far_plus, far_minus, next_low, next_high, prev_low, prev_high = pl.pallas_call(
        functools.partial(mix_kernel, row_count, SPAN),
        out_shape=(jax.ShapeDtypeStruct((quarter, model_width), jnp.bfloat16),) + (piece,) * 6,
        in_specs=[VMEM] * 6,
        out_specs=(VMEM,) * 7,
        scratch_shapes=[
            pltpu.VMEM((row_count + 2 * SPAN, pool_in.shape[1]), jnp.float32),
            pltpu.VMEM((row_count + 2 * SPAN, LANES), jnp.float32),
            pltpu.VMEM((row_count + 2 * SPAN, LANES), jnp.float32),
            pltpu.VMEM((row_count, out_weight.shape[0]), jnp.bfloat16),
        ],
        name="mix",
    )(pool_in, docs, prior, pool_map, pool_scale[None], out_weight)

    own = (expert_gate[0], expert_up[0], expert_down[0])
    near, relay, over, back = weight_moves(expert_count, tp_count)
    plus = [(y, (y + 1) % tp_count) for y in range(tp_count)]
    minus = [(y, (y - 1) % tp_count) for y in range(tp_count)]

    def pass_on(array, pairs):
        return lax.ppermute(array, TP, pairs)

    def joined(left, right):
        return (left.astype(jnp.float32) + right.astype(jnp.float32)).astype(jnp.bfloat16)

    from_low = pass_on(far_plus, plus)
    from_high = pass_on(far_minus, minus)
    got_next_low = pass_on(next_low, plus)
    got_prev_high = pass_on(prev_high, minus)
    got_next_high = pass_on(joined(next_high, from_low), plus)
    got_prev_low = pass_on(joined(prev_low, from_high), minus)
    held = []
    for array in own:
        first = lax.ppermute(array, ALL, near)
        second = lax.ppermute(first, ALL, relay)
        late = lax.ppermute(array, ALL, over)
        other = lax.ppermute(first, ALL, back)
        last = lax.ppermute(second, ALL, over)
        held.append((array, late, first, second, other, last))

    own_routes = lax.dynamic_slice_in_dim(routes, tp_index * quarter, quarter, 0)
    places, tokens = slot_tables(own_routes, expert_count, capacity, top_count, lax.axis_index("yh"))

    dispatch, mixed_rows = pl.pallas_call(
        functools.partial(dispatch_kernel, quarter, model_width, slots),
        out_shape=(
            jax.ShapeDtypeStruct((slots, chunks, LANES), jnp.bfloat16),
            jax.ShapeDtypeStruct((quarter, model_width), jnp.bfloat16),
        ),
        in_specs=[SMEM] + [VMEM] * 7,
        out_specs=(VMEM, VMEM),
        scratch_shapes=[
            pltpu.VMEM((quarter * chunks, LANES), jnp.float32),
            pltpu.VMEM((quarter, chunks, LANES), jnp.bfloat16),
        ],
        name="dispatch",
    )(tokens, held_rows, got_next_low, got_next_high, got_prev_low, got_prev_high, stream, norm_gain[None])

    send = dispatch.reshape(expert_count, capacity, chunks, LANES)
    arrived = lax.all_to_all(send, ("pair", "yl"), 0, 0, tiled=True)

    ff = expert_gate.shape[2]
    flat_weight = route_weight.reshape(-1)
    is_home = lambda: (lax.axis_index("core") == (lax.axis_index("yl") + lax.axis_index("yh")) % 2).astype(jnp.int32)
    hidden = pl.pallas_call(
        functools.partial(hidden_kernel, slots, model_width, ff, is_home),
        out_shape=jax.ShapeDtypeStruct((slots, ff * tp_count), jnp.bfloat16),
        in_specs=[HBM] * 13,
        out_specs=VMEM,
        scratch_shapes=[
            pltpu.VMEM((slots * chunks, LANES), jnp.bfloat16),
            pltpu.VMEM((slots * chunks, LANES), jnp.float32),
            pltpu.VMEM((slots, model_width), jnp.bfloat16),
            pltpu.VMEM((tp_count, model_width, ff), jnp.bfloat16),
            pltpu.VMEM((tp_count, model_width, ff), jnp.bfloat16),
            pltpu.SemaphoreType.DMA((2, tp_count)),
            pltpu.SemaphoreType.DMA,
        ],
        name="hidden",
    )(arrived.reshape(slots * chunks, LANES), *[h[i] for i in range(6) for h in held[:2]])
    expert_rows = pl.pallas_call(
        functools.partial(down_kernel, slots, model_width, ff, is_home),
        out_shape=jax.ShapeDtypeStruct((slots, chunks, LANES), jnp.bfloat16),
        in_specs=[VMEM] + [HBM] * 5 + [VMEM, SMEM],
        out_specs=VMEM,
        scratch_shapes=[
            pltpu.VMEM((slots * chunks, LANES), jnp.float32),
            pltpu.VMEM((ff * tp_count, model_width), jnp.bfloat16),
            pltpu.SemaphoreType.DMA((tp_count, model_width // (4 * LANES))),
        ],
        compiler_params=pltpu.CompilerParams(vmem_limit_bytes=40 << 20),
        name="down",
    )(hidden, *held[2], flat_weight)

    returned = lax.all_to_all(
        expert_rows.reshape(expert_count, capacity, chunks, LANES), ("pair", "yl"), 0, 0, tiled=True
    )
    return pl.pallas_call(
        functools.partial(combine_kernel, quarter, model_width, top_count),
        out_shape=jax.ShapeDtypeStruct((quarter, model_width), jnp.bfloat16),
        in_specs=[SMEM, SMEM, VMEM, VMEM],
        out_specs=VMEM,
        scratch_shapes=[pltpu.VMEM((quarter * chunks, LANES), jnp.float32)],
        compiler_params=pltpu.CompilerParams(vmem_limit_bytes=30 << 20),
        name="combine",
    )(places, flat_weight, returned.reshape(slots, chunks, LANES), mixed_rows)


def solution(mesh):
    split = Mesh(mesh.devices.reshape(mesh.shape["sp"] // 2, 2, mesh.shape["tp"] // 2, 2), ALL)
    in_specs = (
        P(ALL, None),
        P(SP, TP),
        P(SP),
        P(TP, None, None),
        P(TP),
        P(TP, None),
        P(),
        P(SP, None),
        P(ALL, None),
        P(SP, None, TP),
        P(SP, None, TP),
        P(SP, TP, None),
    )
    return jax.shard_map(forward, mesh=split, in_specs=in_specs, out_specs=P(ALL, None), check_vma=False)
```

time: 228 us -> 167 us (0.73)
  waiting for transfers between devices: 135 us -> 29.9 us
  blocking collectives: 0 us -> 49.1 us
  matrix products: 5.32 us -> 0 us
  starting transfers between devices: 52 us -> 54.8 us
    all_to_all x3 -> x1, waiting for transfers between devices: 60.2 us -> 0.01 us  [forward(): arrived = lax.all_to_all(send, ('pair', 'yl'), 0, 0, tiled=True)]
    all_to_all x0 -> x1, blocking collectives: none -> 49.1 us  [forward(): lax.all_to_all(expert_rows.reshape(expert_count, capacity, chunks, LANES)...]
    ppermute x13 -> x22, waiting for transfers between devices: 74.9 us -> 29.9 us  [the longest x3 21.6 us: forward(): second = lax.ppermute(first, ALL, relay)]
    ppermute x13 -> x22, starting transfers between devices: 21.1 us -> 42.5 us  [the longest x6 9.7 us: pass_on(): return lax.ppermute(array, TP, pairs)]
    all_to_all x3 -> x1, starting transfers between devices: 30.9 us -> 12.3 us  [forward(): arrived = lax.all_to_all(send, ('pair', 'yl'), 0, 0, tiled=True)]
    dot_general x1 -> x0, matrix products: 5.32 us -> none  [forward(): jnp.dot(branch, out_weight, preferred_element_type=jnp.float32)]
    pallas_call x0 -> x1, Pallas kernels: none -> 4.7 us  [forward(): pl.pallas_call(functools.partial(mix_kernel, row_count, SPAN), out_shape=...]
    pallas_call x1, Pallas kernels: 10.7 us -> 7.31 us  [forward(): pl.pallas_call(functools.partial(hidden_kernel, slots, model_width, ff, i...]
  transfers between devices with their start and end apart: 16 -> 23, of which waited for: 6 -> 4; matrix products, arithmetic and copies ran while one was open for 2% -> 3% of each run, Pallas kernels for 7% -> 10%
where the time goes in v3:
time: 167 us; the launch traced here: 166 us
  starting transfers between devices  54.8 us (33%)
  blocking collectives  49.1 us (29%)
  waiting for transfers between devices  29.9 us (18%)
  Pallas kernels  23.3 us (14%)
  local copies, waits for them, and re-layouts  4.33 us (3%)
  other arithmetic  4.2 us (3%)
    all_to_all x1, blocking collectives, forward(): lax.all_to_all(expert_rows.reshape(expert_count, capacity, chunks, LANES)...  49.1 us
    ppermute x3, waiting for transfers between devices, forward(): second = lax.ppermute(first, ALL, relay)  21.6 us
    all_to_all x1, starting transfers between devices, forward(): arrived = lax.all_to_all(send, ('pair', 'yl'), 0, 0, tiled=True)  12.3 us
    ppermute x6, starting transfers between devices, pass_on(): return lax.ppermute(array, TP, pairs)  9.7 us
    ppermute x6, waiting for transfers between devices, pass_on(): return lax.ppermute(array, TP, pairs)  8.25 us
    ppermute x3, starting transfers between devices, forward(): last = lax.ppermute(second, ALL, over)  8.16 us
    pallas_call x1, Pallas kernels, forward(): pl.pallas_call(functools.partial(hidden_kernel, slots, model_width, ff, i...  7.31 us
    ppermute x3, starting transfers between devices, forward(): first = lax.ppermute(array, ALL, near)  7.05 us
  transfers between devices with their start and end apart: 23, of which 4 were waited for; matrix products, arithmetic and copies ran while one was open for 3% of the time, Pallas kernels for 10%

profile of v3, /device:TPU:2, one launch (start us, length us, event | category | flops | bytes accessed | tf_op | source)
XLA Modules:
  0.0 165.8 jit_solution(2391264008469721977)
XLA Ops:
  0.0 0.7 convert_element_type.30
  0.7 0.1 slice.16
  0.8 0.7 slice.15
  1.5 0.1 broadcast_in_dim.33
  1.6 1.9 %collective-permute-start = (bf16[16,384]{1,0:T(8,128)(2,1)S(1)}, bf16[16,384]{1,0:T(8,128)(2,1)S(1)}, u32[]{:S(2)}, u32[]{:S(2)}) collective-permute-start(bf16[16,384]{1,0:T(8,128)(2,1)S(1)} %pad_maximum_fusion), channel_id=1, source_target_pairs={{0,4},{4,8},{8,12},{12,16},{16,20},{20,24},{24,28},{28,32},{32,36}... | collective-permute-start | bytes 36872 | tf_op jit(solution)/shard_map/ppermute | solution.py:266
  3.5 3.1 %collective-permute-start.9 = (bf16[2048,256]{1,0:T(8,128)(2,1)}, bf16[2048,256]{1,0:T(8,128)(2,1)}, u32[]{:S(2)}, u32[]{:S(2)}) collective-permute-start(bf16[2048,256]{1,0:T(8,128)(2,1)} %bitcast.34), channel_id=1, source_target_pairs={{0,3},{5,6},{6,5},{3,0},{8,11},{13,14},{14,13},{11,8},{16,19},{21,... | collective-permute-start | bytes 3145736 | tf_op jit(solution)/shard_map/ppermute | solution.py:301
  6.6 0.1 copy.17
  6.7 0.1 eq.41
  6.8 0.0 collective-permute-done.prior_ref
  6.9 0.8 broadcast_in_dim.32.docs_ref
  7.7 4.7 %mix.1 = (bf16[128,2048]{1,0:T(8,128)(2,1)}, bf16[128,1024]{1,0:T(8,128)(2,1)}, bf16[128,1024]{1,0:T(8,128)(2,1)}, bf16[128,1024]{1,0:T(8,128)(2,1)}, bf16[128,1...) custom-call(bf16[512,256]{1,0:T(8,128)(2,1)} %pool_ref.1, ...), custom_call_target="tpu_custom_call" | custom-call | tf_op jit(solution)/shard_map/mix/pallas_call | solution.py:268
  12.4 3.0 %collective-permute-start.4 = (bf16[128,1024]{1,0:T(8,128)(2,1)}, bf16[128,1024]{1,0:T(8,128)(2,1)S(1)}, u32[]{:S(2)}, u32[]{:S(2)}) collective-permute-start(bf16[128,1024]{1,0:T(8,128)(2,1)} %get-tuple-element.19), channel_id=1, source_target_pairs={{0,3},{1,0},{2,1},{3,2},{4,7},{5,4},{6,5},{7,6},{8,11},{9,8},{10,9... | collective-permute-start | bytes 786440 | tf_op jit(solution)/shard_map/ppermute | solution.py:288
  15.4 0.1 reshape.85
  15.6 0.6 reduce-window.6
  16.2 0.2 slice_reduce_fusion
  16.4 0.1 collective-permute-start.2
  16.5 0.1 fusion.2
  16.6 0.4 collective-permute-start.1
  17.0 2.9 %collective-permute-start.6 = (bf16[128,1024]{1,0:T(8,128)(2,1)}, bf16[128,1024]{1,0:T(8,128)(2,1)S(1)}, u32[]{:S(2)}, u32[]{:S(2)}) collective-permute-start(bf16[128,1024]{1,0:T(8,128)(2,1)} %get-tuple-element.20), channel_id=1, source_target_pairs={{0,3},{1,0},{2,1},{3,2},{4,7},{5,4},{6,5},{7,6},{8,11},{9,8},{10,9... | collective-permute-start | bytes 786440 | tf_op jit(solution)/shard_map/ppermute | solution.py:288
  20.0 8.2 %collective-permute-done.4 = bf16[128,1024]{1,0:T(8,128)(2,1)S(1)} collective-permute-done((bf16[128,1024]{1,0:T(8,128)(2,1)}, bf16[128,1024]{1,0:T(8,128)(2,1)S(1)}, u32[]{:S(2)}, u32[]{:S(2)}) %collective-permute-start.4) | collective-permute-done | bytes 262176 | tf_op jit(solution)/shard_map/ppermute | solution.py:288
  28.2 1.0 add_convert_fusion
  29.2 3.1 %collective-permute-start.5 = (bf16[128,1024]{1,0:T(8,128)(2,1)S(1)}, bf16[128,1024]{1,0:T(8,128)(2,1)S(1)}, u32[]{:S(2)}, u32[]{:S(2)}) collective-permute-start(bf16[128,1024]{1,0:T(8,128)(2,1)S(1)} %add_convert_fusion), channel_id=1, source_target_pairs={{0,3},{1,0},{2,1},{3,2},{4,7},{5,4},{6,5},{7,6},{8,11},{9,8},{10,9... | collective-permute-start | bytes 786440 | tf_op jit(solution)/shard_map/ppermute | solution.py:288
  32.3 0.0 collective-permute-done.2
  32.3 1.0 add_convert_fusion.1
  33.3 0.1 collective-permute-start.3
  33.5 0.1 select_reduce_fusion
  33.6 0.0 collective-permute-done.1.nl_ref
  33.6 2.3 %collective-permute-start.7 = (bf16[2048,256]{1,0:T(8,128)(2,1)S(1)}, bf16[2048,256]{1,0:T(8,128)(2,1)}, u32[]{:S(2)}, u32[]{:S(2)}) collective-permute-start(bf16[2048,256]{1,0:T(8,128)(2,1)S(1)} %bitcast.36), channel_id=1, source_target_pairs={{0,4},{5,1},{6,2},{3,7},{8,12},{13,9},{14,10},{11,15},{16,20},{21,... | collective-permute-start | bytes 3145736 | tf_op jit(solution)/shard_map/ppermute | solution.py:303
  35.9 0.0 collective-permute-done.6.ph_ref
  35.9 3.2 %collective-permute-start.10 = (bf16[2048,256]{1,0:T(8,128)(2,1)}, bf16[2048,256]{1,0:T(8,128)(2,1)}, u32[]{:S(2)}, u32[]{:S(2)}) collective-permute-start(bf16[2048,256]{1,0:T(8,128)(2,1)} %bitcast.6.refs_1_), channel_id=1, source_target_pairs={{0,3},{5,6},{6,5},{3,0},{8,11},{13,14},{14,13},{11,8},{16,19},{21,... | collective-permute-start | bytes 3145736 | tf_op jit(solution)/shard_map/ppermute | solution.py:301
  39.2 0.0 collective-permute-done.5.pl_ref
  39.2 2.3 %collective-permute-start.8 = (bf16[2048,256]{1,0:T(8,128)(2,1)}, bf16[2048,256]{1,0:T(8,128)(2,1)}, u32[]{:S(2)}, u32[]{:S(2)}) collective-permute-start(bf16[2048,256]{1,0:T(8,128)(2,1)} %bitcast.6.refs_1_), channel_id=1, source_target_pairs={{0,4},{5,1},{6,2},{3,7},{8,12},{13,9},{14,10},{11,15},{16,20},{21,... | collective-permute-start | bytes 3145736 | tf_op jit(solution)/shard_map/ppermute | solution.py:303
  41.4 0.0 collective-permute-done.3.nh_ref
  41.4 0.7 copy-done.10
  42.1 0.7 collective-permute-start.18
  42.9 0.5 add_select_fusion.tok_ref
  43.4 4.1 %dispatch.1 = (bf16[384,16,128]{2,1,0:T(8,128)(2,1)}, bf16[128,2048]{1,0:T(8,128)(2,1)}) custom-call(s32[384]{0:T(512)} %add_select_fusion.tok_ref, bf16[128,2048]{1,0:T(8,128)(2,1)} %get-tuple-element.14.own_ref, bf16[128,1024]{1,0:T(8,128)(2,1)} %copy-done.7, bf16[128,1024]{1,0:T(8,128)(2,1)} %copy-done.10, bf16[128,1024]{1,0:T(8,128)(2,1)} %copy-done.9, ...), custom_call_target="tpu_custom_call" | custom-call | tf_op jit(solution)/shard_map/dispatch/pallas_call | solution.py:311
  47.5 12.3 %all-to-all-start = ((bf16[64,6,16,128]{3,2,1,0:T(8,128)(2,1)}), bf16[64,6,16,128]{3,2,1,0:T(8,128)(2,1)}, u32[]{:S(2)}, u32[]{:S(2)}) async-start(bf16[64,6,16,128]{3,2,1,0:T(8,128)(2,1)} %bitcast.33), calls=%async_computation | async-start | bytes 3145728 | tf_op jit(solution)/shard_map/all_to_all | solution.py:327
  59.9 0.1 collective-permute-start.11
  59.9 0.0 collective-permute-done.10.refs_5_
  60.0 3.5 %collective-permute-start.12 = (bf16[2048,256]{1,0:T(8,128)(2,1)}, bf16[2048,256]{1,0:T(8,128)(2,1)}, u32[]{:S(2)}, u32[]{:S(2)}) collective-permute-start(bf16[2048,256]{1,0:T(8,128)(2,1)} %collective-permute-done.10.refs_5_), channel_id=1, source_target_pairs={{4,3},{1,6},{2,5},{7,0},{12,11},{9,14},{10,13},{15,8},{20,19},{17,... | collective-permute-start | bytes 3145736 | tf_op jit(solution)/shard_map/ppermute | solution.py:302
  63.5 0.0 collective-permute-done.7.refs_2_
  63.5 1.3 collective-permute-start.13
  64.8 1.3 collective-permute-start.14
  66.1 1.3 collective-permute-start.19
  67.4 8.3 %collective-permute-done.11.refs_6_ = bf16[2048,256]{1,0:T(8,128)(2,1)} collective-permute-done((bf16[2048,256]{1,0:T(8,128)(2,1)}, bf16[2048,256]{1,0:T(8,128)(2,1)}, u32[]{:S(2)}, u32[]{:S(2)}) %collective-permute-start.11) | collective-permute-done | bytes 1048608 | tf_op jit(solution)/shard_map/ppermute | solution.py:302
  75.7 2.7 %collective-permute-start.15 = (bf16[2048,256]{1,0:T(8,128)(2,1)}, bf16[2048,256]{1,0:T(8,128)(2,1)}, u32[]{:S(2)}, u32[]{:S(2)}) collective-permute-start(bf16[2048,256]{1,0:T(8,128)(2,1)} %collective-permute-done.11.refs_6_), channel_id=1, source_target_pairs={{0,4},{5,1},{6,2},{3,7},{8,12},{13,9},{14,10},{11,15},{16,20},{21,... | collective-permute-start | bytes 3145736 | tf_op jit(solution)/shard_map/ppermute | solution.py:305
  78.4 8.5 %collective-permute-done.12.refs_7_ = bf16[2048,256]{1,0:T(8,128)(2,1)} collective-permute-done((bf16[2048,256]{1,0:T(8,128)(2,1)}, bf16[2048,256]{1,0:T(8,128)(2,1)}, u32[]{:S(2)}, u32[]{:S(2)}) %collective-permute-start.12) | collective-permute-done | bytes 1048608 | tf_op jit(solution)/shard_map/ppermute | solution.py:302
  86.9 2.7 %collective-permute-start.16 = (bf16[2048,256]{1,0:T(8,128)(2,1)}, bf16[2048,256]{1,0:T(8,128)(2,1)}, u32[]{:S(2)}, u32[]{:S(2)}) collective-permute-start(bf16[2048,256]{1,0:T(8,128)(2,1)} %collective-permute-done.12.refs_7_), channel_id=1, source_target_pairs={{0,4},{5,1},{6,2},{3,7},{8,12},{13,9},{14,10},{11,15},{16,20},{21,... | collective-permute-start | bytes 3145736 | tf_op jit(solution)/shard_map/ppermute | solution.py:305
  89.6 2.3 %collective-permute-start.17 = (bf16[256,2048]{1,0:T(8,128)(2,1)S(1)}, bf16[256,2048]{1,0:T(8,128)(2,1)}, u32[]{:S(2)}, u32[]{:S(2)}) collective-permute-start(bf16[256,2048]{1,0:T(8,128)(2,1)S(1)} %bitcast.31), channel_id=1, source_target_pairs={{0,4},{5,1},{6,2},{3,7},{8,12},{13,9},{14,10},{11,15},{16,20},{21,... | collective-permute-start | bytes 3145736 | tf_op jit(solution)/shard_map/ppermute | solution.py:303
  92.0 1.3 collective-permute-start.20
  93.3 4.8 %collective-permute-done.19.refs_3_ = bf16[256,2048]{1,0:T(8,128)(2,1)S(1)} collective-permute-done((bf16[256,2048]{1,0:T(8,128)(2,1)S(1)}, bf16[256,2048]{1,0:T(8,128)(2,1)S(1)}, u32[]{:S(2)}, u32[]{:S(2)}) %collective-permute-start.19) | collective-permute-done | bytes 1048608 | tf_op jit(solution)/shard_map/ppermute | solution.py:302
  98.1 2.7 %collective-permute-start.21 = (bf16[256,2048]{1,0:T(8,128)(2,1)S(1)}, bf16[256,2048]{1,0:T(8,128)(2,1)}, u32[]{:S(2)}, u32[]{:S(2)}) collective-permute-start(bf16[256,2048]{1,0:T(8,128)(2,1)S(1)} %collective-permute-done.19.refs_3_), channel_id=1, source_target_pairs={{0,4},{5,1},{6,2},{3,7},{8,12},{13,9},{14,10},{11,15},{16,20},{21,... | collective-permute-start | bytes 3145736 | tf_op jit(solution)/shard_map/ppermute | solution.py:305
  100.8 0.1 copy.20
  100.9 0.1 reshape.87.refs_6_.weight_ref
  101.0 0.0 collective-permute-done.15.refs_10_
  101.0 0.0 collective-permute-done.16.refs_11_
  101.1 7.3 %hidden.1.hidden_ref = bf16[384,1024]{1,0:T(8,128)(2,1)} custom-call(bf16[6144,128]{1,0:T(8,128)(2,1)} %bitcast.4.x_ref, bf16[2048,256]{1,0:T(8,128)(2,1)} %bitcast.35, bf16[2048,256]{1,0:T(8,128)(2,1)} %bitcast.6.refs_1_, bf16[2048,256]{1,0:T(8,128)(2,1)} %collective-permute-done.7.refs_2_, bf16[2048,256]{1,0:T(8,128)(2,1)} %collective-permute-done.8.refs_3_, ...), custom_call_target="tpu_custom_call" | custom-call | tf_op jit(solution)/shard_map/hidden/pallas_call | solution.py:332
  108.4 0.0 collective-permute-done.20.refs_4_
  108.4 0.0 collective-permute-done.21.refs_5_
  108.4 1.1 copy-done.1
  109.5 5.0 %down.1 = bf16[384,16,128]{2,1,0:T(8,128)(2,1)S(1)} custom-call(bf16[384,1024]{1,0:T(8,128)(2,1)S(1)} %copy-done.1, bf16[256,2048]{1,0:T(8,128)(2,1)S(1)} %bitcast.32, bf16[256,2048]{1,0:T(8,128)(2,1)} %collective-permute-done.17.refs_1_, bf16[256,2048]{1,0:T(8,128)(2,1)S(1)} %collective-permute-done.18.refs_2_, ...), custom_call_target="tpu_custom_call" | custom-call | tf_op jit(solution)/shard_map/down/pallas_call | solution.py:348
  114.6 49.1 %all_to_all.10 = bf16[64,6,16,128]{3,2,1,0:T(8,128)(2,1)S(1)} all-to-all(bf16[64,6,16,128]{3,2,1,0:T(8,128)(2,1)S(1)} %bitcast.28), channel_id=1, replica_groups=mesh['pair'=32,'core'=2,'yh'=2,'yl'=2] {'pair','yl'}, dimensions={0} | all-to-all | bytes 3145728 | tf_op jit(solution)/shard_map/all_to_all | solution.py:362
  163.6 2.2 %combine.1 = bf16[128,2048]{1,0:T(8,128)(2,1)} custom-call(s32[256]{0:T(256)S(1)} %multiply_add_fusion.pos_ref, f32[256]{0:T(256)S(1)} %reshape.87.refs_6_.weight_ref, bf16[384,16,128]{2,1,0:T(8,128)(2,1)S(1)} %bitcast.29, bf16[128,2048]{1,0:T(8,128)(2,1)S(1)} %copy-done.3), custom_call_target="tpu_custom_call" | custom-call | tf_op jit(solution)/shard_map/combine/pallas_call | solution.py:365
  (37 shorter events, 0.1 us)
Async XLA Ops:
  0.0 6.6 %copy-start = (s32[512,2]{0,1:T(2,128)S(1)}, s32[512,2]{0,1:T(2,128)}, u32[]{:S(2)}) copy-start(s32[512,2]{0,1:T(2,128)} %param.19) | copy-start | bytes 12292
  1.6 5.3 %collective-permute-start = (bf16[16,384]{1,0:T(8,128)(2,1)S(1)}, bf16[16,384]{1,0:T(8,128)(2,1)S(1)}, u32[]{:S(2)}, u32[]{:S(2)}) collective-permute-start(bf16[16,384]{1,0:T(8,128)(2,1)S(1)} %pad_maximum_fusion), channel_id=1, source_target_pairs={{0,4},{4,8},{8,12},{12,16},{16,20},{20,24},{24,28},{28,32},{32,36}... | collective-permute-start | bytes 36872 | tf_op jit(solution)/shard_map/ppermute | solution.py:266
  3.5 56.4 %collective-permute-start.9 = (bf16[2048,256]{1,0:T(8,128)(2,1)}, bf16[2048,256]{1,0:T(8,128)(2,1)}, u32[]{:S(2)}, u32[]{:S(2)}) collective-permute-start(bf16[2048,256]{1,0:T(8,128)(2,1)} %bitcast.34), channel_id=1, source_target_pairs={{0,3},{5,6},{6,5},{3,0},{8,11},{13,14},{14,13},{11,8},{16,19},{21,... | collective-permute-start | bytes 3145736 | tf_op jit(solution)/shard_map/ppermute | solution.py:301
  6.8 0.8 copy-start.11
  7.6 26.0 %copy-start.4 = (bf16[1,2048,256]{2,1,0:T(8,128)(2,1)S(1)}, bf16[1,2048,256]{2,1,0:T(8,128)(2,1)}, u32[]{:S(2)}) copy-start(bf16[1,2048,256]{2,1,0:T(8,128)(2,1)} %param.21) | copy-start | bytes 3145732
  12.3 29.8 %copy-start.2 = (bf16[1,256,2048]{2,1,0:T(8,128)(2,1)S(1)}, bf16[1,256,2048]{2,1,0:T(8,128)(2,1)}, u32[]{:S(2)}) copy-start(bf16[1,256,2048]{2,1,0:T(8,128)(2,1)} %param.23) | copy-start | bytes 3145732
  12.4 15.8 %collective-permute-start.4 = (bf16[128,1024]{1,0:T(8,128)(2,1)}, bf16[128,1024]{1,0:T(8,128)(2,1)S(1)}, u32[]{:S(2)}, u32[]{:S(2)}) collective-permute-start(bf16[128,1024]{1,0:T(8,128)(2,1)} %get-tuple-element.19), channel_id=1, source_target_pairs={{0,3},{1,0},{2,1},{3,2},{4,7},{5,4},{6,5},{7,6},{8,11},{9,8},{10,9... | collective-permute-start | bytes 786440 | tf_op jit(solution)/shard_map/ppermute | solution.py:288
  16.4 15.9 %collective-permute-start.2 = (bf16[128,1024]{1,0:T(8,128)(2,1)}, bf16[128,1024]{1,0:T(8,128)(2,1)S(1)}, u32[]{:S(2)}, u32[]{:S(2)}) collective-permute-start(bf16[128,1024]{1,0:T(8,128)(2,1)} %get-tuple-element.17), channel_id=1, source_target_pairs={{0,1},{1,2},{2,3},{3,0},{4,5},{5,6},{6,7},{7,4},{8,9},{9,10},{10,1... | collective-permute-start | bytes 786440 | tf_op jit(solution)/shard_map/ppermute | solution.py:288
  16.6 17.0 %collective-permute-start.1 = (bf16[128,1024]{1,0:T(8,128)(2,1)}, bf16[128,1024]{1,0:T(8,128)(2,1)S(1)}, u32[]{:S(2)}, u32[]{:S(2)}) collective-permute-start(bf16[128,1024]{1,0:T(8,128)(2,1)} %get-tuple-element.15), channel_id=1, source_target_pairs={{0,1},{1,2},{2,3},{3,0},{4,5},{5,6},{6,7},{7,4},{8,9},{9,10},{10,1... | collective-permute-start | bytes 786440 | tf_op jit(solution)/shard_map/ppermute | solution.py:288
  17.0 18.9 %collective-permute-start.6 = (bf16[128,1024]{1,0:T(8,128)(2,1)}, bf16[128,1024]{1,0:T(8,128)(2,1)S(1)}, u32[]{:S(2)}, u32[]{:S(2)}) collective-permute-start(bf16[128,1024]{1,0:T(8,128)(2,1)} %get-tuple-element.20), channel_id=1, source_target_pairs={{0,3},{1,0},{2,1},{3,2},{4,7},{5,4},{6,5},{7,6},{8,11},{9,8},{10,9... | collective-permute-start | bytes 786440 | tf_op jit(solution)/shard_map/ppermute | solution.py:288
  29.2 9.9 %collective-permute-start.5 = (bf16[128,1024]{1,0:T(8,128)(2,1)S(1)}, bf16[128,1024]{1,0:T(8,128)(2,1)S(1)}, u32[]{:S(2)}, u32[]{:S(2)}) collective-permute-start(bf16[128,1024]{1,0:T(8,128)(2,1)S(1)} %add_convert_fusion), channel_id=1, source_target_pairs={{0,3},{1,0},{2,1},{3,2},{4,7},{5,4},{6,5},{7,6},{8,11},{9,8},{10,9... | collective-permute-start | bytes 786440 | tf_op jit(solution)/shard_map/ppermute | solution.py:288
  33.3 8.1 %collective-permute-start.3 = (bf16[128,1024]{1,0:T(8,128)(2,1)S(1)}, bf16[128,1024]{1,0:T(8,128)(2,1)S(1)}, u32[]{:S(2)}, u32[]{:S(2)}) collective-permute-start(bf16[128,1024]{1,0:T(8,128)(2,1)S(1)} %add_convert_fusion.1), channel_id=1, source_target_pairs={{0,1},{1,2},{2,3},{3,0},{4,5},{5,6},{6,7},{7,4},{8,9},{9,10},{10,1... | collective-permute-start | bytes 786440 | tf_op jit(solution)/shard_map/ppermute | solution.py:288
  33.6 9.8 %copy-start.7 = (bf16[128,1024]{1,0:T(8,128)(2,1)}, bf16[128,1024]{1,0:T(8,128)(2,1)S(1)}, u32[]{:S(2)}) copy-start(bf16[128,1024]{1,0:T(8,128)(2,1)S(1)} %collective-permute-done.1.nl_ref) | copy-start | bytes 786436
  33.6 29.8 %collective-permute-start.7 = (bf16[2048,256]{1,0:T(8,128)(2,1)S(1)}, bf16[2048,256]{1,0:T(8,128)(2,1)}, u32[]{:S(2)}, u32[]{:S(2)}) collective-permute-start(bf16[2048,256]{1,0:T(8,128)(2,1)S(1)} %bitcast.36), channel_id=1, source_target_pairs={{0,4},{5,1},{6,2},{3,7},{8,12},{13,9},{14,10},{11,15},{16,20},{21,... | collective-permute-start | bytes 3145736 | tf_op jit(solution)/shard_map/ppermute | solution.py:303
  35.9 5.5 %copy-start.8 = (bf16[128,1024]{1,0:T(8,128)(2,1)}, bf16[128,1024]{1,0:T(8,128)(2,1)S(1)}, u32[]{:S(2)}) copy-start(bf16[128,1024]{1,0:T(8,128)(2,1)S(1)} %collective-permute-done.6.ph_ref) | copy-start | bytes 786436
  35.9 24.0 %collective-permute-start.10 = (bf16[2048,256]{1,0:T(8,128)(2,1)}, bf16[2048,256]{1,0:T(8,128)(2,1)}, u32[]{:S(2)}, u32[]{:S(2)}) collective-permute-start(bf16[2048,256]{1,0:T(8,128)(2,1)} %bitcast.6.refs_1_), channel_id=1, source_target_pairs={{0,3},{5,6},{6,5},{3,0},{8,11},{13,14},{14,13},{11,8},{16,19},{21,... | collective-permute-start | bytes 3145736 | tf_op jit(solution)/shard_map/ppermute | solution.py:301
  39.2 2.3 %copy-start.9 = (bf16[128,1024]{1,0:T(8,128)(2,1)}, bf16[128,1024]{1,0:T(8,128)(2,1)S(1)}, u32[]{:S(2)}) copy-start(bf16[128,1024]{1,0:T(8,128)(2,1)S(1)} %collective-permute-done.5.pl_ref) | copy-start | bytes 786436
  39.2 25.6 %collective-permute-start.8 = (bf16[2048,256]{1,0:T(8,128)(2,1)}, bf16[2048,256]{1,0:T(8,128)(2,1)}, u32[]{:S(2)}, u32[]{:S(2)}) collective-permute-start(bf16[2048,256]{1,0:T(8,128)(2,1)} %bitcast.6.refs_1_), channel_id=1, source_target_pairs={{0,4},{5,1},{6,2},{3,7},{8,12},{13,9},{14,10},{11,15},{16,20},{21,... | collective-permute-start | bytes 3145736 | tf_op jit(solution)/shard_map/ppermute | solution.py:303
  41.4 0.7 copy-start.10
  42.1 23.9 %collective-permute-start.18 = (bf16[256,2048]{1,0:T(8,128)(2,1)S(1)}, bf16[256,2048]{1,0:T(8,128)(2,1)S(1)}, u32[]{:S(2)}, u32[]{:S(2)}) collective-permute-start(bf16[256,2048]{1,0:T(8,128)(2,1)S(1)} %bitcast.30), channel_id=1, source_target_pairs={{0,3},{5,6},{6,5},{3,0},{8,11},{13,14},{14,13},{11,8},{16,19},{21,... | collective-permute-start | bytes 3145736 | tf_op jit(solution)/shard_map/ppermute | solution.py:301
  47.5 53.3 %copy-start.12 = (f32[128,2]{0,1:T(2,128)S(1)}, f32[128,2]{0,1:T(2,128)}, u32[]{:S(2)}) copy-start(f32[128,2]{0,1:T(2,128)} %param.20) | copy-start | bytes 3076
  47.5 53.5 %all-to-all-start = ((bf16[64,6,16,128]{3,2,1,0:T(8,128)(2,1)}), bf16[64,6,16,128]{3,2,1,0:T(8,128)(2,1)}, u32[]{:S(2)}, u32[]{:S(2)}) async-start(bf16[64,6,16,128]{3,2,1,0:T(8,128)(2,1)} %bitcast.33), calls=%async_computation | async-start | bytes 3145728 | tf_op jit(solution)/shard_map/all_to_all | solution.py:327
  59.9 15.8 %collective-permute-start.11 = (bf16[2048,256]{1,0:T(8,128)(2,1)}, bf16[2048,256]{1,0:T(8,128)(2,1)}, u32[]{:S(2)}, u32[]{:S(2)}) collective-permute-start(bf16[2048,256]{1,0:T(8,128)(2,1)} %collective-permute-done.9.refs_4_), channel_id=1, source_target_pairs={{4,3},{1,6},{2,5},{7,0},{12,11},{9,14},{10,13},{15,8},{20,19},{17,... | collective-permute-start | bytes 3145736 | tf_op jit(solution)/shard_map/ppermute | solution.py:302
  60.0 27.0 %collective-permute-start.12 = (bf16[2048,256]{1,0:T(8,128)(2,1)}, bf16[2048,256]{1,0:T(8,128)(2,1)}, u32[]{:S(2)}, u32[]{:S(2)}) collective-permute-start(bf16[2048,256]{1,0:T(8,128)(2,1)} %collective-permute-done.10.refs_5_), channel_id=1, source_target_pairs={{4,3},{1,6},{2,5},{7,0},{12,11},{9,14},{10,13},{15,8},{20,19},{17,... | collective-permute-start | bytes 3145736 | tf_op jit(solution)/shard_map/ppermute | solution.py:302
  63.5 26.2 %collective-permute-start.13 = (bf16[2048,256]{1,0:T(8,128)(2,1)}, bf16[2048,256]{1,0:T(8,128)(2,1)S(1)}, u32[]{:S(2)}, u32[]{:S(2)}) collective-permute-start(bf16[2048,256]{1,0:T(8,128)(2,1)} %collective-permute-done.9.refs_4_), channel_id=1, source_target_pairs={{4,0},{1,5},{2,6},{7,3},{12,8},{9,13},{10,14},{15,11},{20,16},{17,... | collective-permute-start | bytes 3145736 | tf_op jit(solution)/shard_map/ppermute | solution.py:304
  64.8 27.2 %collective-permute-start.14 = (bf16[2048,256]{1,0:T(8,128)(2,1)}, bf16[2048,256]{1,0:T(8,128)(2,1)S(1)}, u32[]{:S(2)}, u32[]{:S(2)}) collective-permute-start(bf16[2048,256]{1,0:T(8,128)(2,1)} %collective-permute-done.10.refs_5_), channel_id=1, source_target_pairs={{4,0},{1,5},{2,6},{7,3},{12,8},{9,13},{10,14},{15,11},{20,16},{17,... | collective-permute-start | bytes 3145736 | tf_op jit(solution)/shard_map/ppermute | solution.py:304
  66.1 32.0 %collective-permute-start.19 = (bf16[256,2048]{1,0:T(8,128)(2,1)S(1)}, bf16[256,2048]{1,0:T(8,128)(2,1)S(1)}, u32[]{:S(2)}, u32[]{:S(2)}) collective-permute-start(bf16[256,2048]{1,0:T(8,128)(2,1)S(1)} %collective-permute-done.18.refs_2_), channel_id=1, source_target_pairs={{4,3},{1,6},{2,5},{7,0},{12,11},{9,14},{10,13},{15,8},{20,19},{17,... | collective-permute-start | bytes 3145736 | tf_op jit(solution)/shard_map/ppermute | solution.py:302
  75.7 25.3 %collective-permute-start.15 = (bf16[2048,256]{1,0:T(8,128)(2,1)}, bf16[2048,256]{1,0:T(8,128)(2,1)}, u32[]{:S(2)}, u32[]{:S(2)}) collective-permute-start(bf16[2048,256]{1,0:T(8,128)(2,1)} %collective-permute-done.11.refs_6_), channel_id=1, source_target_pairs={{0,4},{5,1},{6,2},{3,7},{8,12},{13,9},{14,10},{11,15},{16,20},{21,... | collective-permute-start | bytes 3145736 | tf_op jit(solution)/shard_map/ppermute | solution.py:305
  86.9 14.1 %collective-permute-start.16 = (bf16[2048,256]{1,0:T(8,128)(2,1)}, bf16[2048,256]{1,0:T(8,128)(2,1)}, u32[]{:S(2)}, u32[]{:S(2)}) collective-permute-start(bf16[2048,256]{1,0:T(8,128)(2,1)} %collective-permute-done.12.refs_7_), channel_id=1, source_target_pairs={{0,4},{5,1},{6,2},{3,7},{8,12},{13,9},{14,10},{11,15},{16,20},{21,... | collective-permute-start | bytes 3145736 | tf_op jit(solution)/shard_map/ppermute | solution.py:305
  89.6 8.4 %copy-start.5 = (bf16[2048,256]{1,0:T(8,128)(2,1)}, bf16[2048,256]{1,0:T(8,128)(2,1)S(1)}, u32[]{:S(2)}) copy-start(bf16[2048,256]{1,0:T(8,128)(2,1)S(1)} %collective-permute-done.13.refs_8_) | copy-start | bytes 3145732
  89.6 18.7 %collective-permute-start.17 = (bf16[256,2048]{1,0:T(8,128)(2,1)S(1)}, bf16[256,2048]{1,0:T(8,128)(2,1)}, u32[]{:S(2)}, u32[]{:S(2)}) collective-permute-start(bf16[256,2048]{1,0:T(8,128)(2,1)S(1)} %bitcast.31), channel_id=1, source_target_pairs={{0,4},{5,1},{6,2},{3,7},{8,12},{13,9},{14,10},{11,15},{16,20},{21,... | collective-permute-start | bytes 3145736 | tf_op jit(solution)/shard_map/ppermute | solution.py:303
  92.0 6.1 %copy-start.6 = (bf16[2048,256]{1,0:T(8,128)(2,1)}, bf16[2048,256]{1,0:T(8,128)(2,1)S(1)}, u32[]{:S(2)}) copy-start(bf16[2048,256]{1,0:T(8,128)(2,1)S(1)} %collective-permute-done.14.refs_9_) | copy-start | bytes 3145732
  92.0 16.4 %collective-permute-start.20 = (bf16[256,2048]{1,0:T(8,128)(2,1)S(1)}, bf16[256,2048]{1,0:T(8,128)(2,1)}, u32[]{:S(2)}, u32[]{:S(2)}) collective-permute-start(bf16[256,2048]{1,0:T(8,128)(2,1)S(1)} %collective-permute-done.18.refs_2_), channel_id=1, source_target_pairs={{4,0},{1,5},{2,6},{7,3},{12,8},{9,13},{10,14},{15,11},{20,16},{17,... | collective-permute-start | bytes 3145736 | tf_op jit(solution)/shard_map/ppermute | solution.py:304
  98.1 10.4 %collective-permute-start.21 = (bf16[256,2048]{1,0:T(8,128)(2,1)S(1)}, bf16[256,2048]{1,0:T(8,128)(2,1)}, u32[]{:S(2)}, u32[]{:S(2)}) collective-permute-start(bf16[256,2048]{1,0:T(8,128)(2,1)S(1)} %collective-permute-done.19.refs_3_), channel_id=1, source_target_pairs={{0,4},{5,1},{6,2},{3,7},{8,12},{13,9},{14,10},{11,15},{16,20},{21,... | collective-permute-start | bytes 3145736 | tf_op jit(solution)/shard_map/ppermute | solution.py:305
  108.4 1.1 copy-start.1
  114.5 49.1 %copy-start.3 = (bf16[128,2048]{1,0:T(8,128)(2,1)S(1)}, bf16[128,2048]{1,0:T(8,128)(2,1)}, u32[]{:S(2)}) copy-start(bf16[128,2048]{1,0:T(8,128)(2,1)} %get-tuple-element.22.mixed_ref) | copy-start | bytes 1572868

commit v4 on v3

--- a/solution.py
+++ b/solution.py
@@ -99,36 +99,31 @@
         out_ref[slot] = tiles[tok_ref[slot]]
 
 
-def hidden_kernel(rows, width, ff, half, x_ref, *refs):
-    own, late, near, both, other, last = [refs[2 * i : 2 * i + 2] for i in range(6)]
-    out_ref, got, wide, flat, gates, ups, sems, got_sem = refs[12:]
+def expert_kernel(rows, width, ff, half, x_ref, *refs):
+    own, swapped, near, both, last = [refs[3 * i : 3 * i + 3] for i in range(5)]
+    out_ref, wide, flat, hidden, gates, ups, downs, sems = refs[16:]
     chunks = width // LANES
     is_home = half()
-    home_side = (own, near, both, other)
-    away_side = (late, near, both, last)
-    targets = (gates, ups)
-
-    got_copy = pltpu.make_async_copy(x_ref, got, got_sem)
-    got_copy.start()
+    home_side = (own, near, both, swapped)
+    away_side = (last, near, both, swapped)
+    targets = (gates, ups, downs)
 
     def copy_in(side, place, j):
         return pltpu.make_async_copy(side[place][j], targets[j].at[place], sems.at[j, place])
 
-    for place in range(4):
-        for j in range(2):
-            if home_side[place] is away_side[place]:
+    for place, j in [(place, j) for place in range(4) for j in range(2)] + [(place, 2) for place in range(4)]:
+        if home_side[place] is away_side[place]:
+            copy_in(home_side, place, j).start()
+        else:
+            @pl.when(is_home)
+            def _():
                 copy_in(home_side, place, j).start()
-            else:
-                @pl.when(is_home == 1)
-                def _():
-                    copy_in(home_side, place, j).start()
-
-                @pl.when(is_home == 0)
-                def _():
-                    copy_in(away_side, place, j).start()
-
-    got_copy.wait()
-    spread(wide, rows, chunks, got[...])
+
+            @pl.when(jnp.logical_not(is_home))
+            def _():
+                copy_in(away_side, place, j).start()
+
+    spread(wide, rows, chunks, x_ref[...])
     for chunk in range(chunks):
         flat[:, chunk * LANES : (chunk + 1) * LANES] = wide[tile_rows(rows, chunk), :].astype(jnp.bfloat16)
 
@@ -137,52 +132,15 @@
         copy_in(home_side, place, 1).wait()
         gate_pre = jnp.dot(flat[...], gates[place], preferred_element_type=jnp.float32)
         up_pre = jnp.dot(flat[...], ups[place], preferred_element_type=jnp.float32)
-        hidden = gate_pre / (1.0 + jnp.exp(-gate_pre)) * up_pre
-        out_ref[:, place * ff : (place + 1) * ff] = hidden.astype(jnp.bfloat16)
-
-
-def down_kernel(rows, width, ff, half, hidden_ref, *refs):
-    own, late, near, both, other, last = refs[:6]
-    out_ref, wide, downs, sems = refs[7:]
-    chunks = width // LANES
-    is_home = half()
-    home_side = (own, near, both, other)
-    away_side = (late, near, both, last)
+        product = gate_pre / (1.0 + jnp.exp(-gate_pre)) * up_pre
+        hidden[:, place * ff : (place + 1) * ff] = product.astype(jnp.bfloat16)
+
+    for place in range(4):
+        copy_in(home_side, place, 2).wait()
     step = 4 * LANES
-
-    def copy_in(side, place, begin):
-        cols = pl.ds(begin, step)
-        return pltpu.make_async_copy(
-            side[place].at[:, cols], downs.at[pl.ds(place * ff, ff), cols], sems.at[place, begin // step]
-        )
-
+    weights = downs.reshape(4 * ff, width)
     for begin in range(0, width, step):
-        for place in range(4):
-            if home_side[place] is away_side[place]:
-                copy_in(home_side, place, begin).start()
-            else:
-                @pl.when(is_home == 1)
-                def _():
-                    copy_in(home_side, place, begin).start()
-
-                if place < 3:
-                    @pl.when(is_home == 0)
-                    def _():
-                        copy_in(away_side, place, begin).start()
-
-    @pl.when(is_home == 0)
-    def _():
-        downs[3 * ff :, :] = last[...]
-
-    for begin in range(0, width, step):
-        for place in range(3):
-            copy_in(home_side, place, begin).wait()
-
-        @pl.when(is_home == 1)
-        def _():
-            copy_in(home_side, 3, begin).wait()
-
-        total = jnp.dot(hidden_ref[...], downs[:, begin : begin + step], preferred_element_type=jnp.float32)
+        total = jnp.dot(hidden[...], weights[:, begin : begin + step], preferred_element_type=jnp.float32)
         for piece in range(step // LANES):
             wide[tile_rows(rows, begin // LANES + piece), :] = total[:, piece * LANES : (piece + 1) * LANES]
     out_ref[...] = gathered(wide, rows, chunks)
@@ -296,14 +254,14 @@
     got_prev_high = pass_on(prev_high, minus)
     got_next_high = pass_on(joined(next_high, from_low), plus)
     got_prev_low = pass_on(joined(prev_low, from_high), minus)
+    is_home = lambda: lax.axis_index("core") == (lax.axis_index("yl") + lax.axis_index("yh")) % 2
     held = []
     for array in own:
         first = lax.ppermute(array, ALL, near)
         second = lax.ppermute(first, ALL, relay)
-        late = lax.ppermute(array, ALL, over)
-        other = lax.ppermute(first, ALL, back)
+        swapped = lax.ppermute(jnp.where(is_home(), array, first), ALL, over + back)
         last = lax.ppermute(second, ALL, over)
-        held.append((array, late, first, second, other, last))
+        held.append((array, swapped, first, second, last))
 
     own_routes = lax.dynamic_slice_in_dim(routes, tp_index * quarter, quarter, 0)
     places, tokens = slot_tables(own_routes, expert_count, capacity, top_count, lax.axis_index("yh"))
@@ -328,36 +286,23 @@
 
     ff = expert_gate.shape[2]
     flat_weight = route_weight.reshape(-1)
-    is_home = lambda: (lax.axis_index("core") == (lax.axis_index("yl") + lax.axis_index("yh")) % 2).astype(jnp.int32)
-    hidden = pl.pallas_call(
-        functools.partial(hidden_kernel, slots, model_width, ff, is_home),
-        out_shape=jax.ShapeDtypeStruct((slots, ff * tp_count), jnp.bfloat16),
-        in_specs=[HBM] * 13,
-        out_specs=VMEM,
-        scratch_shapes=[
-            pltpu.VMEM((slots * chunks, LANES), jnp.bfloat16),
-            pltpu.VMEM((slots * chunks, LANES), jnp.float32),
-            pltpu.VMEM((slots, model_width), jnp.bfloat16),
-            pltpu.VMEM((tp_count, model_width, ff), jnp.bfloat16),
-            pltpu.VMEM((tp_count, model_width, ff), jnp.bfloat16),
-            pltpu.SemaphoreType.DMA((2, tp_count)),
-            pltpu.SemaphoreType.DMA,
-        ],
-        name="hidden",
-    )(arrived.reshape(slots * chunks, LANES), *[h[i] for i in range(6) for h in held[:2]])
     expert_rows = pl.pallas_call(
-        functools.partial(down_kernel, slots, model_width, ff, is_home),
+        functools.partial(expert_kernel, slots, model_width, ff, is_home),
         out_shape=jax.ShapeDtypeStruct((slots, chunks, LANES), jnp.bfloat16),
-        in_specs=[VMEM] + [HBM] * 5 + [VMEM, SMEM],
+        in_specs=[VMEM] + [HBM] * 15 + [SMEM],
         out_specs=VMEM,
         scratch_shapes=[
             pltpu.VMEM((slots * chunks, LANES), jnp.float32),
-            pltpu.VMEM((ff * tp_count, model_width), jnp.bfloat16),
-            pltpu.SemaphoreType.DMA((tp_count, model_width // (4 * LANES))),
+            pltpu.VMEM((slots, model_width), jnp.bfloat16),
+            pltpu.VMEM((slots, ff * tp_count), jnp.bfloat16),
+            pltpu.VMEM((tp_count, model_width, ff), jnp.bfloat16),
+            pltpu.VMEM((tp_count, model_width, ff), jnp.bfloat16),
+            pltpu.VMEM((tp_count, ff, model_width), jnp.bfloat16),
+            pltpu.SemaphoreType.DMA((3, tp_count)),
         ],
-        compiler_params=pltpu.CompilerParams(vmem_limit_bytes=40 << 20),
-        name="down",
-    )(hidden, *held[2], flat_weight)
+        compiler_params=pltpu.CompilerParams(vmem_limit_bytes=32 << 20),
+        name="experts",
+    )(arrived.reshape(slots * chunks, LANES), *[h[i] for i in range(5) for h in held], flat_weight)
 
     returned = lax.all_to_all(
         expert_rows.reshape(expert_count, capacity, chunks, LANES), ("pair", "yl"), 0, 0, tiled=True

time: 167 us -> 166 us (level)
  starting transfers between devices: 54.8 us -> 44.6 us
  waiting for transfers between devices: 29.9 us -> 35.8 us
  other arithmetic: 4.2 us -> 9.09 us
  Pallas kernels: 23.3 us -> 18.8 us
  local copies, waits for them, and re-layouts: 4.33 us -> 6.63 us
    ppermute x6 -> x3, starting transfers between devices: 10.8 us -> 4.56 us  [forward(): swapped = lax.ppermute(jnp.where(is_home(), array, first), ALL, over + back)]
    select_n x0 -> x3, other arithmetic: none -> 4.86 us  [forward(): swapped = lax.ppermute(jnp.where(is_home(), array, first), ALL, over + back)]
    pallas_call x2 -> x1, Pallas kernels: 12.3 us -> 7.88 us  [forward(): pl.pallas_call(functools.partial(expert_kernel, slots, model_width, ff, i...]
    ppermute x6, waiting for transfers between devices: 8.25 us -> 12.6 us  [pass_on(): return lax.ppermute(array, TP, pairs)]
    ppermute x3, waiting for transfers between devices: 0.01 us -> 2.79 us  [forward(): first = lax.ppermute(array, ALL, near)]
    ppermute x3, waiting for transfers between devices: 21.6 us -> 19.1 us  [forward(): second = lax.ppermute(first, ALL, relay)]
    unnamed x27 -> x25, local copies, waits for them, and re-layouts: 1.98 us -> 4.26 us
    ppermute x3, starting transfers between devices: 4.91 us -> 2.98 us  [forward(): second = lax.ppermute(first, ALL, relay)]
  transfers between devices with their start and end apart: 23 -> 20, of which waited for: 4 -> 6; matrix products, arithmetic and copies ran while one was open for 3% -> 6% of each run, Pallas kernels for 10% -> 5%
where the time goes in v4:
time: 166 us
  blocking collectives  50.7 us (31%)
  starting transfers between devices  44.6 us (27%)
  waiting for transfers between devices  35.8 us (22%)
  Pallas kernels  18.8 us (11%)
  other arithmetic  9.09 us (5%)
  local copies, waits for them, and re-layouts  6.63 us (4%)
    all_to_all x1, blocking collectives, forward(): lax.all_to_all(expert_rows.reshape(expert_count, capacity, chunks, LANES)...  50.7 us
    ppermute x3, waiting for transfers between devices, forward(): second = lax.ppermute(first, ALL, relay)  19.1 us
    all_to_all x1, starting transfers between devices, forward(): arrived = lax.all_to_all(send, ('pair', 'yl'), 0, 0, tiled=True)  13.1 us
    ppermute x6, waiting for transfers between devices, pass_on(): return lax.ppermute(array, TP, pairs)  12.6 us
    ppermute x6, starting transfers between devices, pass_on(): return lax.ppermute(array, TP, pairs)  8.7 us
    pallas_call x1, Pallas kernels, forward(): pl.pallas_call(functools.partial(expert_kernel, slots, model_width, ff, i...  7.88 us
    ppermute x3, starting transfers between devices, forward(): last = lax.ppermute(second, ALL, over)  6.81 us
    ppermute x3, starting transfers between devices, forward(): first = lax.ppermute(array, ALL, near)  6.54 us
  transfers between devices with their start and end apart: 20, of which 6 were waited for; matrix products, arithmetic and copies ran while one was open for 6% of the time, Pallas kernels for 5%

profile of v4, /device:TPU:2, one launch (start us, length us, event | category | flops | bytes accessed | tf_op | source)
XLA Modules:
  0.0 165.8 jit_solution(16512401123196223025)
XLA Ops:
  0.0 0.7 convert_element_type.30
  0.7 0.1 slice.16
  0.8 0.7 slice.15
  1.5 0.1 broadcast_in_dim.33
  1.6 1.9 %collective-permute-start = (bf16[16,384]{1,0:T(8,128)(2,1)S(1)}, bf16[16,384]{1,0:T(8,128)(2,1)S(1)}, u32[]{:S(2)}, u32[]{:S(2)}) collective-permute-start(bf16[16,384]{1,0:T(8,128)(2,1)S(1)} %pad_maximum_fusion), channel_id=1, source_target_pairs={{0,4},{4,8},{8,12},{12,16},{16,20},{20,24},{24,28},{28,32},{32,36}... | collective-permute-start | bytes 36872 | tf_op jit(solution)/shard_map/ppermute | solution.py:224
  3.5 3.1 %collective-permute-start.9 = (bf16[2048,256]{1,0:T(8,128)(2,1)}, bf16[2048,256]{1,0:T(8,128)(2,1)}, u32[]{:S(2)}, u32[]{:S(2)}) collective-permute-start(bf16[2048,256]{1,0:T(8,128)(2,1)} %bitcast.36), channel_id=1, source_target_pairs={{0,3},{5,6},{6,5},{3,0},{8,11},{13,14},{14,13},{11,8},{16,19},{21,... | collective-permute-start | bytes 3145736 | tf_op jit(solution)/shard_map/ppermute | solution.py:260
  6.6 0.1 copy.17
  6.7 0.1 eq.50
  6.9 0.6 reduce-window.6
  7.5 0.2 slice_reduce_fusion
  7.7 0.1 reshape.85
  7.8 0.0 collective-permute-done.prior_ref
  7.8 0.8 broadcast_in_dim.32.docs_ref
  8.6 4.7 %mix.1 = (bf16[128,2048]{1,0:T(8,128)(2,1)}, bf16[128,1024]{1,0:T(8,128)(2,1)}, bf16[128,1024]{1,0:T(8,128)(2,1)}, bf16[128,1024]{1,0:T(8,128)(2,1)}, bf16[128,1...) custom-call(bf16[512,256]{1,0:T(8,128)(2,1)} %pool_ref.1, ...), custom_call_target="tpu_custom_call" | custom-call | tf_op jit(solution)/shard_map/mix/pallas_call | solution.py:226
  13.3 2.0 %collective-permute-start.4 = (bf16[128,1024]{1,0:T(8,128)(2,1)}, bf16[128,1024]{1,0:T(8,128)(2,1)S(1)}, u32[]{:S(2)}, u32[]{:S(2)}) collective-permute-start(bf16[128,1024]{1,0:T(8,128)(2,1)} %get-tuple-element.19), channel_id=1, source_target_pairs={{0,3},{1,0},{2,1},{3,2},{4,7},{5,4},{6,5},{7,6},{8,11},{9,8},{10,9... | collective-permute-start | bytes 786440 | tf_op jit(solution)/shard_map/ppermute | solution.py:246
  15.4 0.1 fusion.2
  15.5 0.1 collective-permute-start.2
  15.6 0.9 collective-permute-start.1
  16.5 2.5 %collective-permute-start.6 = (bf16[128,1024]{1,0:T(8,128)(2,1)}, bf16[128,1024]{1,0:T(8,128)(2,1)S(1)}, u32[]{:S(2)}, u32[]{:S(2)}) collective-permute-start(bf16[128,1024]{1,0:T(8,128)(2,1)} %get-tuple-element.20), channel_id=1, source_target_pairs={{0,3},{1,0},{2,1},{3,2},{4,7},{5,4},{6,5},{7,6},{8,11},{9,8},{10,9... | collective-permute-start | bytes 786440 | tf_op jit(solution)/shard_map/ppermute | solution.py:246
  19.0 9.2 %collective-permute-done.4 = bf16[128,1024]{1,0:T(8,128)(2,1)S(1)} collective-permute-done((bf16[128,1024]{1,0:T(8,128)(2,1)}, bf16[128,1024]{1,0:T(8,128)(2,1)S(1)}, u32[]{:S(2)}, u32[]{:S(2)}) %collective-permute-start.4) | collective-permute-done | bytes 262176 | tf_op jit(solution)/shard_map/ppermute | solution.py:246
  28.2 1.0 add_convert_fusion
  29.2 3.1 %collective-permute-start.5 = (bf16[128,1024]{1,0:T(8,128)(2,1)S(1)}, bf16[128,1024]{1,0:T(8,128)(2,1)S(1)}, u32[]{:S(2)}, u32[]{:S(2)}) collective-permute-start(bf16[128,1024]{1,0:T(8,128)(2,1)S(1)} %add_convert_fusion), channel_id=1, source_target_pairs={{0,3},{1,0},{2,1},{3,2},{4,7},{5,4},{6,5},{7,6},{8,11},{9,8},{10,9... | collective-permute-start | bytes 786440 | tf_op jit(solution)/shard_map/ppermute | solution.py:246
  32.3 1.0 add_convert_fusion.1
  33.3 0.1 collective-permute-start.3
  33.4 0.1 select_reduce_fusion
  33.6 0.0 collective-permute-done.1.nl_ref
  33.6 3.3 %collective-permute-start.11 = (bf16[256,2048]{1,0:T(8,128)(2,1)}, bf16[256,2048]{1,0:T(8,128)(2,1)}, u32[]{:S(2)}, u32[]{:S(2)}) collective-permute-start(bf16[256,2048]{1,0:T(8,128)(2,1)} %bitcast.7.refs_2_), channel_id=1, source_target_pairs={{0,3},{5,6},{6,5},{3,0},{8,11},{13,14},{14,13},{11,8},{16,19},{21,... | collective-permute-start | bytes 3145736 | tf_op jit(solution)/shard_map/ppermute | solution.py:260
  36.9 0.0 collective-permute-done.6.ph_ref
  36.9 0.1 collective-permute-start.7
  37.0 0.6 add_select_fusion.tok_ref
  37.6 0.0 collective-permute-done.5.pl_ref
  37.6 3.4 %collective-permute-done.3.nh_ref = bf16[128,1024]{1,0:T(8,128)(2,1)S(1)} collective-permute-done((bf16[128,1024]{1,0:T(8,128)(2,1)S(1)}, bf16[128,1024]{1,0:T(8,128)(2,1)S(1)}, u32[]{:S(2)}, u32[]{:S(2)}) %collective-permute-start.3) | collective-permute-done | bytes 262176 | tf_op jit(solution)/shard_map/ppermute | solution.py:246
  41.0 0.7 copy-done.9
  41.7 4.0 %dispatch.1 = (bf16[384,16,128]{2,1,0:T(8,128)(2,1)}, bf16[128,2048]{1,0:T(8,128)(2,1)}) custom-call(s32[384]{0:T(512)} %add_select_fusion.tok_ref, bf16[128,2048]{1,0:T(8,128)(2,1)} %get-tuple-element.14.own_ref, bf16[128,1024]{1,0:T(8,128)(2,1)} %copy-done.6, bf16[128,1024]{1,0:T(8,128)(2,1)} %copy-done.9, bf16[128,1024]{1,0:T(8,128)(2,1)} %copy-done.8, ...), custom_call_target="tpu_custom_call" | custom-call | tf_op jit(solution)/shard_map/dispatch/pallas_call | solution.py:269
  45.8 13.1 %all-to-all-start = ((bf16[64,6,16,128]{3,2,1,0:T(8,128)(2,1)}), bf16[64,6,16,128]{3,2,1,0:T(8,128)(2,1)S(1)}, u32[]{:S(2)}, u32[]{:S(2)}) async-start(bf16[64,6,16,128]{3,2,1,0:T(8,128)(2,1)} %bitcast.38), calls=%async_computation | async-start | bytes 3145728 | tf_op jit(solution)/shard_map/all_to_all | solution.py:285
  58.8 0.0 collective-permute-done.9.refs_7_
  58.8 1.3 broadcast_select_fusion.1
  60.2 0.1 collective-permute-start.10
  60.3 0.5 collective-permute-start.14
  60.8 2.8 %collective-permute-done.7.refs_6_ = bf16[2048,256]{1,0:T(8,128)(2,1)} collective-permute-done((bf16[2048,256]{1,0:T(8,128)(2,1)S(1)}, bf16[2048,256]{1,0:T(8,128)(2,1)}, u32[]{:S(2)}, u32[]{:S(2)}) %collective-permute-start.7) | collective-permute-done | bytes 1048608 | tf_op jit(solution)/shard_map/ppermute | solution.py:260
  63.6 2.5 %collective-permute-start.13 = (bf16[2048,256]{1,0:T(8,128)(2,1)}, bf16[2048,256]{1,0:T(8,128)(2,1)}, u32[]{:S(2)}, u32[]{:S(2)}) collective-permute-start(bf16[2048,256]{1,0:T(8,128)(2,1)} %collective-permute-done.7.refs_6_), channel_id=1, source_target_pairs={{4,3},{1,6},{2,5},{7,0},{12,11},{9,14},{10,13},{15,8},{20,19},{17,... | collective-permute-start | bytes 3145736 | tf_op jit(solution)/shard_map/ppermute | solution.py:261
  66.1 0.0 collective-permute-start.15
  66.1 2.3 %broadcast_select_fusion = bf16[256,2048]{1,0:T(8,128)(2,1)} fusion(bf16[256,2048]{1,0:T(8,128)(2,1)} %collective-permute-done.11.refs_8_, pred[]{:T(512)S(6)} %eq.57, bf16[1,256,2048]{2,1,0:T(8,128)(2,1)} %param.23), kind=kLoop, calls=%fused_computation | loop fusion | flops 524288 | bytes 3145729 | tf_op jit(solution)/shard_map/jit(_where)/select_n | solution.py:262
  68.4 3.2 %collective-permute-start.12 = (bf16[256,2048]{1,0:T(8,128)(2,1)}, bf16[256,2048]{1,0:T(8,128)(2,1)}, u32[]{:S(2)}, u32[]{:S(2)}) collective-permute-start(bf16[256,2048]{1,0:T(8,128)(2,1)} %broadcast_select_fusion), channel_id=1, source_target_pairs={{0,4},{5,1},{6,2},{3,7},{8,12},{13,9},{14,10},{11,15},{16,20},{21,... | collective-permute-start | bytes 3145736 | tf_op jit(solution)/shard_map/ppermute | solution.py:262
  71.6 1.2 broadcast_select_fusion.2
  72.8 1.0 copy-done.3
  73.8 1.2 collective-permute-start.8
  75.0 12.3 %collective-permute-done.13.refs_9_ = bf16[2048,256]{1,0:T(8,128)(2,1)} collective-permute-done((bf16[2048,256]{1,0:T(8,128)(2,1)}, bf16[2048,256]{1,0:T(8,128)(2,1)}, u32[]{:S(2)}, u32[]{:S(2)}) %collective-permute-start.13) | collective-permute-done | bytes 1048608 | tf_op jit(solution)/shard_map/ppermute | solution.py:261
  87.4 2.3 %collective-permute-start.16 = (bf16[2048,256]{1,0:T(8,128)(2,1)}, bf16[2048,256]{1,0:T(8,128)(2,1)}, u32[]{:S(2)}, u32[]{:S(2)}) collective-permute-start(bf16[2048,256]{1,0:T(8,128)(2,1)} %collective-permute-done.13.refs_9_), channel_id=1, source_target_pairs={{0,4},{5,1},{6,2},{3,7},{8,12},{13,9},{14,10},{11,15},{16,20},{21,... | collective-permute-start | bytes 3145736 | tf_op jit(solution)/shard_map/ppermute | solution.py:263
  89.6 0.0 collective-permute-done.14.refs_10_
  89.6 2.2 %collective-permute-start.17 = (bf16[2048,256]{1,0:T(8,128)(2,1)}, bf16[2048,256]{1,0:T(8,128)(2,1)}, u32[]{:S(2)}, u32[]{:S(2)}) collective-permute-start(bf16[2048,256]{1,0:T(8,128)(2,1)} %collective-permute-done.14.refs_10_), channel_id=1, source_target_pairs={{0,4},{5,1},{6,2},{3,7},{8,12},{13,9},{14,10},{11,15},{16,20},{21,... | collective-permute-start | bytes 3145736 | tf_op jit(solution)/shard_map/ppermute | solution.py:263
  91.9 6.7 %collective-permute-done.15.refs_11_ = bf16[256,2048]{1,0:T(8,128)(2,1)} collective-permute-done((bf16[256,2048]{1,0:T(8,128)(2,1)}, bf16[256,2048]{1,0:T(8,128)(2,1)}, u32[]{:S(2)}, u32[]{:S(2)}) %collective-permute-start.15) | collective-permute-done | bytes 1048608 | tf_op jit(solution)/shard_map/ppermute | solution.py:261
  98.6 2.3 %collective-permute-start.18 = (bf16[256,2048]{1,0:T(8,128)(2,1)}, bf16[256,2048]{1,0:T(8,128)(2,1)}, u32[]{:S(2)}, u32[]{:S(2)}) collective-permute-start(bf16[256,2048]{1,0:T(8,128)(2,1)} %collective-permute-done.15.refs_11_), channel_id=1, source_target_pairs={{0,4},{5,1},{6,2},{3,7},{8,12},{13,9},{14,10},{11,15},{16,20},{21,... | collective-permute-start | bytes 3145736 | tf_op jit(solution)/shard_map/ppermute | solution.py:263
  100.9 0.1 copy.20
  101.0 0.1 reshape.87.refs_15_.weight_ref
  101.2 0.0 collective-permute-done.12.refs_5_
  101.2 0.0 collective-permute-done.8.refs_3_
  101.2 0.0 collective-permute-done.17.refs_13_
  101.2 1.3 collective-permute-done.18.refs_14_
  102.5 1.2 copy-done.2
  103.7 1.2 copy-done.4
  104.9 7.9 %experts.1 = bf16[384,16,128]{2,1,0:T(8,128)(2,1)S(1)} custom-call(bf16[6144,128]{1,0:T(8,128)(2,1)S(1)} %bitcast.31, bf16[2048,256]{1,0:T(8,128)(2,1)S(1)} %bitcast.35, bf16[2048,256]{1,0:T(8,128)(2,1)S(1)} %bitcast.37, bf16[256,2048]{1,0:T(8,128)(2,1)} %bitcast.7.refs_2_, bf16[2048,256]{1,0:T(8,128)(2,1)} %collective-permute-done.8.refs_3_, ...), custom_call_target="tpu_custom_call" | custom-call | tf_op jit(solution)/shard_map/experts/pallas_call | solution.py:289
  112.8 50.7 %all_to_all.10 = bf16[64,6,16,128]{3,2,1,0:T(8,128)(2,1)S(1)} all-to-all(bf16[64,6,16,128]{3,2,1,0:T(8,128)(2,1)S(1)} %bitcast.32), channel_id=1, replica_groups=mesh['pair'=32,'core'=2,'yh'=2,'yl'=2] {'pair','yl'}, dimensions={0} | all-to-all | bytes 3145728 | tf_op jit(solution)/shard_map/all_to_all | solution.py:307
  163.6 2.2 %combine.1 = bf16[128,2048]{1,0:T(8,128)(2,1)} custom-call(s32[256]{0:T(256)S(1)} %multiply_add_fusion.pos_ref, f32[256]{0:T(256)S(1)} %reshape.87.refs_15_.weight_ref, bf16[384,16,128]{2,1,0:T(8,128)(2,1)S(1)} %bitcast.33, bf16[128,2048]{1,0:T(8,128)(2,1)S(1)} %copy-done.5), custom_call_target="tpu_custom_call" | custom-call | tf_op jit(solution)/shard_map/combine/pallas_call | solution.py:310
  (31 shorter events, 0.1 us)
Async XLA Ops:
  0.0 6.6 %copy-start = (s32[512,2]{0,1:T(2,128)S(1)}, s32[512,2]{0,1:T(2,128)}, u32[]{:S(2)}) copy-start(s32[512,2]{0,1:T(2,128)} %param.19) | copy-start | bytes 12292
  1.6 6.3 %collective-permute-start = (bf16[16,384]{1,0:T(8,128)(2,1)S(1)}, bf16[16,384]{1,0:T(8,128)(2,1)S(1)}, u32[]{:S(2)}, u32[]{:S(2)}) collective-permute-start(bf16[16,384]{1,0:T(8,128)(2,1)S(1)} %pad_maximum_fusion), channel_id=1, source_target_pairs={{0,4},{4,8},{8,12},{12,16},{16,20},{20,24},{24,28},{28,32},{32,36}... | collective-permute-start | bytes 36872 | tf_op jit(solution)/shard_map/ppermute | solution.py:224
  3.5 55.4 %collective-permute-start.9 = (bf16[2048,256]{1,0:T(8,128)(2,1)}, bf16[2048,256]{1,0:T(8,128)(2,1)}, u32[]{:S(2)}, u32[]{:S(2)}) collective-permute-start(bf16[2048,256]{1,0:T(8,128)(2,1)} %bitcast.36), channel_id=1, source_target_pairs={{0,3},{5,6},{6,5},{3,0},{8,11},{13,14},{14,13},{11,8},{16,19},{21,... | collective-permute-start | bytes 3145736 | tf_op jit(solution)/shard_map/ppermute | solution.py:260
  7.8 0.8 copy-start.10
  8.6 28.3 %copy-start.1 = (bf16[1,2048,256]{2,1,0:T(8,128)(2,1)S(1)}, bf16[1,2048,256]{2,1,0:T(8,128)(2,1)}, u32[]{:S(2)}) copy-start(bf16[1,2048,256]{2,1,0:T(8,128)(2,1)} %param.21) | copy-start | bytes 3145732
  13.3 14.9 %collective-permute-start.4 = (bf16[128,1024]{1,0:T(8,128)(2,1)}, bf16[128,1024]{1,0:T(8,128)(2,1)S(1)}, u32[]{:S(2)}, u32[]{:S(2)}) collective-permute-start(bf16[128,1024]{1,0:T(8,128)(2,1)} %get-tuple-element.19), channel_id=1, source_target_pairs={{0,3},{1,0},{2,1},{3,2},{4,7},{5,4},{6,5},{7,6},{8,11},{9,8},{10,9... | collective-permute-start | bytes 786440 | tf_op jit(solution)/shard_map/ppermute | solution.py:246
  15.5 16.8 %collective-permute-start.2 = (bf16[128,1024]{1,0:T(8,128)(2,1)}, bf16[128,1024]{1,0:T(8,128)(2,1)S(1)}, u32[]{:S(2)}, u32[]{:S(2)}) collective-permute-start(bf16[128,1024]{1,0:T(8,128)(2,1)} %get-tuple-element.17), channel_id=1, source_target_pairs={{0,1},{1,2},{2,3},{3,0},{4,5},{5,6},{6,7},{7,4},{8,9},{9,10},{10,1... | collective-permute-start | bytes 786440 | tf_op jit(solution)/shard_map/ppermute | solution.py:246
  15.6 18.0 %collective-permute-start.1 = (bf16[128,1024]{1,0:T(8,128)(2,1)}, bf16[128,1024]{1,0:T(8,128)(2,1)S(1)}, u32[]{:S(2)}, u32[]{:S(2)}) collective-permute-start(bf16[128,1024]{1,0:T(8,128)(2,1)} %get-tuple-element.15), channel_id=1, source_target_pairs={{0,1},{1,2},{2,3},{3,0},{4,5},{5,6},{6,7},{7,4},{8,9},{9,10},{10,1... | collective-permute-start | bytes 786440 | tf_op jit(solution)/shard_map/ppermute | solution.py:246
  16.5 20.4 %collective-permute-start.6 = (bf16[128,1024]{1,0:T(8,128)(2,1)}, bf16[128,1024]{1,0:T(8,128)(2,1)S(1)}, u32[]{:S(2)}, u32[]{:S(2)}) collective-permute-start(bf16[128,1024]{1,0:T(8,128)(2,1)} %get-tuple-element.20), channel_id=1, source_target_pairs={{0,3},{1,0},{2,1},{3,2},{4,7},{5,4},{6,5},{7,6},{8,11},{9,8},{10,9... | collective-permute-start | bytes 786440 | tf_op jit(solution)/shard_map/ppermute | solution.py:246
  29.2 8.4 %collective-permute-start.5 = (bf16[128,1024]{1,0:T(8,128)(2,1)S(1)}, bf16[128,1024]{1,0:T(8,128)(2,1)S(1)}, u32[]{:S(2)}, u32[]{:S(2)}) collective-permute-start(bf16[128,1024]{1,0:T(8,128)(2,1)S(1)} %add_convert_fusion), channel_id=1, source_target_pairs={{0,3},{1,0},{2,1},{3,2},{4,7},{5,4},{6,5},{7,6},{8,11},{9,8},{10,9... | collective-permute-start | bytes 786440 | tf_op jit(solution)/shard_map/ppermute | solution.py:246
  33.3 7.7 %collective-permute-start.3 = (bf16[128,1024]{1,0:T(8,128)(2,1)S(1)}, bf16[128,1024]{1,0:T(8,128)(2,1)S(1)}, u32[]{:S(2)}, u32[]{:S(2)}) collective-permute-start(bf16[128,1024]{1,0:T(8,128)(2,1)S(1)} %add_convert_fusion.1), channel_id=1, source_target_pairs={{0,1},{1,2},{2,3},{3,0},{4,5},{5,6},{6,7},{7,4},{8,9},{9,10},{10,1... | collective-permute-start | bytes 786440 | tf_op jit(solution)/shard_map/ppermute | solution.py:246
  33.6 7.4 %copy-start.6 = (bf16[128,1024]{1,0:T(8,128)(2,1)}, bf16[128,1024]{1,0:T(8,128)(2,1)S(1)}, u32[]{:S(2)}) copy-start(bf16[128,1024]{1,0:T(8,128)(2,1)S(1)} %collective-permute-done.1.nl_ref) | copy-start | bytes 786436
  33.6 32.5 %collective-permute-start.11 = (bf16[256,2048]{1,0:T(8,128)(2,1)}, bf16[256,2048]{1,0:T(8,128)(2,1)}, u32[]{:S(2)}, u32[]{:S(2)}) collective-permute-start(bf16[256,2048]{1,0:T(8,128)(2,1)} %bitcast.7.refs_2_), channel_id=1, source_target_pairs={{0,3},{5,6},{6,5},{3,0},{8,11},{13,14},{14,13},{11,8},{16,19},{21,... | collective-permute-start | bytes 3145736 | tf_op jit(solution)/shard_map/ppermute | solution.py:260
  36.9 4.1 %copy-start.7 = (bf16[128,1024]{1,0:T(8,128)(2,1)}, bf16[128,1024]{1,0:T(8,128)(2,1)S(1)}, u32[]{:S(2)}) copy-start(bf16[128,1024]{1,0:T(8,128)(2,1)S(1)} %collective-permute-done.6.ph_ref) | copy-start | bytes 786436
  36.9 26.7 %collective-permute-start.7 = (bf16[2048,256]{1,0:T(8,128)(2,1)S(1)}, bf16[2048,256]{1,0:T(8,128)(2,1)}, u32[]{:S(2)}, u32[]{:S(2)}) collective-permute-start(bf16[2048,256]{1,0:T(8,128)(2,1)S(1)} %bitcast.34), channel_id=1, source_target_pairs={{0,3},{5,6},{6,5},{3,0},{8,11},{13,14},{14,13},{11,8},{16,19},{21,... | collective-permute-start | bytes 3145736 | tf_op jit(solution)/shard_map/ppermute | solution.py:260
  37.6 3.4 %copy-start.8 = (bf16[128,1024]{1,0:T(8,128)(2,1)}, bf16[128,1024]{1,0:T(8,128)(2,1)S(1)}, u32[]{:S(2)}) copy-start(bf16[128,1024]{1,0:T(8,128)(2,1)S(1)} %collective-permute-done.5.pl_ref) | copy-start | bytes 786436
  41.0 0.7 copy-start.9
  45.8 56.7 %all-to-all-start = ((bf16[64,6,16,128]{3,2,1,0:T(8,128)(2,1)}), bf16[64,6,16,128]{3,2,1,0:T(8,128)(2,1)S(1)}, u32[]{:S(2)}, u32[]{:S(2)}) async-start(bf16[64,6,16,128]{3,2,1,0:T(8,128)(2,1)} %bitcast.38), calls=%async_computation | async-start | bytes 3145728 | tf_op jit(solution)/shard_map/all_to_all | solution.py:285
  60.2 12.6 %collective-permute-start.10 = (bf16[2048,256]{1,0:T(8,128)(2,1)S(1)}, bf16[2048,256]{1,0:T(8,128)(2,1)S(1)}, u32[]{:S(2)}, u32[]{:S(2)}) collective-permute-start(bf16[2048,256]{1,0:T(8,128)(2,1)S(1)} %broadcast_select_fusion.1), channel_id=1, source_target_pairs={{0,4},{5,1},{6,2},{3,7},{8,12},{13,9},{14,10},{11,15},{16,20},{21,... | collective-permute-start | bytes 3145736 | tf_op jit(solution)/shard_map/ppermute | solution.py:262
  60.3 29.3 %collective-permute-start.14 = (bf16[2048,256]{1,0:T(8,128)(2,1)}, bf16[2048,256]{1,0:T(8,128)(2,1)}, u32[]{:S(2)}, u32[]{:S(2)}) collective-permute-start(bf16[2048,256]{1,0:T(8,128)(2,1)} %collective-permute-done.9.refs_7_), channel_id=1, source_target_pairs={{4,3},{1,6},{2,5},{7,0},{12,11},{9,14},{10,13},{15,8},{20,19},{17,... | collective-permute-start | bytes 3145736 | tf_op jit(solution)/shard_map/ppermute | solution.py:261
  63.6 23.8 %collective-permute-start.13 = (bf16[2048,256]{1,0:T(8,128)(2,1)}, bf16[2048,256]{1,0:T(8,128)(2,1)}, u32[]{:S(2)}, u32[]{:S(2)}) collective-permute-start(bf16[2048,256]{1,0:T(8,128)(2,1)} %collective-permute-done.7.refs_6_), channel_id=1, source_target_pairs={{4,3},{1,6},{2,5},{7,0},{12,11},{9,14},{10,13},{15,8},{20,19},{17,... | collective-permute-start | bytes 3145736 | tf_op jit(solution)/shard_map/ppermute | solution.py:261
  66.1 32.5 %collective-permute-start.15 = (bf16[256,2048]{1,0:T(8,128)(2,1)}, bf16[256,2048]{1,0:T(8,128)(2,1)}, u32[]{:S(2)}, u32[]{:S(2)}) collective-permute-start(bf16[256,2048]{1,0:T(8,128)(2,1)} %collective-permute-done.11.refs_8_), channel_id=1, source_target_pairs={{4,3},{1,6},{2,5},{7,0},{12,11},{9,14},{10,13},{15,8},{20,19},{17,... | collective-permute-start | bytes 3145736 | tf_op jit(solution)/shard_map/ppermute | solution.py:261
  68.4 32.5 %copy-start.11 = (f32[128,2]{0,1:T(2,128)S(1)}, f32[128,2]{0,1:T(2,128)}, u32[]{:S(2)}) copy-start(f32[128,2]{0,1:T(2,128)} %param.20) | copy-start | bytes 3076
  68.4 32.8 %collective-permute-start.12 = (bf16[256,2048]{1,0:T(8,128)(2,1)}, bf16[256,2048]{1,0:T(8,128)(2,1)}, u32[]{:S(2)}, u32[]{:S(2)}) collective-permute-start(bf16[256,2048]{1,0:T(8,128)(2,1)} %broadcast_select_fusion), channel_id=1, source_target_pairs={{0,4},{5,1},{6,2},{3,7},{8,12},{13,9},{14,10},{11,15},{16,20},{21,... | collective-permute-start | bytes 3145736 | tf_op jit(solution)/shard_map/ppermute | solution.py:262
  72.8 1.0 copy-start.3
  73.8 27.4 %collective-permute-start.8 = (bf16[2048,256]{1,0:T(8,128)(2,1)}, bf16[2048,256]{1,0:T(8,128)(2,1)}, u32[]{:S(2)}, u32[]{:S(2)}) collective-permute-start(bf16[2048,256]{1,0:T(8,128)(2,1)} %broadcast_select_fusion.2), channel_id=1, source_target_pairs={{0,4},{5,1},{6,2},{3,7},{8,12},{13,9},{14,10},{11,15},{16,20},{21,... | collective-permute-start | bytes 3145736 | tf_op jit(solution)/shard_map/ppermute | solution.py:262
  87.4 13.8 %collective-permute-start.16 = (bf16[2048,256]{1,0:T(8,128)(2,1)}, bf16[2048,256]{1,0:T(8,128)(2,1)}, u32[]{:S(2)}, u32[]{:S(2)}) collective-permute-start(bf16[2048,256]{1,0:T(8,128)(2,1)} %collective-permute-done.13.refs_9_), channel_id=1, source_target_pairs={{0,4},{5,1},{6,2},{3,7},{8,12},{13,9},{14,10},{11,15},{16,20},{21,... | collective-permute-start | bytes 3145736 | tf_op jit(solution)/shard_map/ppermute | solution.py:263
  89.6 11.6 %collective-permute-start.17 = (bf16[2048,256]{1,0:T(8,128)(2,1)}, bf16[2048,256]{1,0:T(8,128)(2,1)}, u32[]{:S(2)}, u32[]{:S(2)}) collective-permute-start(bf16[2048,256]{1,0:T(8,128)(2,1)} %collective-permute-done.14.refs_10_), channel_id=1, source_target_pairs={{0,4},{5,1},{6,2},{3,7},{8,12},{13,9},{14,10},{11,15},{16,20},{21,... | collective-permute-start | bytes 3145736 | tf_op jit(solution)/shard_map/ppermute | solution.py:263
  98.6 3.9 %collective-permute-start.18 = (bf16[256,2048]{1,0:T(8,128)(2,1)}, bf16[256,2048]{1,0:T(8,128)(2,1)}, u32[]{:S(2)}, u32[]{:S(2)}) collective-permute-start(bf16[256,2048]{1,0:T(8,128)(2,1)} %collective-permute-done.15.refs_11_), channel_id=1, source_target_pairs={{0,4},{5,1},{6,2},{3,7},{8,12},{13,9},{14,10},{11,15},{16,20},{21,... | collective-permute-start | bytes 3145736 | tf_op jit(solution)/shard_map/ppermute | solution.py:263
  102.5 1.2 copy-start.2
  103.7 1.2 copy-start.4
  112.8 50.7 %copy-start.5 = (bf16[128,2048]{1,0:T(8,128)(2,1)S(1)}, bf16[128,2048]{1,0:T(8,128)(2,1)}, u32[]{:S(2)}) copy-start(bf16[128,2048]{1,0:T(8,128)(2,1)} %get-tuple-element.22.mixed_ref) | copy-start | bytes 1572868

commit v5 on v4

--- a/solution.py
+++ b/solution.py
@@ -99,30 +99,33 @@
         out_ref[slot] = tiles[tok_ref[slot]]
 
 
-def expert_kernel(rows, width, ff, half, x_ref, *refs):
-    own, swapped, near, both, last = [refs[3 * i : 3 * i + 3] for i in range(5)]
-    out_ref, wide, flat, hidden, gates, ups, downs, sems = refs[16:]
+def start_copies(is_home, home_side, away_side, copy_in, indices):
+    for place in range(4):
+        for j in indices:
+            if home_side[place] is away_side[place]:
+                copy_in(home_side, place, j).start()
+            else:
+                @pl.when(is_home)
+                def _():
+                    copy_in(home_side, place, j).start()
+
+                @pl.when(jnp.logical_not(is_home))
+                def _():
+                    copy_in(away_side, place, j).start()
+
+
+def hidden_kernel(rows, width, ff, half, x_ref, *refs):
+    own, swapped, near, both, last = [refs[2 * i : 2 * i + 2] for i in range(5)]
+    out_ref, wide, flat, gates, ups, sems = refs[10:]
     chunks = width // LANES
-    is_home = half()
     home_side = (own, near, both, swapped)
     away_side = (last, near, both, swapped)
-    targets = (gates, ups, downs)
+    targets = (gates, ups)
 
     def copy_in(side, place, j):
         return pltpu.make_async_copy(side[place][j], targets[j].at[place], sems.at[j, place])
 
-    for place, j in [(place, j) for place in range(4) for j in range(2)] + [(place, 2) for place in range(4)]:
-        if home_side[place] is away_side[place]:
-            copy_in(home_side, place, j).start()
-        else:
-            @pl.when(is_home)
-            def _():
-                copy_in(home_side, place, j).start()
-
-            @pl.when(jnp.logical_not(is_home))
-            def _():
-                copy_in(away_side, place, j).start()
-
+    start_copies(half(), home_side, away_side, copy_in, (0, 1))
     spread(wide, rows, chunks, x_ref[...])
     for chunk in range(chunks):
         flat[:, chunk * LANES : (chunk + 1) * LANES] = wide[tile_rows(rows, chunk), :].astype(jnp.bfloat16)
@@ -133,14 +136,23 @@
         gate_pre = jnp.dot(flat[...], gates[place], preferred_element_type=jnp.float32)
         up_pre = jnp.dot(flat[...], ups[place], preferred_element_type=jnp.float32)
         product = gate_pre / (1.0 + jnp.exp(-gate_pre)) * up_pre
-        hidden[:, place * ff : (place + 1) * ff] = product.astype(jnp.bfloat16)
-
+        out_ref[:, place * ff : (place + 1) * ff] = product.astype(jnp.bfloat16)
+
+
+def down_kernel(rows, width, ff, half, hidden_ref, own, swapped, near, both, last, after_ref, out_ref, wide, downs, sems):
+    chunks = width // LANES
+    home_side = ((own,), (near,), (both,), (swapped,))
+    away_side = ((last,), home_side[1], home_side[2], home_side[3])
+
+    def copy_in(side, place, j):
+        return pltpu.make_async_copy(side[place][j], downs.at[pl.ds(place * ff, ff)], sems.at[place])
+
+    start_copies(half(), home_side, away_side, copy_in, (0,))
     for place in range(4):
-        copy_in(home_side, place, 2).wait()
+        copy_in(home_side, place, 0).wait()
     step = 4 * LANES
-    weights = downs.reshape(4 * ff, width)
     for begin in range(0, width, step):
-        total = jnp.dot(hidden[...], weights[:, begin : begin + step], preferred_element_type=jnp.float32)
+        total = jnp.dot(hidden_ref[...], downs[:, begin : begin + step], preferred_element_type=jnp.float32)
         for piece in range(step // LANES):
             wide[tile_rows(rows, begin // LANES + piece), :] = total[:, piece * LANES : (piece + 1) * LANES]
     out_ref[...] = gathered(wide, rows, chunks)
@@ -286,23 +298,34 @@
 
     ff = expert_gate.shape[2]
     flat_weight = route_weight.reshape(-1)
-    expert_rows = pl.pallas_call(
-        functools.partial(expert_kernel, slots, model_width, ff, is_home),
-        out_shape=jax.ShapeDtypeStruct((slots, chunks, LANES), jnp.bfloat16),
-        in_specs=[VMEM] + [HBM] * 15 + [SMEM],
+    hidden = pl.pallas_call(
+        functools.partial(hidden_kernel, slots, model_width, ff, is_home),
+        out_shape=jax.ShapeDtypeStruct((slots, ff * tp_count), jnp.bfloat16),
+        in_specs=[VMEM] + [HBM] * 10,
         out_specs=VMEM,
         scratch_shapes=[
             pltpu.VMEM((slots * chunks, LANES), jnp.float32),
             pltpu.VMEM((slots, model_width), jnp.bfloat16),
-            pltpu.VMEM((slots, ff * tp_count), jnp.bfloat16),
             pltpu.VMEM((tp_count, model_width, ff), jnp.bfloat16),
             pltpu.VMEM((tp_count, model_width, ff), jnp.bfloat16),
-            pltpu.VMEM((tp_count, ff, model_width), jnp.bfloat16),
-            pltpu.SemaphoreType.DMA((3, tp_count)),
+            pltpu.SemaphoreType.DMA((2, tp_count)),
         ],
-        compiler_params=pltpu.CompilerParams(vmem_limit_bytes=32 << 20),
-        name="experts",
-    )(arrived.reshape(slots * chunks, LANES), *[h[i] for i in range(5) for h in held], flat_weight)
+        compiler_params=pltpu.CompilerParams(vmem_limit_bytes=24 << 20),
+        name="hidden",
+    )(arrived.reshape(slots * chunks, LANES), *[h[i] for i in range(5) for h in held[:2]])
+    expert_rows = pl.pallas_call(
+        functools.partial(down_kernel, slots, model_width, ff, is_home),
+        out_shape=jax.ShapeDtypeStruct((slots, chunks, LANES), jnp.bfloat16),
+        in_specs=[VMEM] + [HBM] * 5 + [SMEM],
+        out_specs=VMEM,
+        scratch_shapes=[
+            pltpu.VMEM((slots * chunks, LANES), jnp.float32),
+            pltpu.VMEM((ff * tp_count, model_width), jnp.bfloat16),
+            pltpu.SemaphoreType.DMA((tp_count,)),
+        ],
+        compiler_params=pltpu.CompilerParams(vmem_limit_bytes=24 << 20),
+        name="down",
+    )(hidden, *held[2], flat_weight)
 
     returned = lax.all_to_all(
         expert_rows.reshape(expert_count, capacity, chunks, LANES), ("pair", "yl"), 0, 0, tiled=True

time: 166 us -> 173 us (1.042)
  waiting for transfers between devices: 35.8 us -> 45 us
  blocking collectives: 50.7 us -> 48.5 us
  starting transfers between devices: 44.6 us -> 42.4 us
  Pallas kernels: 18.8 us -> 20.9 us
    ppermute x6, waiting for transfers between devices: 12.6 us -> 22.5 us  [pass_on(): return lax.ppermute(array, TP, pairs)]
    ppermute x3, waiting for transfers between devices: 19.1 us -> 22.5 us  [forward(): second = lax.ppermute(first, ALL, relay)]
    ppermute x3, waiting for transfers between devices: 2.79 us -> 0.01 us  [forward(): first = lax.ppermute(array, ALL, near)]
    all_to_all x1, blocking collectives: 50.7 us -> 48.5 us  [forward(): lax.all_to_all(expert_rows.reshape(expert_count, capacity, chunks, LANES)...]
    pallas_call x1 -> x2, Pallas kernels: 7.88 us -> 10.1 us  [the longest x1 5.21 us: forward(): pl.pallas_call(functools.partial(hidden_kernel, slots, model_width, ff, i...]
  transfers between devices with their start and end apart: 20 -> 20, of which waited for: 6 -> 6; matrix products, arithmetic and copies ran while one was open for 6% -> 6% of each run, Pallas kernels for 5% -> 8%
where the time goes in v5:
time: 173 us
  blocking collectives  48.5 us (28%)
  waiting for transfers between devices  45 us (26%)
  starting transfers between devices  42.4 us (25%)
  Pallas kernels  20.9 us (12%)
  other arithmetic  8.97 us (5%)
  local copies, waits for them, and re-layouts  6.66 us (4%)
    all_to_all x1, blocking collectives, forward(): lax.all_to_all(expert_rows.reshape(expert_count, capacity, chunks, LANES)...  48.5 us
    ppermute x3, waiting for transfers between devices, forward(): second = lax.ppermute(first, ALL, relay)  22.5 us
    ppermute x6, waiting for transfers between devices, pass_on(): return lax.ppermute(array, TP, pairs)  22.5 us
    all_to_all x1, starting transfers between devices, forward(): arrived = lax.all_to_all(send, ('pair', 'yl'), 0, 0, tiled=True)  12.7 us
    ppermute x6, starting transfers between devices, pass_on(): return lax.ppermute(array, TP, pairs)  8.71 us
    ppermute x3, starting transfers between devices, forward(): first = lax.ppermute(array, ALL, near)  6.84 us
    ppermute x3, starting transfers between devices, forward(): last = lax.ppermute(second, ALL, over)  6.8 us
    pallas_call x1, Pallas kernels, forward(): pl.pallas_call(functools.partial(hidden_kernel, slots, model_width, ff, i...  5.21 us
  transfers between devices with their start and end apart: 20, of which 6 were waited for; matrix products, arithmetic and copies ran while one was open for 6% of the time, Pallas kernels for 8%

profile of v5, /device:TPU:2, one launch (start us, length us, event | category | flops | bytes accessed | tf_op | source)
XLA Modules:
  0.0 172.7 jit_solution(3334049770956426487)
XLA Ops:
  0.0 0.7 convert_element_type.30
  0.7 0.1 slice.16
  0.8 0.7 slice.15
  1.5 0.1 broadcast_in_dim.33
  1.6 1.9 %collective-permute-start = (bf16[16,384]{1,0:T(8,128)(2,1)S(1)}, bf16[16,384]{1,0:T(8,128)(2,1)S(1)}, u32[]{:S(2)}, u32[]{:S(2)}) collective-permute-start(bf16[16,384]{1,0:T(8,128)(2,1)S(1)} %pad_maximum_fusion), channel_id=1, source_target_pairs={{0,4},{4,8},{8,12},{12,16},{16,20},{20,24},{24,28},{28,32},{32,36}... | collective-permute-start | bytes 36872 | tf_op jit(solution)/shard_map/ppermute | solution.py:236
  3.5 3.1 %collective-permute-start.9 = (bf16[2048,256]{1,0:T(8,128)(2,1)}, bf16[2048,256]{1,0:T(8,128)(2,1)}, u32[]{:S(2)}, u32[]{:S(2)}) collective-permute-start(bf16[2048,256]{1,0:T(8,128)(2,1)} %bitcast.36), channel_id=1, source_target_pairs={{0,3},{5,6},{6,5},{3,0},{8,11},{13,14},{14,13},{11,8},{16,19},{21,... | collective-permute-start | bytes 3145736 | tf_op jit(solution)/shard_map/ppermute | solution.py:272
  6.6 0.2 collective-permute-start.7
  6.8 0.1 copy.17
  6.9 0.1 eq.50
  7.1 0.6 reduce-window.6
  7.7 0.2 slice_reduce_fusion
  7.9 0.1 reshape.85
  8.1 0.0 collective-permute-done.prior_ref
  8.1 0.8 broadcast_in_dim.32.docs_ref
  8.9 4.6 %mix.1 = (bf16[128,2048]{1,0:T(8,128)(2,1)}, bf16[128,1024]{1,0:T(8,128)(2,1)}, bf16[128,1024]{1,0:T(8,128)(2,1)}, bf16[128,1024]{1,0:T(8,128)(2,1)}, bf16[128,1...) custom-call(bf16[512,256]{1,0:T(8,128)(2,1)} %pool_ref.1, ...), custom_call_target="tpu_custom_call" | custom-call | tf_op jit(solution)/shard_map/mix/pallas_call | solution.py:238
  13.5 3.3 %collective-permute-start.4 = (bf16[128,1024]{1,0:T(8,128)(2,1)}, bf16[128,1024]{1,0:T(8,128)(2,1)S(1)}, u32[]{:S(2)}, u32[]{:S(2)}) collective-permute-start(bf16[128,1024]{1,0:T(8,128)(2,1)} %get-tuple-element.19), channel_id=1, source_target_pairs={{0,3},{1,0},{2,1},{3,2},{4,7},{5,4},{6,5},{7,6},{8,11},{9,8},{10,9... | collective-permute-start | bytes 786440 | tf_op jit(solution)/shard_map/ppermute | solution.py:258
  16.8 0.1 fusion.2
  16.9 0.1 collective-permute-start.2
  17.0 0.1 collective-permute-start.1
  17.1 19.5 %collective-permute-done.4 = bf16[128,1024]{1,0:T(8,128)(2,1)S(1)} collective-permute-done((bf16[128,1024]{1,0:T(8,128)(2,1)}, bf16[128,1024]{1,0:T(8,128)(2,1)S(1)}, u32[]{:S(2)}, u32[]{:S(2)}) %collective-permute-start.4) | collective-permute-done | bytes 262176 | tf_op jit(solution)/shard_map/ppermute | solution.py:258
  36.6 3.0 %collective-permute-start.6 = (bf16[128,1024]{1,0:T(8,128)(2,1)}, bf16[128,1024]{1,0:T(8,128)(2,1)S(1)}, u32[]{:S(2)}, u32[]{:S(2)}) collective-permute-start(bf16[128,1024]{1,0:T(8,128)(2,1)} %get-tuple-element.20), channel_id=1, source_target_pairs={{0,3},{1,0},{2,1},{3,2},{4,7},{5,4},{6,5},{7,6},{8,11},{9,8},{10,9... | collective-permute-start | bytes 786440 | tf_op jit(solution)/shard_map/ppermute | solution.py:258
  39.6 1.0 add_convert_fusion
  40.7 0.0 collective-permute-done.2
  40.7 1.8 %collective-permute-start.5 = (bf16[128,1024]{1,0:T(8,128)(2,1)S(1)}, bf16[128,1024]{1,0:T(8,128)(2,1)S(1)}, u32[]{:S(2)}, u32[]{:S(2)}) collective-permute-start(bf16[128,1024]{1,0:T(8,128)(2,1)S(1)} %add_convert_fusion), channel_id=1, source_target_pairs={{0,3},{1,0},{2,1},{3,2},{4,7},{5,4},{6,5},{7,6},{8,11},{9,8},{10,9... | collective-permute-start | bytes 786440 | tf_op jit(solution)/shard_map/ppermute | solution.py:258
  42.4 1.0 add_convert_fusion.1
  43.5 0.0 collective-permute-done.1.nl_ref
  43.5 0.4 collective-permute-start.3
  43.9 0.1 select_reduce_fusion
  44.0 2.0 %collective-permute-done.6.ph_ref = bf16[128,1024]{1,0:T(8,128)(2,1)S(1)} collective-permute-done((bf16[128,1024]{1,0:T(8,128)(2,1)}, bf16[128,1024]{1,0:T(8,128)(2,1)S(1)}, u32[]{:S(2)}, u32[]{:S(2)}) %collective-permute-start.6) | collective-permute-done | bytes 262176 | tf_op jit(solution)/shard_map/ppermute | solution.py:258
  46.0 3.5 %collective-permute-start.15 = (bf16[256,2048]{1,0:T(8,128)(2,1)}, bf16[256,2048]{1,0:T(8,128)(2,1)}, u32[]{:S(2)}, u32[]{:S(2)}) collective-permute-start(bf16[256,2048]{1,0:T(8,128)(2,1)} %bitcast.7.own), channel_id=1, source_target_pairs={{0,3},{5,6},{6,5},{3,0},{8,11},{13,14},{14,13},{11,8},{16,19},{21,... | collective-permute-start | bytes 3145736 | tf_op jit(solution)/shard_map/ppermute | solution.py:272
  49.5 0.6 add_select_fusion.tok_ref
  50.1 0.0 collective-permute-done.5.pl_ref
  50.1 1.0 collective-permute-done.3.nh_ref
  51.2 0.7 copy-done.9
  51.9 4.0 %dispatch.1 = (bf16[384,16,128]{2,1,0:T(8,128)(2,1)}, bf16[128,2048]{1,0:T(8,128)(2,1)}) custom-call(s32[384]{0:T(512)} %add_select_fusion.tok_ref, bf16[128,2048]{1,0:T(8,128)(2,1)} %get-tuple-element.14.own_ref, bf16[128,1024]{1,0:T(8,128)(2,1)} %copy-done.6, bf16[128,1024]{1,0:T(8,128)(2,1)} %copy-done.9, bf16[128,1024]{1,0:T(8,128)(2,1)} %copy-done.8, ...), custom_call_target="tpu_custom_call" | custom-call | tf_op jit(solution)/shard_map/dispatch/pallas_call | solution.py:281
  55.9 12.7 %all-to-all-start = ((bf16[64,6,16,128]{3,2,1,0:T(8,128)(2,1)}), bf16[64,6,16,128]{3,2,1,0:T(8,128)(2,1)S(1)}, u32[]{:S(2)}, u32[]{:S(2)}) async-start(bf16[64,6,16,128]{3,2,1,0:T(8,128)(2,1)} %bitcast.38), calls=%async_computation | async-start | bytes 3145728 | tf_op jit(solution)/shard_map/all_to_all | solution.py:297
  68.6 0.0 copy-start.1
  68.6 0.0 collective-permute-done.7.refs_4_
  68.6 0.1 collective-permute-start.11
  68.7 1.5 collective-permute-start.12
  70.2 1.3 broadcast_select_fusion.1
  71.6 0.7 collective-permute-start.10
  72.3 0.0 collective-permute-done.15.near
  72.3 0.1 collective-permute-start.17
  72.4 1.1 broadcast_select_fusion.2
  73.5 3.1 %collective-permute-start.8 = (bf16[2048,256]{1,0:T(8,128)(2,1)}, bf16[2048,256]{1,0:T(8,128)(2,1)}, u32[]{:S(2)}, u32[]{:S(2)}) collective-permute-start(bf16[2048,256]{1,0:T(8,128)(2,1)} %broadcast_select_fusion.2), channel_id=1, source_target_pairs={{0,4},{5,1},{6,2},{3,7},{8,12},{13,9},{14,10},{11,15},{16,20},{21,... | collective-permute-start | bytes 3145736 | tf_op jit(solution)/shard_map/ppermute | solution.py:274
  76.5 7.9 %collective-permute-done.11.refs_6_ = bf16[2048,256]{1,0:T(8,128)(2,1)} collective-permute-done((bf16[2048,256]{1,0:T(8,128)(2,1)}, bf16[2048,256]{1,0:T(8,128)(2,1)}, u32[]{:S(2)}, u32[]{:S(2)}) %collective-permute-start.11) | collective-permute-done | bytes 1048608 | tf_op jit(solution)/shard_map/ppermute | solution.py:273
  84.5 2.2 %collective-permute-start.13 = (bf16[2048,256]{1,0:T(8,128)(2,1)}, bf16[2048,256]{1,0:T(8,128)(2,1)}, u32[]{:S(2)}, u32[]{:S(2)}) collective-permute-start(bf16[2048,256]{1,0:T(8,128)(2,1)} %collective-permute-done.11.refs_6_), channel_id=1, source_target_pairs={{0,4},{5,1},{6,2},{3,7},{8,12},{13,9},{14,10},{11,15},{16,20},{21,... | collective-permute-start | bytes 3145736 | tf_op jit(solution)/shard_map/ppermute | solution.py:275
  86.7 9.0 %collective-permute-done.12.refs_7_ = bf16[2048,256]{1,0:T(8,128)(2,1)} collective-permute-done((bf16[2048,256]{1,0:T(8,128)(2,1)}, bf16[2048,256]{1,0:T(8,128)(2,1)}, u32[]{:S(2)}, u32[]{:S(2)}) %collective-permute-start.12) | collective-permute-done | bytes 1048608 | tf_op jit(solution)/shard_map/ppermute | solution.py:273
  95.7 2.3 %collective-permute-start.14 = (bf16[2048,256]{1,0:T(8,128)(2,1)}, bf16[2048,256]{1,0:T(8,128)(2,1)}, u32[]{:S(2)}, u32[]{:S(2)}) collective-permute-start(bf16[2048,256]{1,0:T(8,128)(2,1)} %collective-permute-done.12.refs_7_), channel_id=1, source_target_pairs={{0,4},{5,1},{6,2},{3,7},{8,12},{13,9},{14,10},{11,15},{16,20},{21,... | collective-permute-start | bytes 3145736 | tf_op jit(solution)/shard_map/ppermute | solution.py:275
  98.0 2.3 %broadcast_select_fusion = bf16[256,2048]{1,0:T(8,128)(2,1)} fusion(bf16[256,2048]{1,0:T(8,128)(2,1)} %collective-permute-done.15.near, pred[]{:T(512)S(6)} %eq.57, bf16[1,256,2048]{2,1,0:T(8,128)(2,1)} %param.23), kind=kLoop, calls=%fused_computation | loop fusion | flops 524288 | bytes 3145729 | tf_op jit(solution)/shard_map/jit(_where)/select_n | solution.py:274
  100.3 0.0 collective-permute-done.10.refs_3_
  100.3 1.0 copy-done.3
  101.3 5.6 %collective-permute-done.17.both = bf16[256,2048]{1,0:T(8,128)(2,1)} collective-permute-done((bf16[256,2048]{1,0:T(8,128)(2,1)}, bf16[256,2048]{1,0:T(8,128)(2,1)}, u32[]{:S(2)}, u32[]{:S(2)}) %collective-permute-start.17) | collective-permute-done | bytes 1048608 | tf_op jit(solution)/shard_map/ppermute | solution.py:273
  106.9 2.2 %collective-permute-start.18 = (bf16[256,2048]{1,0:T(8,128)(2,1)}, bf16[256,2048]{1,0:T(8,128)(2,1)}, u32[]{:S(2)}, u32[]{:S(2)}) collective-permute-start(bf16[256,2048]{1,0:T(8,128)(2,1)} %collective-permute-done.17.both), channel_id=1, source_target_pairs={{0,4},{5,1},{6,2},{3,7},{8,12},{13,9},{14,10},{11,15},{16,20},{21,... | collective-permute-start | bytes 3145736 | tf_op jit(solution)/shard_map/ppermute | solution.py:275
  109.2 0.1 copy.20
  109.3 0.1 reshape.87.after_ref.weight_ref
  109.5 0.0 copy-start.2
  109.5 1.2 copy-done.2
  110.7 1.2 copy-done.4
  111.9 5.2 %hidden.1.hidden_ref = bf16[384,1024]{1,0:T(8,128)(2,1)S(1)} custom-call(bf16[6144,128]{1,0:T(8,128)(2,1)S(1)} %bitcast.31, bf16[2048,256]{1,0:T(8,128)(2,1)S(1)} %bitcast.35, bf16[2048,256]{1,0:T(8,128)(2,1)S(1)} %bitcast.37, bf16[2048,256]{1,0:T(8,128)(2,1)} %collective-permute-done.8.refs_2_, bf16[2048,256]{1,0:T(8,128)(2,1)S(1)} %copy-done.4, ...), custom_call_target="tpu_custom_call" | custom-call | tf_op jit(solution)/shard_map/hidden/pallas_call | solution.py:301
  117.2 4.8 %down.1 = bf16[384,16,128]{2,1,0:T(8,128)(2,1)S(1)} custom-call(bf16[384,1024]{1,0:T(8,128)(2,1)S(1)} %hidden.1.hidden_ref, bf16[256,2048]{1,0:T(8,128)(2,1)} %bitcast.7.own, bf16[256,2048]{1,0:T(8,128)(2,1)} %collective-permute-done.16.swapped, bf16[256,2048]{1,0:T(8,128)(2,1)} %collective-permute-done.15.near, ...), custom_call_target="tpu_custom_call" | custom-call | tf_op jit(solution)/shard_map/down/pallas_call | solution.py:316
  122.0 48.5 %all_to_all.10 = bf16[64,6,16,128]{3,2,1,0:T(8,128)(2,1)S(1)} all-to-all(bf16[64,6,16,128]{3,2,1,0:T(8,128)(2,1)S(1)} %bitcast.33), channel_id=1, replica_groups=mesh['pair'=32,'core'=2,'yh'=2,'yl'=2] {'pair','yl'}, dimensions={0} | all-to-all | bytes 3145728 | tf_op jit(solution)/shard_map/all_to_all | solution.py:330
  170.5 2.2 %combine.1 = bf16[128,2048]{1,0:T(8,128)(2,1)} custom-call(s32[256]{0:T(256)S(1)} %multiply_add_fusion.pos_ref, f32[256]{0:T(256)S(1)} %reshape.87.after_ref.weight_ref, bf16[384,16,128]{2,1,0:T(8,128)(2,1)S(1)} %bitcast.32, bf16[128,2048]{1,0:T(8,128)(2,1)S(1)} %copy-done.5), custom_call_target="tpu_custom_call" | custom-call | tf_op jit(solution)/shard_map/combine/pallas_call | solution.py:333
  (32 shorter events, 0.1 us)
Async XLA Ops:
  0.0 6.8 %copy-start = (s32[512,2]{0,1:T(2,128)S(1)}, s32[512,2]{0,1:T(2,128)}, u32[]{:S(2)}) copy-start(s32[512,2]{0,1:T(2,128)} %param.19) | copy-start | bytes 12292
  1.6 6.5 %collective-permute-start = (bf16[16,384]{1,0:T(8,128)(2,1)S(1)}, bf16[16,384]{1,0:T(8,128)(2,1)S(1)}, u32[]{:S(2)}, u32[]{:S(2)}) collective-permute-start(bf16[16,384]{1,0:T(8,128)(2,1)S(1)} %pad_maximum_fusion), channel_id=1, source_target_pairs={{0,4},{4,8},{8,12},{12,16},{16,20},{20,24},{24,28},{28,32},{32,36}... | collective-permute-start | bytes 36872 | tf_op jit(solution)/shard_map/ppermute | solution.py:236
  3.5 65.3 %collective-permute-start.9 = (bf16[2048,256]{1,0:T(8,128)(2,1)}, bf16[2048,256]{1,0:T(8,128)(2,1)}, u32[]{:S(2)}, u32[]{:S(2)}) collective-permute-start(bf16[2048,256]{1,0:T(8,128)(2,1)} %bitcast.36), channel_id=1, source_target_pairs={{0,3},{5,6},{6,5},{3,0},{8,11},{13,14},{14,13},{11,8},{16,19},{21,... | collective-permute-start | bytes 3145736 | tf_op jit(solution)/shard_map/ppermute | solution.py:272
  6.6 62.0 %collective-permute-start.7 = (bf16[2048,256]{1,0:T(8,128)(2,1)}, bf16[2048,256]{1,0:T(8,128)(2,1)}, u32[]{:S(2)}, u32[]{:S(2)}) collective-permute-start(bf16[2048,256]{1,0:T(8,128)(2,1)} %bitcast.34), channel_id=1, source_target_pairs={{0,3},{5,6},{6,5},{3,0},{8,11},{13,14},{14,13},{11,8},{16,19},{21,... | collective-permute-start | bytes 3145736 | tf_op jit(solution)/shard_map/ppermute | solution.py:272
  8.1 0.8 copy-start.10
  13.5 23.1 %collective-permute-start.4 = (bf16[128,1024]{1,0:T(8,128)(2,1)}, bf16[128,1024]{1,0:T(8,128)(2,1)S(1)}, u32[]{:S(2)}, u32[]{:S(2)}) collective-permute-start(bf16[128,1024]{1,0:T(8,128)(2,1)} %get-tuple-element.19), channel_id=1, source_target_pairs={{0,3},{1,0},{2,1},{3,2},{4,7},{5,4},{6,5},{7,6},{8,11},{9,8},{10,9... | collective-permute-start | bytes 786440 | tf_op jit(solution)/shard_map/ppermute | solution.py:258
  16.9 23.7 %collective-permute-start.2 = (bf16[128,1024]{1,0:T(8,128)(2,1)}, bf16[128,1024]{1,0:T(8,128)(2,1)S(1)}, u32[]{:S(2)}, u32[]{:S(2)}) collective-permute-start(bf16[128,1024]{1,0:T(8,128)(2,1)} %get-tuple-element.17), channel_id=1, source_target_pairs={{0,1},{1,2},{2,3},{3,0},{4,5},{5,6},{6,7},{7,4},{8,9},{9,10},{10,1... | collective-permute-start | bytes 786440 | tf_op jit(solution)/shard_map/ppermute | solution.py:258
  17.0 26.4 %collective-permute-start.1 = (bf16[128,1024]{1,0:T(8,128)(2,1)}, bf16[128,1024]{1,0:T(8,128)(2,1)S(1)}, u32[]{:S(2)}, u32[]{:S(2)}) collective-permute-start(bf16[128,1024]{1,0:T(8,128)(2,1)} %get-tuple-element.15), channel_id=1, source_target_pairs={{0,1},{1,2},{2,3},{3,0},{4,5},{5,6},{6,7},{7,4},{8,9},{9,10},{10,1... | collective-permute-start | bytes 786440 | tf_op jit(solution)/shard_map/ppermute | solution.py:258
  36.6 9.4 %collective-permute-start.6 = (bf16[128,1024]{1,0:T(8,128)(2,1)}, bf16[128,1024]{1,0:T(8,128)(2,1)S(1)}, u32[]{:S(2)}, u32[]{:S(2)}) collective-permute-start(bf16[128,1024]{1,0:T(8,128)(2,1)} %get-tuple-element.20), channel_id=1, source_target_pairs={{0,3},{1,0},{2,1},{3,2},{4,7},{5,4},{6,5},{7,6},{8,11},{9,8},{10,9... | collective-permute-start | bytes 786440 | tf_op jit(solution)/shard_map/ppermute | solution.py:258
  40.7 9.4 %collective-permute-start.5 = (bf16[128,1024]{1,0:T(8,128)(2,1)S(1)}, bf16[128,1024]{1,0:T(8,128)(2,1)S(1)}, u32[]{:S(2)}, u32[]{:S(2)}) collective-permute-start(bf16[128,1024]{1,0:T(8,128)(2,1)S(1)} %add_convert_fusion), channel_id=1, source_target_pairs={{0,3},{1,0},{2,1},{3,2},{4,7},{5,4},{6,5},{7,6},{8,11},{9,8},{10,9... | collective-permute-start | bytes 786440 | tf_op jit(solution)/shard_map/ppermute | solution.py:258
  43.5 7.7 %copy-start.6 = (bf16[128,1024]{1,0:T(8,128)(2,1)}, bf16[128,1024]{1,0:T(8,128)(2,1)S(1)}, u32[]{:S(2)}) copy-start(bf16[128,1024]{1,0:T(8,128)(2,1)S(1)} %collective-permute-done.1.nl_ref) | copy-start | bytes 786436
  43.5 7.7 %collective-permute-start.3 = (bf16[128,1024]{1,0:T(8,128)(2,1)S(1)}, bf16[128,1024]{1,0:T(8,128)(2,1)S(1)}, u32[]{:S(2)}, u32[]{:S(2)}) collective-permute-start(bf16[128,1024]{1,0:T(8,128)(2,1)S(1)} %add_convert_fusion.1), channel_id=1, source_target_pairs={{0,1},{1,2},{2,3},{3,0},{4,5},{5,6},{6,7},{7,4},{8,9},{9,10},{10,1... | collective-permute-start | bytes 786440 | tf_op jit(solution)/shard_map/ppermute | solution.py:258
  46.0 5.1 %copy-start.7 = (bf16[128,1024]{1,0:T(8,128)(2,1)}, bf16[128,1024]{1,0:T(8,128)(2,1)S(1)}, u32[]{:S(2)}) copy-start(bf16[128,1024]{1,0:T(8,128)(2,1)S(1)} %collective-permute-done.6.ph_ref) | copy-start | bytes 786436
  46.0 26.3 %collective-permute-start.15 = (bf16[256,2048]{1,0:T(8,128)(2,1)}, bf16[256,2048]{1,0:T(8,128)(2,1)}, u32[]{:S(2)}, u32[]{:S(2)}) collective-permute-start(bf16[256,2048]{1,0:T(8,128)(2,1)} %bitcast.7.own), channel_id=1, source_target_pairs={{0,3},{5,6},{6,5},{3,0},{8,11},{13,14},{14,13},{11,8},{16,19},{21,... | collective-permute-start | bytes 3145736 | tf_op jit(solution)/shard_map/ppermute | solution.py:272
  50.1 1.0 copy-start.8
  51.1 0.7 copy-start.9
  55.9 53.6 %all-to-all-start = ((bf16[64,6,16,128]{3,2,1,0:T(8,128)(2,1)}), bf16[64,6,16,128]{3,2,1,0:T(8,128)(2,1)S(1)}, u32[]{:S(2)}, u32[]{:S(2)}) async-start(bf16[64,6,16,128]{3,2,1,0:T(8,128)(2,1)} %bitcast.38), calls=%async_computation | async-start | bytes 3145728 | tf_op jit(solution)/shard_map/all_to_all | solution.py:297
  68.6 3.8 %copy-start.1 = (bf16[1,2048,256]{2,1,0:T(8,128)(2,1)S(1)}, bf16[1,2048,256]{2,1,0:T(8,128)(2,1)}, u32[]{:S(2)}) copy-start(bf16[1,2048,256]{2,1,0:T(8,128)(2,1)} %param.21) | copy-start | bytes 3145732
  68.6 15.8 %collective-permute-start.11 = (bf16[2048,256]{1,0:T(8,128)(2,1)}, bf16[2048,256]{1,0:T(8,128)(2,1)}, u32[]{:S(2)}, u32[]{:S(2)}) collective-permute-start(bf16[2048,256]{1,0:T(8,128)(2,1)} %collective-permute-done.7.refs_4_), channel_id=1, source_target_pairs={{4,3},{1,6},{2,5},{7,0},{12,11},{9,14},{10,13},{15,8},{20,19},{17,... | collective-permute-start | bytes 3145736 | tf_op jit(solution)/shard_map/ppermute | solution.py:273
  68.7 27.0 %collective-permute-start.12 = (bf16[2048,256]{1,0:T(8,128)(2,1)}, bf16[2048,256]{1,0:T(8,128)(2,1)}, u32[]{:S(2)}, u32[]{:S(2)}) collective-permute-start(bf16[2048,256]{1,0:T(8,128)(2,1)} %collective-permute-done.9.refs_5_), channel_id=1, source_target_pairs={{4,3},{1,6},{2,5},{7,0},{12,11},{9,14},{10,13},{15,8},{20,19},{17,... | collective-permute-start | bytes 3145736 | tf_op jit(solution)/shard_map/ppermute | solution.py:273
  71.6 28.7 %collective-permute-start.10 = (bf16[2048,256]{1,0:T(8,128)(2,1)S(1)}, bf16[2048,256]{1,0:T(8,128)(2,1)S(1)}, u32[]{:S(2)}, u32[]{:S(2)}) collective-permute-start(bf16[2048,256]{1,0:T(8,128)(2,1)S(1)} %broadcast_select_fusion.1), channel_id=1, source_target_pairs={{0,4},{5,1},{6,2},{3,7},{8,12},{13,9},{14,10},{11,15},{16,20},{21,... | collective-permute-start | bytes 3145736 | tf_op jit(solution)/shard_map/ppermute | solution.py:274
  72.3 34.7 %collective-permute-start.17 = (bf16[256,2048]{1,0:T(8,128)(2,1)}, bf16[256,2048]{1,0:T(8,128)(2,1)}, u32[]{:S(2)}, u32[]{:S(2)}) collective-permute-start(bf16[256,2048]{1,0:T(8,128)(2,1)} %collective-permute-done.15.near), channel_id=1, source_target_pairs={{4,3},{1,6},{2,5},{7,0},{12,11},{9,14},{10,13},{15,8},{20,19},{17,... | collective-permute-start | bytes 3145736 | tf_op jit(solution)/shard_map/ppermute | solution.py:273
  73.5 35.7 %copy-start.11 = (f32[128,2]{0,1:T(2,128)S(1)}, f32[128,2]{0,1:T(2,128)}, u32[]{:S(2)}) copy-start(f32[128,2]{0,1:T(2,128)} %param.20) | copy-start | bytes 3076
  73.5 36.0 %collective-permute-start.8 = (bf16[2048,256]{1,0:T(8,128)(2,1)}, bf16[2048,256]{1,0:T(8,128)(2,1)}, u32[]{:S(2)}, u32[]{:S(2)}) collective-permute-start(bf16[2048,256]{1,0:T(8,128)(2,1)} %broadcast_select_fusion.2), channel_id=1, source_target_pairs={{0,4},{5,1},{6,2},{3,7},{8,12},{13,9},{14,10},{11,15},{16,20},{21,... | collective-permute-start | bytes 3145736 | tf_op jit(solution)/shard_map/ppermute | solution.py:274
  84.5 25.0 %collective-permute-start.13 = (bf16[2048,256]{1,0:T(8,128)(2,1)}, bf16[2048,256]{1,0:T(8,128)(2,1)}, u32[]{:S(2)}, u32[]{:S(2)}) collective-permute-start(bf16[2048,256]{1,0:T(8,128)(2,1)} %collective-permute-done.11.refs_6_), channel_id=1, source_target_pairs={{0,4},{5,1},{6,2},{3,7},{8,12},{13,9},{14,10},{11,15},{16,20},{21,... | collective-permute-start | bytes 3145736 | tf_op jit(solution)/shard_map/ppermute | solution.py:275
  95.7 13.8 %collective-permute-start.14 = (bf16[2048,256]{1,0:T(8,128)(2,1)}, bf16[2048,256]{1,0:T(8,128)(2,1)}, u32[]{:S(2)}, u32[]{:S(2)}) collective-permute-start(bf16[2048,256]{1,0:T(8,128)(2,1)} %collective-permute-done.12.refs_7_), channel_id=1, source_target_pairs={{0,4},{5,1},{6,2},{3,7},{8,12},{13,9},{14,10},{11,15},{16,20},{21,... | collective-permute-start | bytes 3145736 | tf_op jit(solution)/shard_map/ppermute | solution.py:275
  100.3 1.0 copy-start.3
  101.3 15.8 %collective-permute-start.16 = (bf16[256,2048]{1,0:T(8,128)(2,1)}, bf16[256,2048]{1,0:T(8,128)(2,1)}, u32[]{:S(2)}, u32[]{:S(2)}) collective-permute-start(bf16[256,2048]{1,0:T(8,128)(2,1)} %broadcast_select_fusion), channel_id=1, source_target_pairs={{0,4},{5,1},{6,2},{3,7},{8,12},{13,9},{14,10},{11,15},{16,20},{21,... | collective-permute-start | bytes 3145736 | tf_op jit(solution)/shard_map/ppermute | solution.py:274
  106.9 10.2 %collective-permute-start.18 = (bf16[256,2048]{1,0:T(8,128)(2,1)}, bf16[256,2048]{1,0:T(8,128)(2,1)}, u32[]{:S(2)}, u32[]{:S(2)}) collective-permute-start(bf16[256,2048]{1,0:T(8,128)(2,1)} %collective-permute-done.17.both), channel_id=1, source_target_pairs={{0,4},{5,1},{6,2},{3,7},{8,12},{13,9},{14,10},{11,15},{16,20},{21,... | collective-permute-start | bytes 3145736 | tf_op jit(solution)/shard_map/ppermute | solution.py:275
  109.5 1.2 copy-start.2
  110.7 1.2 copy-start.4
  122.0 48.5 %copy-start.5 = (bf16[128,2048]{1,0:T(8,128)(2,1)S(1)}, bf16[128,2048]{1,0:T(8,128)(2,1)}, u32[]{:S(2)}) copy-start(bf16[128,2048]{1,0:T(8,128)(2,1)} %get-tuple-element.22.mixed_ref) | copy-start | bytes 1572868
